TPU v7x, 32 devices: a whole 2x2x4 slice. The times are simulated.
32 devices in a mesh: sp: 4 (over y, x), tp: 8 (over z, core).
Axes of the slice: x: 2, y: 2, z: 4, core: 2. Of those that a mesh axis runs over, the one named last changes fastest.
Arguments:
- query_heads: bfloat16 [4096, 2048], P('sp', 'tp'), may hold values from -256 to 256
- key_heads: bfloat16 [4096, 1024], P('sp', 'tp'), may hold values from -7 to 7
- value_heads: bfloat16 [4096, 1024], P('sp', 'tp'), may hold values from -6 to 6
- sink_logit: float32 [32], P('tp'), may hold values from 3 to 7
- residual: bfloat16 [4096, 2048], P(('sp', 'tp')), may hold values from -6 to 6
- out_weight: bfloat16 [2048, 2048], replicated, may hold values from -0.5 to 0.5
- norm_gain: float32 [2048], replicated, may hold values from 0.1 to 1.9
- routes: int32 [4096, 2], P('sp'), may hold values from 0 to 3, all different within a row; in each aligned block of 128 rows (0 to 127, 128 to 255, ...) at most 80 rows name the same one
- route_weight: float32 [4096, 2], P(('sp', 'tp')), may hold values from 0.2 to 1
- gate_weight: bfloat16 [4, 2048, 2048], P('sp', None, 'tp'), may hold values from -0.3125 to 0.3125
- up_weight: bfloat16 [4, 2048, 2048], P('sp', None, 'tp'), may hold values from -0.3125 to 0.3125
- down_weight: bfloat16 [4, 2048, 2048], P('sp', 'tp'), may hold values from -0.0625 to 0.0625
Outputs:
- updated: bfloat16 [4096, 2048], P(('sp', 'tp'))
Inputs may be any that keep to these rules, and one draw needn't show every extreme that they name: `routes`: each row names 2 different experts. In each aligned block of 128 rows no expert is named more than 80 times, and in every draw some block names some expert exactly 80 times.
All inputs are finite; a program needn't handle non-finite values.
Results may differ from a plain program's by a relative error of at most 0.023.
Values may be sent and summed in bfloat16 or wider, within the bound.
No kernel may reach another device: no remote copies, remote signals or barrier semaphores. Data moves between devices by JAX's collectives and lax.ppermute only.
A program may use at most 128 MiB of HBM per device.

v0:
```python
import jax
import jax.numpy as jnp
from jax import lax
from jax.sharding import PartitionSpec as P

HEAD = 64
WINDOW = 128


eps = 1e-06
clamp_limit = 7.0
sigmoid_alpha = 1.702


def from_behind(block, axis, distance):
    devices = range(lax.axis_size(axis))
    route = [(i - distance, i) for i in devices if i - distance in devices]
    return lax.ppermute(block, axis, route)


def expert_hidden(row_block, gate_local, up_local):
    gate_pre = jnp.dot(row_block, gate_local, preferred_element_type=jnp.float32)
    upward = jnp.dot(row_block, up_local, preferred_element_type=jnp.float32)
    capped = jnp.minimum(gate_pre, clamp_limit)
    linear = jnp.clip(upward, -clamp_limit, clamp_limit)
    return (capped * jax.nn.sigmoid(sigmoid_alpha * capped) * (linear + 1.0)).astype(jnp.bfloat16)


def slot_layout(own_routes, expert_count, capacity):
    flat_ids = own_routes.reshape(-1)
    one_hot = (flat_ids[:, None] == jnp.arange(expert_count, dtype=jnp.int32)[None, :]).astype(
        jnp.int32
    )
    before = jnp.cumsum(one_hot, axis=0) - one_hot
    ranked = jnp.sum(before * one_hot, axis=1)
    return flat_ids * capacity + ranked


def fill_slots(normed_rows, slot_ids, expert_count, capacity, choose_count):
    targets = jnp.arange(expert_count * capacity, dtype=jnp.int32)
    matched = (targets[:, None] == slot_ids[None, :]).astype(jnp.bfloat16)
    repeated = jnp.repeat(normed_rows, choose_count, axis=0)
    filled = jnp.dot(matched, repeated, preferred_element_type=jnp.float32).astype(jnp.bfloat16)
    return filled.reshape(expert_count, capacity, normed_rows.shape[1])


def local(
    query_heads,
    key_heads,
    value_heads,
    sink_logit,
    residual,
    out_weight,
    norm_gain,
    routes,
    route_weight,
    gate_weight,
    up_weight,
    down_weight,
):
    sp_count = lax.axis_size("sp")
    span_rows = query_heads.shape[0]
    kv_local = key_heads.shape[1] // HEAD
    group_size = query_heads.shape[1] // key_heads.shape[1]
    block_count = span_rows // WINDOW
    key_tail, value_tail = from_behind(
        (key_heads[span_rows - WINDOW :], value_heads[span_rows - WINDOW :]), "sp", 1
    )

    def banded(current, tail):
        shaped = current.reshape(block_count, WINDOW, kv_local, HEAD)
        earlier = jnp.concatenate([tail.reshape(1, WINDOW, kv_local, HEAD), shaped[:-1]], axis=0)
        return jnp.concatenate([earlier, shaped], axis=1)

    key_band = banded(key_heads, key_tail)
    value_band = banded(value_heads, value_tail)
    query_blocks = query_heads.reshape(block_count, WINDOW, kv_local, group_size, HEAD)
    scores = jnp.einsum(
        "nqhgd,nkhd->nhgqk", query_blocks, key_band, preferred_element_type=jnp.float32
    ) * HEAD ** (-0.5)
    query_pos = jnp.arange(WINDOW)[:, None]
    key_col = jnp.arange(2 * WINDOW)[None, :]
    distance = query_pos + WINDOW - key_col
    block_ids = jnp.arange(block_count)[:, None, None]
    key_global = lax.axis_index("sp") * span_rows + (block_ids - 1) * WINDOW + key_col[None]
    allowed = (distance[None] >= 0) & (distance[None] < WINDOW) & (key_global >= 0)
    logits = jnp.where(allowed[:, None, None], scores, -jnp.inf)
    sink_term = sink_logit.reshape(kv_local, group_size)[None, :, :, None, None]
    row_max = jnp.maximum(jnp.max(logits, axis=-1, keepdims=True), sink_term)
    raised = jnp.exp(logits - row_max)
    weights_bf = (
        raised / (jnp.sum(raised, axis=-1, keepdims=True) + jnp.exp(sink_term - row_max))
    ).astype(jnp.bfloat16)
    attended = jnp.einsum(
        "nhgqk,nkhd->nqhgd", weights_bf, value_band, preferred_element_type=jnp.float32
    )
    attended = attended.astype(jnp.bfloat16).reshape(span_rows, query_heads.shape[1])
    tok_rows = residual.shape[0]
    tp_index = lax.axis_index("tp")
    token_heads = lax.all_to_all(attended, "tp", split_axis=0, concat_axis=1, tiled=True)
    mixed = jnp.dot(token_heads, out_weight, preferred_element_type=jnp.float32)
    stream = (residual.astype(jnp.float32) + mixed).astype(jnp.bfloat16)
    stream32 = stream.astype(jnp.float32)
    normed = (
        stream32
        * lax.rsqrt(jnp.mean(stream32 * stream32, axis=-1, keepdims=True) + eps)
        * norm_gain
    ).astype(jnp.bfloat16)
    choose_count = routes.shape[1]
    capacity = max(2, 5 * tok_rows * choose_count // (4 * sp_count))
    model_width = normed.shape[1]
    gate_local = gate_weight[0]
    up_local = up_weight[0]
    down_local = down_weight[0]
    own_routes = lax.dynamic_slice_in_dim(routes, tp_index * tok_rows, tok_rows, 0)
    own_slots = slot_layout(own_routes, sp_count, capacity)
    outgoing = fill_slots(normed, own_slots, sp_count, capacity, choose_count)
    arrived = lax.all_to_all(outgoing, "sp", split_axis=0, concat_axis=0, tiled=True)
    hidden = expert_hidden(
        lax.all_gather(arrived[None], "tp", axis=0, tiled=True).reshape(-1, model_width),
        gate_local,
        up_local,
    )
    summed = lax.psum_scatter(
        jnp.dot(hidden, down_local, preferred_element_type=jnp.float32).astype(jnp.bfloat16),
        "tp",
        scatter_dimension=0,
        tiled=True,
    )
    expert_out = summed.reshape(sp_count, capacity, model_width)
    returned = lax.all_to_all(expert_out, "sp", split_axis=0, concat_axis=0, tiled=True)
    picked = returned.reshape(-1, model_width)[own_slots].reshape(
        tok_rows, choose_count, model_width
    )
    combined = jnp.sum(picked.astype(jnp.float32) * route_weight[:, :, None], axis=1)
    return (stream32 + combined).astype(jnp.bfloat16)


def solution(mesh):
    placed = (
        P("sp", "tp"),
        P("sp", "tp"),
        P("sp", "tp"),
        P("tp"),
        P(("sp", "tp"), None),
        P(),
        P(),
        P("sp", None),
        P(("sp", "tp"), None),
        P("sp", None, "tp"),
        P("sp", None, "tp"),
        P("sp", "tp", None),
    )
    return jax.shard_map(
        local, mesh=mesh, in_specs=placed, out_specs=P(("sp", "tp"), None), check_vma=False
    )
```

profile of v0, /device:TPU:0, one launch (start us, length us, event | category | flops | bytes accessed | tf_op | source)
XLA Modules:
  0.0 353.1 jit_solution(9478695877296077979)
XLA Ops:
  6.5 1.5 slice.27
  8.0 5.5 %collective-permute-start.1 = (bf16[128,128]{1,0:T(8,128)(2,1)}, bf16[128,128]{1,0:T(8,128)(2,1)}, u32[]{:S(2)}, u32[]{:S(2)}) collective-permute-start(bf16[128,128]{1,0:T(8,128)(2,1)} %slice.27), channel_id=1, source_target_pairs={{0,8},{8,16},{16,24},{1,9},{9,17},{17,25},{2,10},{10,18},{18,26},{... | collective-permute-start | bytes 98312 | tf_op jit(solution)/shard_map/ppermute | solution.py:18
  13.5 1.4 slice.24
  14.9 2.8 collective-permute-start
  17.8 0.3 broadcast_and_fusion
  18.2 1.2 reshape.215
  19.4 1.2 reshape.213
  20.6 3.2 reshape.216
  23.8 0.2 reshape.214
  24.0 0.9 copy.46
  25.0 0.4 copy.48
  25.4 0.2 reshape.212
  25.6 0.9 copy.41
  26.6 0.4 copy.43
  26.9 0.9 copy.44
  27.8 2.2 fusion.4
  30.0 1.8 copy-done.1
  31.9 1.0 fusion.3
  33.0 0.1 copy.39
  33.1 4.2 %fusion.8 = bf16[8,2,64,2,128]{4,2,3,1,0:T(8,128)(2,1)} fusion(f32[8,2,256,128,2]{3,2,4,1,0:T(8,128)} %copy-done.1, f32[8,2,2,128]{3,2,1,0:T(2,128)S(1)} %exponential_add_fusion, f32[8,2,2,128]{3,2,1,0:T(2,128)S(1)} %broadcast_maximum_fusion, pred[8,128,256]{1,2,0:T(8,128)(4,1)S(1)} %broadcast_and_fusion, bf16[8,128,2,64]{1,3,2,0:T(8,128)(2,1)S(1)} %copy.43, ...), kind=kOutput, calls=%fused_computation.18 | convolution fusion | flops 141295616 | bytes 5537792 | tf_op jit(solution)/shard_map/nhgqk,nkhd->nqhgd/dot_general | solution.py:94
  37.3 4.9 %all-to-all-start = ((bf16[8,128,256]{1,2,0:T(8,128)(2,1)}), bf16[8,128,256]{1,2,0:T(8,128)(2,1)S(1)}, u32[]{:S(2)}, u32[]{:S(2)}) async-start(bf16[8,128,256]{1,2,0:T(8,128)(2,1)} %bitcast.8), calls=%async_computation | async-start | bytes 1048576 | tf_op jit(solution)/shard_map/all_to_all | solution.py:100
  42.2 0.7 broadcast_multiply_fusion
  42.9 0.1 copy.52
  43.0 0.1 eq.40
  43.2 0.1 reshape.192
  43.3 1.2 reduce-window.6
  44.6 0.1 copy.54
  45.0 12.5 %all-to-all-done = bf16[8,128,256]{1,2,0:T(8,128)(2,1)S(1)} async-done(((bf16[8,128,256]{1,2,0:T(8,128)(2,1)}), bf16[8,128,256]{1,2,0:T(8,128)(2,1)S(1)}, u32[]{:S(2)}, u32[]{:S(2)}) %all-to-all-start) | async-done | bytes 524320 | tf_op jit(solution)/shard_map/all_to_all | solution.py:100
  57.5 4.8 %multiply_reduce_fusion.1 = (f32[128]{0:T(128)S(1)}, f32[128,2048]{1,0:T(8,128)S(1)}) fusion(bf16[128,2048]{0,1:T(8,128)(2,1)S(1)} %bitcast.74, bf16[2048,2048]{1,0:T(8,128)(2,1)} %param.17, bf16[128,2048]{1,0:T(8,128)(2,1)} %param.16), kind=kOutput, calls=%fused_computation.26 | convolution fusion | flops 1075314560 | bytes 10486272 | tf_op jit(solution)/shard_map/dot_general | solution.py:101
  62.3 0.2 multiply_convert_fusion
  62.5 1.6 broadcast_in_dim.18
  64.1 1.5 reshape.194
  65.6 0.5 convolution_convert_fusion.1
  66.1 20.1 %all_to_all.29 = bf16[4,80,2048]{2,1,0:T(8,128)(2,1)} all-to-all(bf16[4,80,2048]{2,1,0:T(8,128)(2,1)S(1)} %bitcast.73), channel_id=1, replica_groups=mesh['sp'=4,'tp'=8] {'sp'}, dimensions={0} | all-to-all | bytes 2621440 | tf_op jit(solution)/shard_map/all_to_all | solution.py:118
  86.2 0.2 reduce-scatter.2.cloned.1.call-start
  86.5 97.2 %all-gather.3.cloned.1.call-done = bf16[32,80,2048]{2,1,0:T(8,128)(2,1)} async-done(((bf16[4,80,2048]{2,1,0:T(8,128)(2,1)}), bf16[32,80,2048]{2,1,0:T(8,128)(2,1)}) %all-gather.3.cloned.1.call-update) | async-done | bytes 10485776 | tf_op jit(solution)/shard_map/all_gather | solution.py:120
  183.7 8.7 %convolution_minimum_fusion = f32[2560,256]{1,0:T(8,128)} fusion(bf16[2560,2048]{1,0:T(8,128)(2,1)} %bitcast.81, bf16[1,2048,256]{2,1,0:T(8,128)(2,1)} %param.21), kind=kOutput, calls=%fused_computation.6 | convolution fusion | flops 2685009920 | bytes 14155776 | tf_op jit(solution)/shard_map/dot_general | solution.py:22
  192.4 16.1 %convolution_convert_fusion = bf16[2560,2048]{1,0:T(8,128)(2,1)} fusion(bf16[1,256,2048]{2,1,0:T(8,128)(2,1)S(1)} %copy-done, bf16[2560,2048]{1,0:T(8,128)(2,1)} %bitcast.82, f32[2560,256]{1,0:T(8,128)} %convolution_minimum_fusion, bf16[1,2048,256]{2,1,0:T(8,128)(2,1)S(1)} %copy-done.4), kind=kOutput, calls=%fused_computation.1 | convolution fusion | flops 5379850240 | bytes 25690112 | tf_op jit(solution)/shard_map/dot_general | solution.py:125
  208.6 107.8 %reduce-scatter.2.cloned.1.call-done = bf16[320,2048]{1,0:T(8,128)(2,1)} async-done(((bf16[2560,2048]{1,0:T(8,128)(2,1)}), bf16[320,2048]{1,0:T(8,128)(2,1)}) %reduce-scatter.2.cloned.1.call-update) | async-done | bytes 1310736 | tf_op jit(solution)/shard_map/reduce_scatter | solution.py:124
  316.4 3.8 %all-to-all-start.2 = ((bf16[4,80,2048]{2,1,0:T(8,128)(2,1)}), bf16[4,80,2048]{2,1,0:T(8,128)(2,1)S(1)}, u32[]{:S(2)}, u32[]{:S(2)}) async-start(bf16[4,80,2048]{2,1,0:T(8,128)(2,1)} %bitcast.75), calls=%async_computation.3 | async-start | bytes 2621440 | tf_op jit(solution)/shard_map/all_to_all | solution.py:131
  320.1 0.1 copy.56
  320.3 0.1 mul.109
  320.4 0.1 copy.57
  320.5 14.2 %all-to-all-done.2 = bf16[4,80,2048]{2,1,0:T(8,128)(2,1)S(1)} async-done(((bf16[4,80,2048]{2,1,0:T(8,128)(2,1)}), bf16[4,80,2048]{2,1,0:T(8,128)(2,1)S(1)}, u32[]{:S(2)}, u32[]{:S(2)}) %all-to-all-start.2) | async-done | bytes 1310752 | tf_op jit(solution)/shard_map/all_to_all | solution.py:131
  334.8 2.3 gather_fusion
  337.1 3.4 reshape.199
  340.5 4.8 %multiply_reduce_fusion = f32[128,2048]{1,0:T(8,128)S(1)} fusion(f32[128,2,2048]{2,1,0:T(2,128)} %reshape.199, f32[128,2]{1,0:T(8,128)S(1)} %copy.57), kind=kLoop, calls=%fused_computation.16 | loop fusion | flops 786432 | bytes 3146752 | tf_op jit(solution)/shard_map/reduce_sum | solution.py:135
  345.3 0.9 add_convert_fusion
  (38 shorter events, 0.8 us)
Async XLA Ops:
  6.5 185.9 %copy-start = (bf16[1,256,2048]{2,1,0:T(8,128)(2,1)S(1)}, bf16[1,256,2048]{2,1,0:T(8,128)(2,1)}, u32[]{:S(2)}) copy-start(bf16[1,256,2048]{2,1,0:T(8,128)(2,1)} %param.23) | copy-start | bytes 3145732
  6.5 17.3 %slice-start = ((bf16[1024,128]{1,0:T(8,128)(2,1)}), bf16[896,128]{1,0:T(8,128)(2,1)S(1)}, s32[]{:S(2)}) async-start(bf16[1024,128]{1,0:T(8,128)(2,1)} %param.13), calls=%async_computation.6 | async-start | bytes 458752 | tf_op jit(solution)/shard_map/slice | solution.py:72
  6.5 18.9 %slice-start.1 = ((bf16[1024,128]{1,0:T(8,128)(2,1)}), bf16[896,128]{1,0:T(8,128)(2,1)S(1)}, s32[]{:S(2)}) async-start(bf16[1024,128]{1,0:T(8,128)(2,1)} %param.14), calls=%async_computation.7 | async-start | bytes 458752 | tf_op jit(solution)/shard_map/slice | solution.py:72
  6.5 18.8 %copy-start.5 = (f32[4]{0:T(128)S(1)}, f32[4]{0:T(128)}, u32[]{:S(2)}) copy-start(f32[4]{0:T(128)} %param.15) | copy-start | bytes 52
  8.0 18.9 %collective-permute-start.1 = (bf16[128,128]{1,0:T(8,128)(2,1)}, bf16[128,128]{1,0:T(8,128)(2,1)}, u32[]{:S(2)}, u32[]{:S(2)}) collective-permute-start(bf16[128,128]{1,0:T(8,128)(2,1)} %slice.27), channel_id=1, source_target_pairs={{0,8},{8,16},{16,24},{1,9},{9,17},{17,25},{2,10},{10,18},{18,26},{... | collective-permute-start | bytes 98312 | tf_op jit(solution)/shard_map/ppermute | solution.py:18
  14.9 18.1 %collective-permute-start = (bf16[128,128]{1,0:T(8,128)(2,1)}, bf16[128,128]{1,0:T(8,128)(2,1)S(1)}, u32[]{:S(2)}, u32[]{:S(2)}) collective-permute-start(bf16[128,128]{1,0:T(8,128)(2,1)} %slice.24), channel_id=1, source_target_pairs={{0,8},{8,16},{16,24},{1,9},{9,17},{17,25},{2,10},{10,18},{18,26},{... | collective-permute-start | bytes 98312 | tf_op jit(solution)/shard_map/ppermute | solution.py:18
  30.0 1.9 copy-start.1
  37.3 20.2 %all-to-all-start = ((bf16[8,128,256]{1,2,0:T(8,128)(2,1)}), bf16[8,128,256]{1,2,0:T(8,128)(2,1)S(1)}, u32[]{:S(2)}, u32[]{:S(2)}) async-start(bf16[8,128,256]{1,2,0:T(8,128)(2,1)} %bitcast.8), calls=%async_computation | async-start | bytes 1048576 | tf_op jit(solution)/shard_map/all_to_all | solution.py:100
  42.2 141.5 %all-gather.3.cloned.1.call-start = ((), (), s32[]{:S(2)}) async-start(), calls=%async_computation.5 | async-start | bytes 11796480 | tf_op jit(solution)/shard_map/all_gather | solution.py:120
  57.5 4.8 %copy-start.2 = (f32[2048]{0:T(1024)S(1)}, f32[2048]{0:T(1024)}, u32[]{:S(2)}) copy-start(f32[2048]{0:T(1024)} %param.18) | copy-start | bytes 24580
  86.2 230.1 %reduce-scatter.2.cloned.1.call-start = ((), (), s32[]{:S(2)}) async-start(), calls=%async_computation.4 | async-start | bytes 11796480 | tf_op jit(solution)/shard_map/reduce_scatter | solution.py:124
  183.7 8.7 %copy-start.4 = (bf16[1,2048,256]{2,1,0:T(8,128)(2,1)S(1)}, bf16[1,2048,256]{2,1,0:T(8,128)(2,1)}, u32[]{:S(2)}) copy-start(bf16[1,2048,256]{2,1,0:T(8,128)(2,1)} %param.22) | copy-start | bytes 3145732
  208.5 111.9 %copy-start.3 = (f32[128,2]{0,1:T(2,128)S(1)}, f32[128,2]{0,1:T(2,128)}, u32[]{:S(2)}) copy-start(f32[128,2]{0,1:T(2,128)} %param.20) | copy-start | bytes 3076
  316.4 18.4 %all-to-all-start.2 = ((bf16[4,80,2048]{2,1,0:T(8,128)(2,1)}), bf16[4,80,2048]{2,1,0:T(8,128)(2,1)S(1)}, u32[]{:S(2)}, u32[]{:S(2)}) async-start(bf16[4,80,2048]{2,1,0:T(8,128)(2,1)} %bitcast.75), calls=%async_computation.3 | async-start | bytes 2621440 | tf_op jit(solution)/shard_map/all_to_all | solution.py:131
Sparse Core Ops, SparseCore 0:
  86.4 97.2 all-gather.2
  208.7 107.6 reduce-scatter.1
where the time goes:
time: 354 us; the launch traced here: 353 us
  waiting for transfers between devices  232 us (66%)
  matrix products  36.5 us (10%)
  local copies, waits for them, and re-layouts  24.2 us (7%)
  blocking collectives  20.1 us (6%)
  starting transfers between devices  17.1 us (5%)
  between operations  13.7 us (4%)
  other arithmetic  9.63 us (3%)
    reduce_scatter x1, waiting for transfers between devices, local(): lax.psum_scatter(jnp.dot(hidden, down_local, preferred_element_type=jnp.f...  108 us
    all_gather x1, waiting for transfers between devices, local(): lax.all_gather(arrived[None], 'tp', axis=0, tiled=True)  97.2 us
    all_to_all x1, blocking collectives, local(): lax.all_to_all(outgoing, 'sp', split_axis=0, concat_axis=0, tiled=True)  20.1 us
    dot_general x1, matrix products, local(): jnp.dot(hidden, down_local, preferred_element_type=jnp.float32)  16.1 us
    all_to_all x1, waiting for transfers between devices, local(): lax.all_to_all(expert_out, 'sp', split_axis=0, concat_axis=0, tiled=True)  14.2 us
    all_to_all x1, waiting for transfers between devices, local(): lax.all_to_all(attended, 'tp', split_axis=0, concat_axis=1, tiled=True)  12.5 us
    dot_general x1, matrix products, expert_hidden(): jnp.dot(row_block, gate_local, preferred_element_type=jnp.float32)  8.73 us
    ppermute x2, starting transfers between devices, from_behind(): return lax.ppermute(block, axis, route)  8.26 us
  transfers between devices with their start and end apart: 6, of which 4 were waited for; matrix products, arithmetic and copies ran while one was open for 5% of the time, Pallas kernels for 0%

commit v1 on v0

v1 whole, which is shorter than its diff:
```python
import functools

import jax
import jax.numpy as jnp
from jax import lax
from jax.experimental import pallas as pl
from jax.experimental.pallas import tpu as pltpu
from jax.sharding import PartitionSpec as P


HEAD = 64
WINDOW = 128
LANES = 128
SLOT_TILE = 16


eps = 1e-06
clamp_limit = 7.0
sigmoid_alpha = 1.702

F32 = jnp.float32
BF16 = jnp.bfloat16


def exchange(block, axis, partner):
    devices = range(lax.axis_size(axis))
    return lax.ppermute(block, axis, [(i, partner(i)) for i in devices])


def from_behind(block, axis):
    devices = range(lax.axis_size(axis))
    return lax.ppermute(block, axis, [(i - 1, i) for i in devices if i > 0])


def attention_kernel(
    info_ref, sink_ref, q_ref, k_ref, kp_ref, v_ref, vp_ref, tail_ref, out_ref, *, kv_local, group_size
):
    block = pl.program_id(0)
    head_block = block == 0
    kv_cols = kv_local * HEAD
    tail = tail_ref[...]
    k_prev = jnp.where(head_block, tail[:, :kv_cols], kp_ref[...])
    v_prev = jnp.where(head_block, tail[:, kv_cols:], vp_ref[...])
    k_now = k_ref[...]
    v_now = v_ref[...]
    row = lax.broadcasted_iota(jnp.int32, (WINDOW, 2 * WINDOW), 0)
    col = lax.broadcasted_iota(jnp.int32, (WINDOW, 2 * WINDOW), 1)
    distance = row + WINDOW - col
    first_col = jnp.where(head_block & (info_ref[0] == 0), WINDOW, 0)
    allowed = (distance >= 0) & (distance < WINDOW) & (col >= first_col)
    queries = q_ref[...]
    pieces = []
    for kv in range(kv_local):
        part = slice(kv * HEAD, (kv + 1) * HEAD)
        keys = jnp.concatenate([k_prev[:, part], k_now[:, part]], axis=0)
        values = jnp.concatenate([v_prev[:, part], v_now[:, part]], axis=0)
        for g in range(group_size):
            head = kv * group_size + g
            scores = lax.dot_general(
                queries[:, head * HEAD : (head + 1) * HEAD],
                keys,
                (((1,), (1,)), ((), ())),
                preferred_element_type=F32,
            ) * HEAD ** (-0.5)
            logits = jnp.where(allowed, scores, -jnp.inf)
            sink = sink_ref[head]
            top = jnp.maximum(jnp.max(logits, axis=-1, keepdims=True), sink)
            raised = jnp.exp(logits - top)
            total = jnp.sum(raised, axis=-1, keepdims=True) + jnp.exp(sink - top)
            probs = (raised * (1.0 / total)).astype(BF16)
            pieces.append(jnp.dot(probs, values, preferred_element_type=F32).astype(BF16))
    out_ref[...] = jnp.concatenate(pieces, axis=-1).reshape(out_ref.shape)


def attend(query_heads, key_heads, value_heads, sink_logit, tail, tok_rows):
    span, q_cols = query_heads.shape
    kv_cols = key_heads.shape[1]
    kv_local = kv_cols // HEAD
    group_size = q_cols // kv_cols
    blocks = span // WINDOW
    smem = pl.BlockSpec(memory_space=pltpu.SMEM)
    info = lax.axis_index("sp").astype(jnp.int32).reshape(1)
    return pl.pallas_call(
        functools.partial(attention_kernel, kv_local=kv_local, group_size=group_size),
        grid=(blocks,),
        in_specs=[
            smem,
            smem,
            pl.BlockSpec((WINDOW, q_cols), lambda n: (n, 0)),
            pl.BlockSpec((WINDOW, kv_cols), lambda n: (n, 0)),
            pl.BlockSpec((WINDOW, kv_cols), lambda n: (jnp.maximum(n - 1, 0), 0)),
            pl.BlockSpec((WINDOW, kv_cols), lambda n: (n, 0)),
            pl.BlockSpec((WINDOW, kv_cols), lambda n: (jnp.maximum(n - 1, 0), 0)),
            pl.BlockSpec((WINDOW, 2 * kv_cols), lambda n: (0, 0)),
        ],
        out_specs=pl.BlockSpec((WINDOW // tok_rows, tok_rows, q_cols), lambda n: (n, 0, 0)),
        out_shape=jax.ShapeDtypeStruct((span // tok_rows, tok_rows, q_cols), BF16),
        name="attend",
    )(info, sink_logit, query_heads, key_heads, key_heads, value_heads, value_heads, tail)


def pack(meta, normed, send_refs, index, expert_count, slots):
    for distance, send_ref in enumerate(send_refs):
        hot, _ = placement(meta, index ^ distance, expert_count)
        send_ref[...] = lax.dot_general(
            hot[:, :slots], normed, (((0,), (0,)), ((), ())), preferred_element_type=F32
        ).astype(BF16)


def project_kernel(
    info_ref, att_ref, w_ref, res_ref, gain_ref, meta_ref, stream_ref, ext_ref, *refs, expert_count, slots, tile
):
    send_refs, acc_ref = refs[:-1], refs[-1]
    sources, _, cols = att_ref.shape
    width = stream_ref.shape[1]
    for n in range(width // tile):
        part = slice(n * tile, (n + 1) * tile)
        total = None
        for k in range(sources):
            piece = jnp.dot(
                att_ref[k], w_ref[k * cols : (k + 1) * cols, part], preferred_element_type=F32
            )
            total = piece if total is None else total + piece
        acc_ref[:, part] = total
    stream = (res_ref[...].astype(F32) + acc_ref[...]).astype(BF16)
    stream_ref[...] = stream
    wide = stream.astype(F32)
    scale = lax.rsqrt(jnp.mean(wide * wide, axis=-1, keepdims=True) + eps)
    normed = (wide * scale * gain_ref[...]).astype(BF16)
    ext_ref[:, :width] = normed
    ext_ref[:, width:] = meta_ref[...]
    pack(meta_ref[...], normed, send_refs, info_ref[0], expert_count, slots)


def project(index, gathered, out_weight, residual, norm_gain, meta, expert_count, slots):
    _, rows, _ = gathered.shape
    width = out_weight.shape[1]
    whole = pl.BlockSpec(memory_space=pltpu.VMEM)
    send = jax.ShapeDtypeStruct((slots, width), BF16)
    outs = pl.pallas_call(
        functools.partial(
            project_kernel, expert_count=expert_count, slots=slots, tile=min(512, width)
        ),
        in_specs=[pl.BlockSpec(memory_space=pltpu.SMEM)] + [whole] * 5,
        out_specs=[whole] * (2 + expert_count),
        out_shape=[
            jax.ShapeDtypeStruct((rows, width), BF16),
            jax.ShapeDtypeStruct((rows, width + LANES), BF16),
        ]
        + [send] * expert_count,
        scratch_shapes=[pltpu.VMEM((rows, width), F32)],
        name="project",
    )(index, gathered, out_weight, residual, norm_gain.reshape(1, width), meta)
    return outs[0], outs[1], outs[2:]


def pack_kernel(info_ref, ext_ref, *send_refs, expert_count, slots):
    width = ext_ref.shape[1] - LANES
    pack(ext_ref[:, width:], ext_ref[:, :width], send_refs, info_ref[0], expert_count, slots)


def pack_far(index, ext, expert_count, slots):
    whole = pl.BlockSpec(memory_space=pltpu.VMEM)
    send = jax.ShapeDtypeStruct((slots, ext.shape[1] - LANES), BF16)
    return pl.pallas_call(
        functools.partial(pack_kernel, expert_count=expert_count, slots=slots),
        in_specs=[pl.BlockSpec(memory_space=pltpu.SMEM), whole],
        out_specs=[whole] * expert_count,
        out_shape=[send] * expert_count,
        name="pack_far",
    )(index, ext)


def token_meta(own_routes, route_weight, expert_count):
    chosen = own_routes[:, :, None] == jnp.arange(expert_count, dtype=jnp.int32)
    weight = jnp.sum(jnp.where(chosen, route_weight[:, :, None], 0.0), axis=1)
    terms = [jnp.any(chosen, axis=1).astype(F32)]
    for _ in range(3):
        term = lax.reduce_precision(weight, 8, 7)
        terms.append(term)
        weight = weight - term
    packed = jnp.concatenate(terms, axis=1)
    return jnp.pad(packed, ((0, 0), (0, LANES - packed.shape[1]))).astype(BF16)


def placement(meta, expert, expert_count):
    rows = meta.shape[0]
    lane = lax.broadcasted_iota(jnp.int32, meta.shape, 1)
    wide = meta.astype(F32)
    chosen = jnp.sum(jnp.where(lane == expert, wide, 0.0), axis=1, keepdims=True)
    of_weight = (lane > expert_count - 1) & (lane < 4 * expert_count)
    of_weight &= lax.rem(lane, expert_count) == expert
    weight = jnp.sum(jnp.where(of_weight, wide, 0.0), axis=1, keepdims=True)
    earlier = lax.broadcasted_iota(jnp.int32, (rows, rows), 1) < lax.broadcasted_iota(
        jnp.int32, (rows, rows), 0
    )
    before = jnp.dot(
        earlier.astype(F32).astype(BF16),
        jnp.broadcast_to(chosen, (rows, LANES)).astype(BF16),
        preferred_element_type=F32,
    )
    slot = lax.broadcasted_iota(jnp.int32, (rows, LANES), 1)
    hot = (before.astype(jnp.int32) == slot) & (chosen > 0.5)
    return hot.astype(F32).astype(BF16), weight


def gate_up_kernel(*refs, groups, slots, pieces, hid):
    row_refs, refs = refs[:groups], refs[groups:]
    gates, tops, ends = refs[:pieces], refs[pieces : 2 * pieces], refs[2 * pieces : 3 * pieces]
    hidden_ref, picked_ref, weight_ref, sems = refs[3 * pieces :]
    cut = tops[0].shape[0]
    copies = []
    for p in range(pieces):
        targets = (
            weight_ref.at[p, 0],
            weight_ref.at[p, 1, pl.ds(0, cut)],
            weight_ref.at[p, 1, pl.ds(cut, ends[p].shape[0])],
        )
        copies.append(
            [
                pltpu.make_async_copy(source, target, sems.at[p, j])
                for j, (source, target) in enumerate(zip((gates[p], tops[p], ends[p]), targets))
            ]
        )
    for group in copies:
        for copy in group:
            copy.start()
    for b in range(groups):
        picked_ref[b * slots : (b + 1) * slots, :] = row_refs[b][...]
    picked = picked_ref[...]
    for p in range(pieces):
        for copy in copies[p]:
            copy.wait()
        gate_pre = jnp.dot(picked, weight_ref[p, 0], preferred_element_type=F32)
        upward = jnp.dot(picked, weight_ref[p, 1], preferred_element_type=F32)
        capped = jnp.minimum(gate_pre, clamp_limit)
        linear = jnp.clip(upward, -clamp_limit, clamp_limit)
        hidden = capped * jax.nn.sigmoid(sigmoid_alpha * capped) * (linear + 1.0)
        hidden_ref[:, p * hid : (p + 1) * hid] = hidden.astype(BF16)


def gate_up(rows, gates, tops, ends):
    groups, pieces = len(rows), len(gates)
    slots, width = rows[0].shape
    hid = gates[0].shape[1]
    whole = pl.BlockSpec(memory_space=pltpu.VMEM)
    anywhere = pl.BlockSpec(memory_space=pl.ANY)
    return pl.pallas_call(
        functools.partial(gate_up_kernel, groups=groups, slots=slots, pieces=pieces, hid=hid),
        in_specs=[whole] * groups + [anywhere] * (3 * pieces),
        out_specs=whole,
        out_shape=jax.ShapeDtypeStruct((groups * slots, pieces * hid), BF16),
        scratch_shapes=[
            pltpu.VMEM((groups * slots, width), BF16),
            pltpu.VMEM((pieces, 2, width, hid), BF16),
            pltpu.SemaphoreType.DMA((pieces, 3)),
        ],
    )(*rows, *gates, *tops, *ends)


def down_kernel(hidden_ref, *refs, groups, slots, pieces, hid, tile):
    downs = refs[:pieces]
    out_refs = refs[pieces:]
    width = out_refs[0].shape[1]
    for n in range(width // tile):
        cols = slice(n * tile, (n + 1) * tile)
        total = None
        for p in range(pieces):
            part = jnp.dot(
                hidden_ref[:, p * hid : (p + 1) * hid],
                downs[p][:, cols],
                preferred_element_type=F32,
            )
            total = part if total is None else total + part
        expert_out = total.astype(BF16)
        for b in range(groups):
            out_refs[b][:, cols] = expert_out[b * slots : (b + 1) * slots, :]


def down(hidden, downs, groups):
    hid, width = downs[0].shape
    pieces = len(downs)
    slots = hidden.shape[0] // groups
    whole = pl.BlockSpec(memory_space=pltpu.VMEM)
    body = functools.partial(
        down_kernel, groups=groups, slots=slots, pieces=pieces, hid=hid, tile=min(512, width)
    )
    return pl.pallas_call(
        body,
        in_specs=[whole] * (1 + pieces),
        out_specs=[whole] * groups,
        out_shape=[jax.ShapeDtypeStruct((slots, width), BF16)] * groups,
    )(hidden, *downs)


def unpack(meta, back_refs, index, expert_count, slots):
    total = None
    for distance, back_ref in enumerate(back_refs):
        hot, weight = placement(meta, index ^ distance, expert_count)
        spread = jnp.dot(hot[:, :slots], back_ref[...], preferred_element_type=F32) * weight
        total = spread if total is None else total + spread
    return total


def combine_far_kernel(info_ref, meta_ref, *refs, expert_count, slots):
    refs[-1][...] = unpack(meta_ref[...], refs[:-1], info_ref[0], expert_count, slots).astype(BF16)


def combine_own_kernel(info_ref, meta_ref, stream_ref, far_ref, *refs, expert_count, slots):
    total = unpack(meta_ref[...], refs[:-1], info_ref[0], expert_count, slots)
    total += stream_ref[...].astype(F32) + far_ref[...].astype(F32)
    refs[-1][...] = total.astype(BF16)


def combine(kernel, index, ext, extra, backs):
    slots, width = backs[0].shape
    rows = ext.shape[0]
    meta_at = width // LANES
    whole = pl.BlockSpec(memory_space=pltpu.VMEM)
    return pl.pallas_call(
        functools.partial(kernel, expert_count=len(backs), slots=slots),
        grid=(1,),
        in_specs=[
            pl.BlockSpec(memory_space=pltpu.SMEM),
            pl.BlockSpec((rows, LANES), lambda i: (0, meta_at)),
        ]
        + [whole] * (len(extra) + len(backs)),
        out_specs=whole,
        out_shape=jax.ShapeDtypeStruct((rows, width), BF16),
    )(index, ext, *extra, *backs)


def layer(
    query_heads,
    key_heads,
    value_heads,
    sink_logit,
    residual,
    out_weight,
    norm_gain,
    routes,
    route_weight,
    gate_weight,
    up_weight,
    down_weight,
):
    expert_count = lax.axis_size("sp")
    half = lax.axis_size("tp") // 2
    tok_rows = residual.shape[0]
    choose_count = routes.shape[1]
    tp_index = lax.axis_index("tp")
    index = lax.axis_index("sp").astype(jnp.int32).reshape(1)

    def across(block):
        return exchange(block, "tp", lambda i: (i + half) % (2 * half))

    def to_experts(blocks):
        return [blocks[0]] + [exchange(blocks[d], "sp", lambda i, d=d: i ^ d) for d in range(1, expert_count)]

    tail = jnp.concatenate([key_heads[-WINDOW:], value_heads[-WINDOW:]], axis=1)
    tail = from_behind(tail, "sp")
    gates, downs = [gate_weight[0]], [down_weight[0]]
    tops, ends = jnp.split(up_weight[0], 2, axis=0)
    tops, ends = [tops], [ends]
    for distance in range(1, half):
        if distance % 2:
            step, source = 1, distance - 1
        else:
            step, source = distance, 0
        for held in (gates, tops, ends, downs):
            held.append(exchange(held[source], "tp", lambda i, s=step: i ^ s))

    attended = attend(query_heads, key_heads, value_heads, sink_logit, tail, tok_rows)
    gathered = lax.all_to_all(attended, "tp", split_axis=0, concat_axis=0, tiled=True)
    own_routes = lax.dynamic_slice_in_dim(routes, tp_index * tok_rows, tok_rows, 0)
    meta = token_meta(own_routes, route_weight, expert_count)

    capacity = max(2, 5 * tok_rows * choose_count // (4 * expert_count))
    slots = -(-capacity // SLOT_TILE) * SLOT_TILE
    stream, ext, send_own = project(index, gathered, out_weight, residual, norm_gain, meta, expert_count, slots)
    ext_far = across(ext)
    rows_own = to_experts(send_own)
    hidden_own = gate_up(rows_own, gates, tops, ends)
    rows_far = to_experts(pack_far(index, ext_far, expert_count, slots))
    hidden_far = gate_up(rows_far, gates, tops, ends)
    backs_far = to_experts(down(hidden_far, downs, expert_count))
    backs_own = to_experts(down(hidden_own, downs, expert_count))
    part_far = across(combine(combine_far_kernel, index, ext_far, (), backs_far))
    return combine(combine_own_kernel, index, ext, (stream, part_far), backs_own)


def solution(mesh):
    placed = (
        P("sp", "tp"),
        P("sp", "tp"),
        P("sp", "tp"),
        P("tp"),
        P(("sp", "tp"), None),
        P(),
        P(),
        P("sp", None),
        P(("sp", "tp"), None),
        P("sp", None, "tp"),
        P("sp", None, "tp"),
        P("sp", "tp", None),
    )
    return jax.shard_map(layer, mesh=mesh, in_specs=placed, out_specs=P(("sp", "tp"), None), check_vma=False)
```

time: 354 us -> 217 us (0.61)
  waiting for transfers between devices: 232 us -> 117 us
  Pallas kernels: 0 us -> 51.5 us
  matrix products: 36.5 us -> 0 us
  starting transfers between devices: 17.1 us -> 38.8 us
  blocking collectives: 20.1 us -> 0 us
  local copies, waits for them, and re-layouts: 24.2 us -> 7.56 us
  between operations: 13.7 us -> 0.18 us
  other arithmetic: 9.63 us -> 0.74 us
    ppermute x2 -> x27, waiting for transfers between devices: 0.01 us -> 117 us  [the longest x26 115 us: exchange(): return lax.ppermute(block, axis, [(i, partner(i)) for i in devices])]
    reduce_scatter x1 -> x0, waiting for transfers between devices: 108 us -> none  [local(): lax.psum_scatter(jnp.dot(hidden, down_local, preferred_element_type=jnp.f...]
    all_gather x1 -> x0, waiting for transfers between devices: 97.2 us -> none  [local(): lax.all_gather(arrived[None], 'tp', axis=0, tiled=True)]
    pallas_call x0 -> x9, Pallas kernels: none -> 51.5 us  [the longest x2 14.4 us: gate_up(): pl.pallas_call(functools.partial(gate_up_kernel, groups=groups, slots=slo...]
    dot_general x6 -> x0, matrix products: 36.5 us -> none  [the longest x1 16.1 us: local(): jnp.dot(hidden, down_local, preferred_element_type=jnp.float32)]
    all_to_all x2 -> x1, waiting for transfers between devices: 26.8 us -> 0.01 us  [layer(): lax.all_to_all(attended, 'tp', split_axis=0, concat_axis=0, tiled=True)]
    ppermute x2 -> x27, starting transfers between devices: 8.26 us -> 33.9 us  [the longest x26 29 us: exchange(): return lax.ppermute(block, axis, [(i, partner(i)) for i in devices])]
    all_to_all x1 -> x0, blocking collectives: 20.1 us -> none  [local(): lax.all_to_all(outgoing, 'sp', split_axis=0, concat_axis=0, tiled=True)]
  transfers between devices with their start and end apart: 6 -> 28, of which waited for: 4 -> 14; matrix products, arithmetic and copies ran while one was open for 5% -> 1% of each run, Pallas kernels for 0% -> 15%
where the time goes in v1:
time: 217 us; the launch traced here: 216 us
  waiting for transfers between devices  117 us (54%)
  Pallas kernels  51.5 us (24%)
  starting transfers between devices  38.8 us (18%)
  local copies, waits for them, and re-layouts  7.56 us (3%)
    ppermute x26, waiting for transfers between devices, exchange(): return lax.ppermute(block, axis, [(i, partner(i)) for i in devices])  115 us
    ppermute x26, starting transfers between devices, exchange(): return lax.ppermute(block, axis, [(i, partner(i)) for i in devices])  29 us
    pallas_call x2, Pallas kernels, gate_up(): pl.pallas_call(functools.partial(gate_up_kernel, groups=groups, slots=slo...  14.4 us
    pallas_call x1, Pallas kernels, attend(): pl.pallas_call(functools.partial(attention_kernel, kv_local=kv_local, gro...  9.93 us
    pallas_call x2, Pallas kernels, down(): pl.pallas_call(body, in_specs=[whole] * (1 + pieces), out_specs=[whole] *...  9.81 us
    pallas_call x2, Pallas kernels, combine(): pl.pallas_call(functools.partial(kernel, expert_count=len(backs), slots=s...  7.16 us
    pallas_call x1, Pallas kernels, project(): pl.pallas_call(functools.partial(project_kernel, expert_count=expert_coun...  7.07 us
    ppermute x1, starting transfers between devices, from_behind(): return lax.ppermute(block, axis, [(i - 1, i) for i in devices if i > 0])  4.88 us
  transfers between devices with their start and end apart: 28, of which 14 were waited for; matrix products, arithmetic and copies ran while one was open for 1% of the time, Pallas kernels for 15%

profile of v1, /device:TPU:0, one launch (start us, length us, event | category | flops | bytes accessed | tf_op | source)
XLA Modules:
  0.0 215.7 jit_solution(4626519666439828539)
XLA Ops:
  0.0 0.9 slice.8
  0.9 0.8 slice.9
  1.7 4.9 %collective-permute-start = (bf16[128,256]{1,0:T(8,128)(2,1)S(1)}, bf16[128,256]{1,0:T(8,128)(2,1)S(1)}, u32[]{:S(2)}, u32[]{:S(2)}) collective-permute-start(bf16[128,256]{1,0:T(8,128)(2,1)S(1)} %pad_maximum_fusion), channel_id=1, source_target_pairs={{0,8},{8,16},{16,24},{1,9},{9,17},{17,25},{2,10},{10,18},{18,26},{... | collective-permute-start | bytes 196616 | tf_op jit(solution)/shard_map/ppermute | solution.py:32
  6.6 1.9 collective-permute-done.tail_ref
  9.1 9.9 %attend.1 = bf16[8,128,256]{2,1,0:T(8,128)(2,1)} custom-call(s32[1]{0:T(128)} %bitcast.info_ref, f32[4]{0:T(128)} %sink_ref.1, bf16[1024,256]{1,0:T(8,128)(2,1)} %q_ref.1, bf16[1024,128]{1,0:T(8,128)(2,1)} %kp_ref.1, bf16[1024,128]{1,0:T(8,128)(2,1)} %kp_ref.1, bf16[1024,128]{1,0:T(8,128)(2,1)} %vp_ref.1, bf16[1024,128]{1,0:T(8,128)(2,1)} %vp_ref.1, ...), custom_call_target="tpu_custom_call" | custom-call | tf_op jit(solution)/shard_map/attend/pallas_call | solution.py:83
  19.0 4.9 %all-to-all-start = ((bf16[8,128,256]{2,1,0:T(8,128)(2,1)}), bf16[8,128,256]{2,1,0:T(8,128)(2,1)}, u32[]{:S(2)}, u32[]{:S(2)}) async-start(bf16[8,128,256]{2,1,0:T(8,128)(2,1)} %attend.1), calls=%async_computation | async-start | bytes 1048576 | tf_op jit(solution)/shard_map/all_to_all | solution.py:374
  23.9 1.3 slice_bitcast_fusion
  25.2 2.1 collective-permute-start.12
  27.5 1.8 collective-permute-start.6
  29.5 0.7 select_reduce_fusion
  30.3 17.2 %collective-permute-done.12.refs_14_ = bf16[1024,256]{1,0:T(8,128)(2,1)} collective-permute-done((bf16[1024,256]{1,0:T(8,128)(2,1)S(1)}, bf16[1024,256]{1,0:T(8,128)(2,1)}, u32[]{:S(2)}, u32[]{:S(2)}) %collective-permute-start.12) | collective-permute-done | bytes 524320 | tf_op jit(solution)/shard_map/ppermute | solution.py:27
  48.7 7.1 %project.1 = (bf16[128,2048]{1,0:T(8,128)(2,1)}, bf16[128,2176]{1,0:T(8,128)(2,1)}, bf16[80,2048]{1,0:T(8,128)(2,1)}, bf16[80,2048]{1,0:T(8,128)(2,1)}, bf16[80,...) custom-call(s32[1]{0:T(128)} %bitcast.info_ref, bf16[8,128,256]{2,1,0:T(8,128)(2,1)} %all-to-all-done.att_ref, ...), custom_call_target="tpu_custom_call" | custom-call | tf_op jit(solution)/shard_map/project/pallas_call | solution.py:140
  55.8 2.9 %collective-permute-done.9.refs_10_ = bf16[1024,256]{1,0:T(8,128)(2,1)} collective-permute-done((bf16[1024,256]{1,0:T(8,128)(2,1)S(1)}, bf16[1024,256]{1,0:T(8,128)(2,1)}, u32[]{:S(2)}, u32[]{:S(2)}) %collective-permute-start.9) | collective-permute-done | bytes 524320 | tf_op jit(solution)/shard_map/ppermute | solution.py:27
  58.7 2.5 %collective-permute-start.1 = (bf16[128,2176]{1,0:T(8,128)(2,1)}, bf16[128,2176]{1,0:T(8,128)(2,1)}, u32[]{:S(2)}, u32[]{:S(2)}) collective-permute-start(bf16[128,2176]{1,0:T(8,128)(2,1)} %get-tuple-element.23.meta_ref), channel_id=1, source_target_pairs={{0,4},{1,5},{2,6},{3,7},{4,0},{5,1},{6,2},{7,3},{8,12},{9,13},{10,... | collective-permute-start | bytes 1671176 | tf_op jit(solution)/shard_map/ppermute | solution.py:27
  61.7 31.4 %collective-permute-done.6.refs_6_ = bf16[2048,256]{1,0:T(8,128)(2,1)} collective-permute-done((bf16[2048,256]{1,0:T(8,128)(2,1)}, bf16[2048,256]{1,0:T(8,128)(2,1)}, u32[]{:S(2)}, u32[]{:S(2)}) %collective-permute-start.6) | collective-permute-done | bytes 1048608 | tf_op jit(solution)/shard_map/ppermute | solution.py:27
  93.1 21.9 %collective-permute-done.15.refs_2_ = bf16[256,2048]{1,0:T(8,128)(2,1)} collective-permute-done((bf16[256,2048]{1,0:T(8,128)(2,1)}, bf16[256,2048]{1,0:T(8,128)(2,1)}, u32[]{:S(2)}, u32[]{:S(2)}) %collective-permute-start.15) | collective-permute-done | bytes 1048608 | tf_op jit(solution)/shard_map/ppermute | solution.py:27
  115.5 3.1 %pack_far.1 = (bf16[80,2048]{1,0:T(8,128)(2,1)}, bf16[80,2048]{1,0:T(8,128)(2,1)}, bf16[80,2048]{1,0:T(8,128)(2,1)}, bf16[80,2048]{1,0:T(8,128)(2,1)}) custom-call(s32[1]{0:T(128)} %bitcast.info_ref, bf16[128,2176]{1,0:T(8,128)(2,1)} %collective-permute-done.1.ext_ref.meta_ref), custom_call_target="tpu_custom_call" | custom-call | tf_op jit(solution)/shard_map/pack_far/pallas_call | solution.py:165
  118.7 2.4 %collective-permute-start.2 = (bf16[80,2048]{1,0:T(8,128)(2,1)}, bf16[80,2048]{1,0:T(8,128)(2,1)S(1)}, u32[]{:S(2)}, u32[]{:S(2)}) collective-permute-start(bf16[80,2048]{1,0:T(8,128)(2,1)} %get-tuple-element.26), channel_id=1, source_target_pairs={{0,8},{8,0},{16,24},{24,16},{1,9},{9,1},{17,25},{25,17},{2,10},{10... | collective-permute-start | bytes 983048 | tf_op jit(solution)/shard_map/ppermute | solution.py:27
  121.0 1.5 collective-permute-start.3
  122.5 6.6 %collective-permute-done.2.refs_1_ = bf16[80,2048]{1,0:T(8,128)(2,1)S(1)} collective-permute-done((bf16[80,2048]{1,0:T(8,128)(2,1)}, bf16[80,2048]{1,0:T(8,128)(2,1)S(1)}, u32[]{:S(2)}, u32[]{:S(2)}) %collective-permute-start.2) | collective-permute-done | bytes 327712 | tf_op jit(solution)/shard_map/ppermute | solution.py:27
  129.2 2.7 %collective-permute-start.4 = (bf16[80,2048]{1,0:T(8,128)(2,1)}, bf16[80,2048]{1,0:T(8,128)(2,1)S(1)}, u32[]{:S(2)}, u32[]{:S(2)}) collective-permute-start(bf16[80,2048]{1,0:T(8,128)(2,1)} %get-tuple-element.28), channel_id=1, source_target_pairs={{0,24},{8,16},{16,8},{24,0},{1,25},{9,17},{17,9},{25,1},{2,26},{10... | collective-permute-start | bytes 983048 | tf_op jit(solution)/shard_map/ppermute | solution.py:27
  131.9 7.5 %collective-permute-done.4.refs_3_ = bf16[80,2048]{1,0:T(8,128)(2,1)S(1)} collective-permute-done((bf16[80,2048]{1,0:T(8,128)(2,1)}, bf16[80,2048]{1,0:T(8,128)(2,1)S(1)}, u32[]{:S(2)}, u32[]{:S(2)}) %collective-permute-start.4) | collective-permute-done | bytes 327712 | tf_op jit(solution)/shard_map/ppermute | solution.py:27
  139.4 0.7 copy-done.11
  140.1 7.2 %shard_map.118.hidden_ref = bf16[320,1024]{1,0:T(8,128)(2,1)} custom-call(bf16[80,2048]{1,0:T(8,128)(2,1)} %get-tuple-element.25.refs_0_, bf16[80,2048]{1,0:T(8,128)(2,1)} %copy-done.9, bf16[80,2048]{1,0:T(8,128)(2,1)} %copy-done.10, bf16[80,2048]{1,0:T(8,128)(2,1)} %copy-done.11, bf16[2048,256]{1,0:T(8,128)(2,1)} %bitcast.9, ...), custom_call_target="tpu_custom_call" | custom-call | tf_op jit(solution)/shard_map/pallas_call | solution.py:248
  147.3 4.9 %shard_map.119 = (bf16[80,2048]{1,0:T(8,128)(2,1)}, bf16[80,2048]{1,0:T(8,128)(2,1)}, bf16[80,2048]{1,0:T(8,128)(2,1)}, bf16[80,2048]{1,0:T(8,128)(2,1)}) custom-call(bf16[320,1024]{1,0:T(8,128)(2,1)} %shard_map.118.hidden_ref, bf16[256,2048]{1,0:T(8,128)(2,1)} %bitcast.13, bf16[256,2048]{1,0:T(8,128)(2,1)} %collective-permute-done.14.refs_1_, ...), custom_call_target="tpu_custom_call" | custom-call | tf_op jit(solution)/shard_map/pallas_call | solution.py:288
  152.2 1.5 collective-permute-start.17
  153.7 1.5 collective-permute-start.18
  155.2 0.9 collective-permute-start.19
  156.1 1.1 collective-permute-start.21
  157.2 1.5 collective-permute-start.22
  158.7 4.3 %collective-permute-done.17.refs_1_ = bf16[80,2048]{1,0:T(8,128)(2,1)S(1)} collective-permute-done((bf16[80,2048]{1,0:T(8,128)(2,1)}, bf16[80,2048]{1,0:T(8,128)(2,1)S(1)}, u32[]{:S(2)}, u32[]{:S(2)}) %collective-permute-start.17) | collective-permute-done | bytes 327712 | tf_op jit(solution)/shard_map/ppermute | solution.py:27
  163.0 2.4 %collective-permute-start.23 = (bf16[80,2048]{1,0:T(8,128)(2,1)}, bf16[80,2048]{1,0:T(8,128)(2,1)S(1)}, u32[]{:S(2)}, u32[]{:S(2)}) collective-permute-start(bf16[80,2048]{1,0:T(8,128)(2,1)} %get-tuple-element.36), channel_id=1, source_target_pairs={{0,24},{8,16},{16,8},{24,0},{1,25},{9,17},{17,9},{25,1},{2,26},{10... | collective-permute-start | bytes 983048 | tf_op jit(solution)/shard_map/ppermute | solution.py:27
  165.4 5.6 %collective-permute-done.18.refs_2_ = bf16[80,2048]{1,0:T(8,128)(2,1)S(1)} collective-permute-done((bf16[80,2048]{1,0:T(8,128)(2,1)}, bf16[80,2048]{1,0:T(8,128)(2,1)S(1)}, u32[]{:S(2)}, u32[]{:S(2)}) %collective-permute-start.18) | collective-permute-done | bytes 327712 | tf_op jit(solution)/shard_map/ppermute | solution.py:27
  171.1 0.8 collective-permute-done.19.refs_3_
  171.9 0.7 copy-done.15
  172.6 3.4 %shard_map.120 = bf16[128,2048]{1,0:T(8,128)(2,1)} custom-call(s32[1]{0:T(128)} %bitcast.info_ref, bf16[128,2176]{1,0:T(8,128)(2,1)} %collective-permute-done.1.ext_ref.meta_ref, bf16[80,2048]{1,0:T(8,128)(2,1)} %get-tuple-element.29.refs_0_, bf16[80,2048]{1,0:T(8,128)(2,1)} %copy-done.12, bf16[80,2048]{1,0:T(8,128)(2,1)} %copy-done.13, ...), custom_call_target="tpu_custom_call" | custom-call | tf_op jit(solution)/shard_map/pallas_call | solution.py:320
  176.0 1.7 collective-permute-start.20
  177.7 4.1 %collective-permute-done.22.refs_2_ = bf16[80,2048]{1,0:T(8,128)(2,1)S(1)} collective-permute-done((bf16[80,2048]{1,0:T(8,128)(2,1)}, bf16[80,2048]{1,0:T(8,128)(2,1)S(1)}, u32[]{:S(2)}, u32[]{:S(2)}) %collective-permute-start.22) | collective-permute-done | bytes 327712 | tf_op jit(solution)/shard_map/ppermute | solution.py:27
  181.8 1.5 collective-permute-done.23.refs_3_
  183.3 0.7 copy-done.8
  184.0 7.2 %shard_map.121.hidden_ref = bf16[320,1024]{1,0:T(8,128)(2,1)} custom-call(bf16[80,2048]{1,0:T(8,128)(2,1)} %get-tuple-element.33.refs_0_, bf16[80,2048]{1,0:T(8,128)(2,1)} %copy-done.6, bf16[80,2048]{1,0:T(8,128)(2,1)} %copy-done.7, bf16[80,2048]{1,0:T(8,128)(2,1)} %copy-done.8, bf16[2048,256]{1,0:T(8,128)(2,1)} %bitcast.10, ...), custom_call_target="tpu_custom_call" | custom-call | tf_op jit(solution)/shard_map/pallas_call | solution.py:248
  191.3 4.9 %shard_map.122 = (bf16[80,2048]{1,0:T(8,128)(2,1)}, bf16[80,2048]{1,0:T(8,128)(2,1)}, bf16[80,2048]{1,0:T(8,128)(2,1)}, bf16[80,2048]{1,0:T(8,128)(2,1)}) custom-call(bf16[320,1024]{1,0:T(8,128)(2,1)} %shard_map.121.hidden_ref, bf16[256,2048]{1,0:T(8,128)(2,1)} %bitcast.14, bf16[256,2048]{1,0:T(8,128)(2,1)} %collective-permute-done.14.refs_1_, ...), custom_call_target="tpu_custom_call" | custom-call | tf_op jit(solution)/shard_map/pallas_call | solution.py:288
  196.8 1.8 collective-permute-start.25
  198.6 1.1 collective-permute-start.26
  199.7 7.3 %collective-permute-done.24.refs_1_ = bf16[80,2048]{1,0:T(8,128)(2,1)S(1)} collective-permute-done((bf16[80,2048]{1,0:T(8,128)(2,1)}, bf16[80,2048]{1,0:T(8,128)(2,1)S(1)}, u32[]{:S(2)}, u32[]{:S(2)}) %collective-permute-start.24) | collective-permute-done | bytes 327712 | tf_op jit(solution)/shard_map/ppermute | solution.py:27
  207.0 3.9 %collective-permute-done.25.refs_2_ = bf16[80,2048]{1,0:T(8,128)(2,1)S(1)} collective-permute-done((bf16[80,2048]{1,0:T(8,128)(2,1)}, bf16[80,2048]{1,0:T(8,128)(2,1)S(1)}, u32[]{:S(2)}, u32[]{:S(2)}) %collective-permute-start.25) | collective-permute-done | bytes 327712 | tf_op jit(solution)/shard_map/ppermute | solution.py:27
  210.9 0.7 copy-done.16
  211.9 3.8 %shard_map.123 = bf16[128,2048]{1,0:T(8,128)(2,1)} custom-call(s32[1]{0:T(128)} %bitcast.info_ref, bf16[128,2176]{1,0:T(8,128)(2,1)} %get-tuple-element.23.meta_ref, bf16[128,2048]{1,0:T(8,128)(2,1)} %get-tuple-element.24.stream_ref, bf16[128,2048]{1,0:T(8,128)(2,1)} %copy-done.5, bf16[80,2048]{1,0:T(8,128)(2,1)} %get-tuple-element.37.refs_0_, ...), custom_call_target="tpu_custom_call" | custom-call | tf_op jit(solution)/shard_map/pallas_call | solution.py:320
  (67 shorter events, 4.5 us)
Async XLA Ops:
  0.0 29.5 %copy-start = (s32[1024,2]{0,1:T(2,128)S(1)}, s32[1024,2]{0,1:T(2,128)}, u32[]{:S(2)}) copy-start(s32[1024,2]{0,1:T(2,128)} %param.19) | copy-start | bytes 24580
  0.0 61.2 %copy-start.3 = (bf16[1,2048,256]{2,1,0:T(8,128)(2,1)S(1)}, bf16[1,2048,256]{2,1,0:T(8,128)(2,1)}, u32[]{:S(2)}) copy-start(bf16[1,2048,256]{2,1,0:T(8,128)(2,1)} %param.21) | copy-start | bytes 3145732
  0.0 115.0 %copy-start.4 = (bf16[1,256,2048]{2,1,0:T(8,128)(2,1)S(1)}, bf16[1,256,2048]{2,1,0:T(8,128)(2,1)}, u32[]{:S(2)}) copy-start(bf16[1,256,2048]{2,1,0:T(8,128)(2,1)} %param.23) | copy-start | bytes 3145732
  1.7 6.8 %collective-permute-start = (bf16[128,256]{1,0:T(8,128)(2,1)S(1)}, bf16[128,256]{1,0:T(8,128)(2,1)S(1)}, u32[]{:S(2)}, u32[]{:S(2)}) collective-permute-start(bf16[128,256]{1,0:T(8,128)(2,1)S(1)} %pad_maximum_fusion), channel_id=1, source_target_pairs={{0,8},{8,16},{16,24},{1,9},{9,17},{17,25},{2,10},{10,18},{18,26},{... | collective-permute-start | bytes 196616 | tf_op jit(solution)/shard_map/ppermute | solution.py:32
  8.5 0.6 copy-start.18
  19.0 29.7 %all-to-all-start = ((bf16[8,128,256]{2,1,0:T(8,128)(2,1)}), bf16[8,128,256]{2,1,0:T(8,128)(2,1)}, u32[]{:S(2)}, u32[]{:S(2)}) async-start(bf16[8,128,256]{2,1,0:T(8,128)(2,1)} %attend.1), calls=%async_computation | async-start | bytes 1048576 | tf_op jit(solution)/shard_map/all_to_all | solution.py:374
  25.2 114.2 %copy-start.1 = (bf16[1024,256]{1,0:T(8,128)(2,1)}, bf16[1024,256]{1,0:T(8,128)(2,1)S(1)}, u32[]{:S(2)}) copy-start(bf16[1024,256]{1,0:T(8,128)(2,1)S(1)} %get-tuple-element.41.refs_12_) | copy-start | bytes 1572868
  25.2 114.2 %copy-start.2 = (bf16[1024,256]{1,0:T(8,128)(2,1)}, bf16[1024,256]{1,0:T(8,128)(2,1)S(1)}, u32[]{:S(2)}) copy-start(bf16[1024,256]{1,0:T(8,128)(2,1)S(1)} %get-tuple-element.42.refs_8_) | copy-start | bytes 1572868
  25.2 22.2 %collective-permute-start.12 = (bf16[1024,256]{1,0:T(8,128)(2,1)S(1)}, bf16[1024,256]{1,0:T(8,128)(2,1)}, u32[]{:S(2)}, u32[]{:S(2)}) collective-permute-start(bf16[1024,256]{1,0:T(8,128)(2,1)S(1)} %get-tuple-element.41.refs_12_), channel_id=1, source_target_pairs={{0,2},{1,3},{2,0},{3,1},{4,6},{5,7},{6,4},{7,5},{8,10},{9,11},{10,... | collective-permute-start | bytes 1572872 | tf_op jit(solution)/shard_map/ppermute | solution.py:27
  27.3 20.2 %collective-permute-start.11 = (bf16[1024,256]{1,0:T(8,128)(2,1)S(1)}, bf16[1024,256]{1,0:T(8,128)(2,1)}, u32[]{:S(2)}, u32[]{:S(2)}) collective-permute-start(bf16[1024,256]{1,0:T(8,128)(2,1)S(1)} %get-tuple-element.41.refs_12_), channel_id=1, source_target_pairs={{0,1},{1,0},{2,3},{3,2},{4,5},{5,4},{6,7},{7,6},{8,9},{9,8},{10,11... | collective-permute-start | bytes 1572872 | tf_op jit(solution)/shard_map/ppermute | solution.py:27
  27.3 31.4 %collective-permute-start.9 = (bf16[1024,256]{1,0:T(8,128)(2,1)S(1)}, bf16[1024,256]{1,0:T(8,128)(2,1)}, u32[]{:S(2)}, u32[]{:S(2)}) collective-permute-start(bf16[1024,256]{1,0:T(8,128)(2,1)S(1)} %get-tuple-element.42.refs_8_), channel_id=1, source_target_pairs={{0,2},{1,3},{2,0},{3,1},{4,6},{5,7},{6,4},{7,5},{8,10},{9,11},{10,... | collective-permute-start | bytes 1572872 | tf_op jit(solution)/shard_map/ppermute | solution.py:27
  27.5 65.6 %collective-permute-start.6 = (bf16[2048,256]{1,0:T(8,128)(2,1)}, bf16[2048,256]{1,0:T(8,128)(2,1)}, u32[]{:S(2)}, u32[]{:S(2)}) collective-permute-start(bf16[2048,256]{1,0:T(8,128)(2,1)} %bitcast.8), channel_id=1, source_target_pairs={{0,2},{1,3},{2,0},{3,1},{4,6},{5,7},{6,4},{7,5},{8,10},{9,11},{10,... | collective-permute-start | bytes 3145736 | tf_op jit(solution)/shard_map/ppermute | solution.py:27
  29.3 85.7 %collective-permute-start.15 = (bf16[256,2048]{1,0:T(8,128)(2,1)}, bf16[256,2048]{1,0:T(8,128)(2,1)}, u32[]{:S(2)}, u32[]{:S(2)}) collective-permute-start(bf16[256,2048]{1,0:T(8,128)(2,1)} %bitcast.12), channel_id=1, source_target_pairs={{0,2},{1,3},{2,0},{3,1},{4,6},{5,7},{6,4},{7,5},{8,10},{9,11},{10,... | collective-permute-start | bytes 3145736 | tf_op jit(solution)/shard_map/ppermute | solution.py:27
  47.4 13.7 %collective-permute-start.8 = (bf16[1024,256]{1,0:T(8,128)(2,1)S(1)}, bf16[1024,256]{1,0:T(8,128)(2,1)}, u32[]{:S(2)}, u32[]{:S(2)}) collective-permute-start(bf16[1024,256]{1,0:T(8,128)(2,1)S(1)} %get-tuple-element.42.refs_8_), channel_id=1, source_target_pairs={{0,1},{1,0},{2,3},{3,2},{4,5},{5,4},{6,7},{7,6},{8,9},{9,8},{10,11... | collective-permute-start | bytes 1572872 | tf_op jit(solution)/shard_map/ppermute | solution.py:27
  47.5 13.7 %collective-permute-start.13 = (bf16[1024,256]{1,0:T(8,128)(2,1)}, bf16[1024,256]{1,0:T(8,128)(2,1)}, u32[]{:S(2)}, u32[]{:S(2)}) collective-permute-start(bf16[1024,256]{1,0:T(8,128)(2,1)} %collective-permute-done.12.refs_14_), channel_id=1, source_target_pairs={{0,1},{1,0},{2,3},{3,2},{4,5},{5,4},{6,7},{7,6},{8,9},{9,8},{10,11... | collective-permute-start | bytes 1572872 | tf_op jit(solution)/shard_map/ppermute | solution.py:27
  58.7 56.3 %collective-permute-start.1 = (bf16[128,2176]{1,0:T(8,128)(2,1)}, bf16[128,2176]{1,0:T(8,128)(2,1)}, u32[]{:S(2)}, u32[]{:S(2)}) collective-permute-start(bf16[128,2176]{1,0:T(8,128)(2,1)} %get-tuple-element.23.meta_ref), channel_id=1, source_target_pairs={{0,4},{1,5},{2,6},{3,7},{4,0},{5,1},{6,2},{7,3},{8,12},{9,13},{10,... | collective-permute-start | bytes 1671176 | tf_op jit(solution)/shard_map/ppermute | solution.py:27
  61.2 59.8 %collective-permute-start.5 = (bf16[2048,256]{1,0:T(8,128)(2,1)S(1)}, bf16[2048,256]{1,0:T(8,128)(2,1)}, u32[]{:S(2)}, u32[]{:S(2)}) collective-permute-start(bf16[2048,256]{1,0:T(8,128)(2,1)S(1)} %bitcast.11), channel_id=1, source_target_pairs={{0,1},{1,0},{2,3},{3,2},{4,5},{5,4},{6,7},{7,6},{8,9},{9,8},{10,11... | collective-permute-start | bytes 3145736 | tf_op jit(solution)/shard_map/ppermute | solution.py:27
  61.2 57.5 %collective-permute-start.10 = (bf16[1024,256]{1,0:T(8,128)(2,1)}, bf16[1024,256]{1,0:T(8,128)(2,1)}, u32[]{:S(2)}, u32[]{:S(2)}) collective-permute-start(bf16[1024,256]{1,0:T(8,128)(2,1)} %collective-permute-done.9.refs_10_), channel_id=1, source_target_pairs={{0,1},{1,0},{2,3},{3,2},{4,5},{5,4},{6,7},{7,6},{8,9},{9,8},{10,11... | collective-permute-start | bytes 1572872 | tf_op jit(solution)/shard_map/ppermute | solution.py:27
  93.1 46.3 %collective-permute-start.7 = (bf16[2048,256]{1,0:T(8,128)(2,1)}, bf16[2048,256]{1,0:T(8,128)(2,1)}, u32[]{:S(2)}, u32[]{:S(2)}) collective-permute-start(bf16[2048,256]{1,0:T(8,128)(2,1)} %collective-permute-done.6.refs_6_), channel_id=1, source_target_pairs={{0,1},{1,0},{2,3},{3,2},{4,5},{5,4},{6,7},{7,6},{8,9},{9,8},{10,11... | collective-permute-start | bytes 3145736 | tf_op jit(solution)/shard_map/ppermute | solution.py:27
  115.0 32.3 %collective-permute-start.14 = (bf16[256,2048]{1,0:T(8,128)(2,1)S(1)}, bf16[256,2048]{1,0:T(8,128)(2,1)}, u32[]{:S(2)}, u32[]{:S(2)}) collective-permute-start(bf16[256,2048]{1,0:T(8,128)(2,1)S(1)} %bitcast.15), channel_id=1, source_target_pairs={{0,1},{1,0},{2,3},{3,2},{4,5},{5,4},{6,7},{7,6},{8,9},{9,8},{10,11... | collective-permute-start | bytes 3145736 | tf_op jit(solution)/shard_map/ppermute | solution.py:27
  115.0 32.3 %collective-permute-start.16 = (bf16[256,2048]{1,0:T(8,128)(2,1)}, bf16[256,2048]{1,0:T(8,128)(2,1)}, u32[]{:S(2)}, u32[]{:S(2)}) collective-permute-start(bf16[256,2048]{1,0:T(8,128)(2,1)} %collective-permute-done.15.refs_2_), channel_id=1, source_target_pairs={{0,1},{1,0},{2,3},{3,2},{4,5},{5,4},{6,7},{7,6},{8,9},{9,8},{10,11... | collective-permute-start | bytes 3145736 | tf_op jit(solution)/shard_map/ppermute | solution.py:27
  118.7 10.5 %collective-permute-start.2 = (bf16[80,2048]{1,0:T(8,128)(2,1)}, bf16[80,2048]{1,0:T(8,128)(2,1)S(1)}, u32[]{:S(2)}, u32[]{:S(2)}) collective-permute-start(bf16[80,2048]{1,0:T(8,128)(2,1)} %get-tuple-element.26), channel_id=1, source_target_pairs={{0,8},{8,0},{16,24},{24,16},{1,9},{9,1},{17,25},{25,17},{2,10},{10... | collective-permute-start | bytes 983048 | tf_op jit(solution)/shard_map/ppermute | solution.py:27
  121.0 10.9 %collective-permute-start.3 = (bf16[80,2048]{1,0:T(8,128)(2,1)}, bf16[80,2048]{1,0:T(8,128)(2,1)S(1)}, u32[]{:S(2)}, u32[]{:S(2)}) collective-permute-start(bf16[80,2048]{1,0:T(8,128)(2,1)} %get-tuple-element.27), channel_id=1, source_target_pairs={{0,16},{8,24},{16,0},{24,8},{1,17},{9,25},{17,1},{25,9},{2,18},{10... | collective-permute-start | bytes 983048 | tf_op jit(solution)/shard_map/ppermute | solution.py:27
  129.2 10.2 %copy-start.9 = (bf16[80,2048]{1,0:T(8,128)(2,1)}, bf16[80,2048]{1,0:T(8,128)(2,1)S(1)}, u32[]{:S(2)}) copy-start(bf16[80,2048]{1,0:T(8,128)(2,1)S(1)} %collective-permute-done.2.refs_1_) | copy-start | bytes 983044
  129.2 10.2 %collective-permute-start.4 = (bf16[80,2048]{1,0:T(8,128)(2,1)}, bf16[80,2048]{1,0:T(8,128)(2,1)S(1)}, u32[]{:S(2)}, u32[]{:S(2)}) collective-permute-start(bf16[80,2048]{1,0:T(8,128)(2,1)} %get-tuple-element.28), channel_id=1, source_target_pairs={{0,24},{8,16},{16,8},{24,0},{1,25},{9,17},{17,9},{25,1},{2,26},{10... | collective-permute-start | bytes 983048 | tf_op jit(solution)/shard_map/ppermute | solution.py:27
  131.9 7.5 %copy-start.10 = (bf16[80,2048]{1,0:T(8,128)(2,1)}, bf16[80,2048]{1,0:T(8,128)(2,1)S(1)}, u32[]{:S(2)}) copy-start(bf16[80,2048]{1,0:T(8,128)(2,1)S(1)} %collective-permute-done.3.refs_2_) | copy-start | bytes 983044
  139.4 0.7 copy-start.11
  152.2 10.8 %collective-permute-start.17 = (bf16[80,2048]{1,0:T(8,128)(2,1)}, bf16[80,2048]{1,0:T(8,128)(2,1)S(1)}, u32[]{:S(2)}, u32[]{:S(2)}) collective-permute-start(bf16[80,2048]{1,0:T(8,128)(2,1)} %get-tuple-element.30), channel_id=1, source_target_pairs={{0,8},{8,0},{16,24},{24,16},{1,9},{9,1},{17,25},{25,17},{2,10},{10... | collective-permute-start | bytes 983048 | tf_op jit(solution)/shard_map/ppermute | solution.py:27
  153.7 17.4 %collective-permute-start.18 = (bf16[80,2048]{1,0:T(8,128)(2,1)}, bf16[80,2048]{1,0:T(8,128)(2,1)S(1)}, u32[]{:S(2)}, u32[]{:S(2)}) collective-permute-start(bf16[80,2048]{1,0:T(8,128)(2,1)} %get-tuple-element.31), channel_id=1, source_target_pairs={{0,16},{8,24},{16,0},{24,8},{1,17},{9,25},{17,1},{25,9},{2,18},{10... | collective-permute-start | bytes 983048 | tf_op jit(solution)/shard_map/ppermute | solution.py:27
  155.2 16.7 %collective-permute-start.19 = (bf16[80,2048]{1,0:T(8,128)(2,1)}, bf16[80,2048]{1,0:T(8,128)(2,1)S(1)}, u32[]{:S(2)}, u32[]{:S(2)}) collective-permute-start(bf16[80,2048]{1,0:T(8,128)(2,1)} %get-tuple-element.32), channel_id=1, source_target_pairs={{0,24},{8,16},{16,8},{24,0},{1,25},{9,17},{17,9},{25,1},{2,26},{10... | collective-permute-start | bytes 983048 | tf_op jit(solution)/shard_map/ppermute | solution.py:27
  156.1 21.6 %collective-permute-start.21 = (bf16[80,2048]{1,0:T(8,128)(2,1)}, bf16[80,2048]{1,0:T(8,128)(2,1)S(1)}, u32[]{:S(2)}, u32[]{:S(2)}) collective-permute-start(bf16[80,2048]{1,0:T(8,128)(2,1)} %get-tuple-element.34), channel_id=1, source_target_pairs={{0,8},{8,0},{16,24},{24,16},{1,9},{9,1},{17,25},{25,17},{2,10},{10... | collective-permute-start | bytes 983048 | tf_op jit(solution)/shard_map/ppermute | solution.py:27
  157.2 24.6 %collective-permute-start.22 = (bf16[80,2048]{1,0:T(8,128)(2,1)}, bf16[80,2048]{1,0:T(8,128)(2,1)S(1)}, u32[]{:S(2)}, u32[]{:S(2)}) collective-permute-start(bf16[80,2048]{1,0:T(8,128)(2,1)} %get-tuple-element.35), channel_id=1, source_target_pairs={{0,16},{8,24},{16,0},{24,8},{1,17},{9,25},{17,1},{25,9},{2,18},{10... | collective-permute-start | bytes 983048 | tf_op jit(solution)/shard_map/ppermute | solution.py:27
  163.0 8.9 %copy-start.12 = (bf16[80,2048]{1,0:T(8,128)(2,1)}, bf16[80,2048]{1,0:T(8,128)(2,1)S(1)}, u32[]{:S(2)}) copy-start(bf16[80,2048]{1,0:T(8,128)(2,1)S(1)} %collective-permute-done.17.refs_1_) | copy-start | bytes 983044
  163.0 20.3 %collective-permute-start.23 = (bf16[80,2048]{1,0:T(8,128)(2,1)}, bf16[80,2048]{1,0:T(8,128)(2,1)S(1)}, u32[]{:S(2)}, u32[]{:S(2)}) collective-permute-start(bf16[80,2048]{1,0:T(8,128)(2,1)} %get-tuple-element.36), channel_id=1, source_target_pairs={{0,24},{8,16},{16,8},{24,0},{1,25},{9,17},{17,9},{25,1},{2,26},{10... | collective-permute-start | bytes 983048 | tf_op jit(solution)/shard_map/ppermute | solution.py:27
  171.1 0.8 copy-start.13
  171.9 0.7 copy-start.15
  176.0 34.8 %collective-permute-start.20 = (bf16[128,2048]{1,0:T(8,128)(2,1)}, bf16[128,2048]{1,0:T(8,128)(2,1)S(1)}, u32[]{:S(2)}, u32[]{:S(2)}) collective-permute-start(bf16[128,2048]{1,0:T(8,128)(2,1)} %shard_map.120), channel_id=1, source_target_pairs={{0,4},{1,5},{2,6},{3,7},{4,0},{5,1},{6,2},{7,3},{8,12},{9,13},{10,... | collective-permute-start | bytes 1572872 | tf_op jit(solution)/shard_map/ppermute | solution.py:27
  177.7 5.6 %copy-start.6 = (bf16[80,2048]{1,0:T(8,128)(2,1)}, bf16[80,2048]{1,0:T(8,128)(2,1)S(1)}, u32[]{:S(2)}) copy-start(bf16[80,2048]{1,0:T(8,128)(2,1)S(1)} %collective-permute-done.21.refs_1_) | copy-start | bytes 983044
  181.8 1.5 copy-start.7
  183.3 0.7 copy-start.8
  196.2 10.8 %collective-permute-start.24 = (bf16[80,2048]{1,0:T(8,128)(2,1)}, bf16[80,2048]{1,0:T(8,128)(2,1)S(1)}, u32[]{:S(2)}, u32[]{:S(2)}) collective-permute-start(bf16[80,2048]{1,0:T(8,128)(2,1)} %get-tuple-element.38), channel_id=1, source_target_pairs={{0,8},{8,0},{16,24},{24,16},{1,9},{9,1},{17,25},{25,17},{2,10},{10... | collective-permute-start | bytes 983048 | tf_op jit(solution)/shard_map/ppermute | solution.py:27
  196.8 14.1 %collective-permute-start.25 = (bf16[80,2048]{1,0:T(8,128)(2,1)}, bf16[80,2048]{1,0:T(8,128)(2,1)S(1)}, u32[]{:S(2)}, u32[]{:S(2)}) collective-permute-start(bf16[80,2048]{1,0:T(8,128)(2,1)} %get-tuple-element.39), channel_id=1, source_target_pairs={{0,16},{8,24},{16,0},{24,8},{1,17},{9,25},{17,1},{25,9},{2,18},{10... | collective-permute-start | bytes 983048 | tf_op jit(solution)/shard_map/ppermute | solution.py:27
  198.6 12.3 %collective-permute-start.26 = (bf16[80,2048]{1,0:T(8,128)(2,1)}, bf16[80,2048]{1,0:T(8,128)(2,1)S(1)}, u32[]{:S(2)}, u32[]{:S(2)}) collective-permute-start(bf16[80,2048]{1,0:T(8,128)(2,1)} %get-tuple-element.40), channel_id=1, source_target_pairs={{0,24},{8,16},{16,8},{24,0},{1,25},{9,17},{17,9},{25,1},{2,26},{10... | collective-permute-start | bytes 983048 | tf_op jit(solution)/shard_map/ppermute | solution.py:27
  207.0 3.9 %copy-start.14 = (bf16[80,2048]{1,0:T(8,128)(2,1)}, bf16[80,2048]{1,0:T(8,128)(2,1)S(1)}, u32[]{:S(2)}) copy-start(bf16[80,2048]{1,0:T(8,128)(2,1)S(1)} %collective-permute-done.24.refs_1_) | copy-start | bytes 983044
  210.8 0.7 copy-start.16
  210.8 0.9 copy-start.17
  210.8 1.1 copy-start.5

commit v2 on v1

v2 whole, which is shorter than its diff:
```python
import functools

import jax
import jax.numpy as jnp
from jax import lax
from jax.experimental import pallas as pl
from jax.experimental.pallas import tpu as pltpu
from jax.sharding import PartitionSpec as P


HEAD = 64
WINDOW = 128
LANES = 128
SLOT_TILE = 16


eps = 1e-06
clamp_limit = 7.0
sigmoid_alpha = 1.702

F32 = jnp.float32
BF16 = jnp.bfloat16


def grant(mebibytes):
    return pltpu.CompilerParams(vmem_limit_bytes=mebibytes * 2**20)


def exchange(block, axis, partner):
    devices = range(lax.axis_size(axis))
    return lax.ppermute(block, axis, [(i, partner(i)) for i in devices])


def from_behind(block, axis):
    devices = range(lax.axis_size(axis))
    return lax.ppermute(block, axis, [(i - 1, i) for i in devices if i > 0])


def first_kernel(k_ref, v_ref, gate_ref, tail_ref, top_ref, sem):
    top = pltpu.make_async_copy(gate_ref.at[pl.ds(0, top_ref.shape[0])], top_ref, sem)
    top.start()
    kv_cols = k_ref.shape[1]
    tail_ref[:, :kv_cols] = k_ref[...]
    tail_ref[:, kv_cols:] = v_ref[...]
    top.wait()


def first_moves(key_heads, value_heads, gate):
    span, kv_cols = key_heads.shape
    last = pl.BlockSpec((WINDOW, kv_cols), lambda i: (span // WINDOW - 1, 0))
    stored = pl.BlockSpec(memory_space=pltpu.HBM)
    return pl.pallas_call(
        first_kernel,
        grid=(1,),
        in_specs=[last, last, stored],
        out_specs=[pl.BlockSpec(memory_space=pltpu.VMEM)] * 2,
        out_shape=[
            jax.ShapeDtypeStruct((WINDOW, 2 * kv_cols), BF16),
            jax.ShapeDtypeStruct((gate.shape[0] // 2, gate.shape[1]), BF16),
        ],
        scratch_shapes=[pltpu.SemaphoreType.DMA],
        name="first_moves",
    )(key_heads, value_heads, gate)


def cut_kernel(gate_ref, down_ref, end_ref, left_ref, right_ref, sems):
    rows, cols = end_ref.shape[0], left_ref.shape[1]
    copies = [
        pltpu.make_async_copy(gate_ref.at[pl.ds(rows, rows)], end_ref, sems.at[0]),
        pltpu.make_async_copy(down_ref.at[:, pl.ds(0, cols)], left_ref, sems.at[1]),
        pltpu.make_async_copy(down_ref.at[:, pl.ds(cols, cols)], right_ref, sems.at[2]),
    ]
    for copy in copies:
        copy.start()
    for copy in copies:
        copy.wait()


def cut_weights(gate, down):
    stored = pl.BlockSpec(memory_space=pltpu.HBM)
    half_down = jax.ShapeDtypeStruct((down.shape[0], down.shape[1] // 2), BF16)
    return pl.pallas_call(
        cut_kernel,
        in_specs=[stored] * 2,
        out_specs=[pl.BlockSpec(memory_space=pltpu.VMEM)] * 3,
        out_shape=[
            jax.ShapeDtypeStruct((gate.shape[0] // 2, gate.shape[1]), BF16),
            half_down,
            half_down,
        ],
        scratch_shapes=[pltpu.SemaphoreType.DMA((3,))],
        name="cut_weights",
    )(gate, down)


def attention_kernel(
    info_ref, sink_ref, q_hbm, k_hbm, v_hbm, tail_ref, out_ref, q_ref, k_ref, v_ref, kk_ref, vt_ref,
    logit_ref, spread_ref, rest_ref, sems, *, blocks, kv_local, group_size,
):
    kv_cols = kv_local * HEAD
    copies = [
        pltpu.make_async_copy(source, target, sems.at[j])
        for j, (source, target) in enumerate(((k_hbm, k_ref), (v_hbm, v_ref), (q_hbm, q_ref)))
    ]
    for copy in copies:
        copy.start()
    row = lax.broadcasted_iota(jnp.int32, (WINDOW, 2 * WINDOW), 0)
    col = lax.broadcasted_iota(jnp.int32, (WINDOW, 2 * WINDOW), 1)
    first_head = lax.broadcasted_iota(jnp.int32, (1, 2 * WINDOW), 1) < WINDOW
    before = row > lax.rem(col, WINDOW)
    low = lax.broadcasted_iota(jnp.int32, (WINDOW, 2 * HEAD), 1) < HEAD
    penalty = jnp.where(info_ref[0] == 0, -jnp.inf, 0.0)
    zeros = jnp.zeros((WINDOW, 2 * WINDOW), BF16)
    ones_rows = vt_ref.shape[1] - HEAD
    copies[0].wait()
    copies[1].wait()
    for block in range(blocks + 1):
        to = slice(block * WINDOW, (block + 1) * WINDOW)
        if block == 0:
            keys, values = tail_ref[:, :kv_cols], tail_ref[:, kv_cols:]
        else:
            at = slice((block - 1) * WINDOW, block * WINDOW)
            keys, values = k_ref[at, :], v_ref[at, :]
        turned = values.astype(F32).T.astype(BF16)
        for kv in range(kv_local):
            part = slice(kv * HEAD, (kv + 1) * HEAD)
            kk_ref[kv, to, :] = jnp.concatenate([keys[:, part], keys[:, part]], axis=1)
            vt_ref[kv, :HEAD, to] = turned[part, :]
            vt_ref[kv, HEAD:, to] = jnp.ones((ones_rows, WINDOW), BF16)
    copies[2].wait()
    per_block = out_ref.shape[0] // blocks
    pairs = kv_local * group_size // 2
    work = [(block, pair) for block in range(blocks) for pair in range(pairs)]
    for block, pair in work:
        band = slice(block * WINDOW, (block + 2) * WINDOW)
        queries = q_ref[
            block * WINDOW : (block + 1) * WINDOW, pair * 2 * HEAD : (pair + 1) * 2 * HEAD
        ] * jnp.asarray(HEAD ** (-0.5), BF16)
        blank = jnp.zeros_like(queries)
        stacked = jnp.concatenate(
            [jnp.where(low, queries, blank), jnp.where(low, blank, queries)], axis=0
        )
        scores = lax.dot_general(
            kk_ref[2 * pair // group_size, band, :],
            stacked,
            (((1,), (1,)), ((), ())),
            preferred_element_type=F32,
        )
        earlier = scores[:WINDOW, :]
        if block == 0:
            earlier = earlier + penalty
        logit_ref[block * pairs + pair] = jnp.where(before, earlier, scores[WINDOW:, :])
    for block, pair in work:
        item = block * pairs + pair
        logits = logit_ref[item]
        sink = jnp.where(first_head, sink_ref[2 * pair], sink_ref[2 * pair + 1])
        top = jnp.maximum(jnp.max(logits, axis=0, keepdims=True), sink)
        raised = jnp.exp(logits - top).astype(BF16)
        spread_ref[item, :WINDOW, :] = jnp.where(before, raised, zeros)
        spread_ref[item, WINDOW:, :] = jnp.where(before, zeros, raised)
        rest_ref[item] = jnp.broadcast_to(jnp.exp(sink - top), rest_ref.shape[1:])
    for block, pair in work:
        item = block * pairs + pair
        band = slice(block * WINDOW, (block + 2) * WINDOW)
        summed = jnp.dot(
            vt_ref[2 * pair // group_size, :, band], spread_ref[item], preferred_element_type=F32
        )
        total = summed[HEAD : HEAD + 1, :] + rest_ref[item][:1, :]
        scaled = summed[:HEAD, :] * (1.0 / total)
        turned = jnp.concatenate([scaled[:, :WINDOW], scaled[:, WINDOW:]], axis=0).T
        out_ref[
            block * per_block : (block + 1) * per_block, :, pair * 2 * HEAD : (pair + 1) * 2 * HEAD
        ] = turned.astype(BF16).reshape((per_block, out_ref.shape[1], 2 * HEAD))


def attend(query_heads, key_heads, value_heads, sink_logit, tail, tok_rows):
    span, q_cols = query_heads.shape
    kv_cols = key_heads.shape[1]
    kv_local = kv_cols // HEAD
    smem = pl.BlockSpec(memory_space=pltpu.SMEM)
    whole = pl.BlockSpec(memory_space=pltpu.VMEM)
    stored = pl.BlockSpec(memory_space=pltpu.HBM)
    items = span // WINDOW * q_cols // (2 * HEAD)
    info = lax.axis_index("sp").astype(jnp.int32).reshape(1)
    return pl.pallas_call(
        functools.partial(
            attention_kernel,
            blocks=span // WINDOW,
            kv_local=kv_local,
            group_size=q_cols // kv_cols,
        ),
        in_specs=[smem, smem] + [stored] * 3 + [whole],
        out_specs=whole,
        out_shape=jax.ShapeDtypeStruct((span // tok_rows, tok_rows, q_cols), BF16),
        scratch_shapes=[
            pltpu.VMEM((span, q_cols), BF16),
            pltpu.VMEM((span, kv_cols), BF16),
            pltpu.VMEM((span, kv_cols), BF16),
            pltpu.VMEM((kv_local, span + WINDOW, 2 * HEAD), BF16),
            pltpu.VMEM((kv_local, HEAD + SLOT_TILE, span + WINDOW), BF16),
            pltpu.VMEM((items, WINDOW, 2 * WINDOW), F32),
            pltpu.VMEM((items, 2 * WINDOW, 2 * WINDOW), BF16),
            pltpu.VMEM((items, 8, 2 * WINDOW), F32),
            pltpu.SemaphoreType.DMA((3,)),
        ],
        name="attend",
    )(info, sink_logit, query_heads, key_heads, value_heads, tail)


def slots_of(ids, expert, slots):
    choices, rows = ids.shape
    chosen = jnp.zeros((8, rows), F32)
    for k in range(choices):
        match = jnp.broadcast_to(ids[k : k + 1, :], (8, rows)) == expert
        chosen += jnp.where(match, 1.0, 0.0)
    earlier = lax.broadcasted_iota(jnp.int32, (rows, rows), 0) < lax.broadcasted_iota(
        jnp.int32, (rows, rows), 1
    )
    rank = jnp.dot(
        chosen.astype(BF16), earlier.astype(F32).astype(BF16), preferred_element_type=F32
    )
    place = jnp.where(chosen > 0.5, rank, -1.0).astype(jnp.int32)
    return lax.broadcasted_iota(jnp.int32, (slots, rows), 0) == place[:1, :]


def gather_kernel(info_ref, ids_ref, gather_ref, *, expert_count, slots):
    for block in range(ids_ref.shape[0]):
        for distance in range(expert_count):
            hot = slots_of(ids_ref[block], info_ref[0] ^ distance, slots)
            gather_ref[block, distance] = hot.astype(F32).astype(BF16)


def spread_kernel(info_ref, ids_ref, *refs, expert_count, slots):
    weight_refs, spread_ref = refs[:-1], refs[-1]
    blocks, choices, rows = ids_ref.shape
    for block in range(blocks):
        ids = ids_ref[block]
        for distance in range(expert_count):
            expert = info_ref[0] ^ distance
            weight = jnp.zeros((1, rows), F32)
            for k in range(choices):
                match = ids[k : k + 1, :] == expert
                weight += jnp.where(match, weight_refs[block][k : k + 1, :], 0.0)
            weight = jnp.where(slots_of(ids, expert, LANES), weight, 0.0).T
            high = weight.astype(BF16)
            spread_ref[block, distance, 0] = high
            spread_ref[block, distance, 1] = (weight - high.astype(F32)).astype(BF16)


def table(kernel, operands, shape, expert_count, slots):
    whole = pl.BlockSpec(memory_space=pltpu.VMEM)
    return pl.pallas_call(
        functools.partial(kernel, expert_count=expert_count, slots=slots),
        in_specs=[pl.BlockSpec(memory_space=pltpu.SMEM)] + [whole] * (len(operands) - 1),
        out_specs=whole,
        out_shape=jax.ShapeDtypeStruct(shape, BF16),
        compiler_params=grant(4),
    )(*operands)


def pack(gather_ref, normed, send_refs):
    for distance, send_ref in enumerate(send_refs):
        send_ref[...] = jnp.dot(
            gather_ref[0, distance], normed, preferred_element_type=F32
        ).astype(BF16)


def project_kernel(
    att_ref, w_hbm, res_ref, gain_ref, gather_ref, stream_ref, *refs, expert_count, parts, tile
):
    part_refs, send_refs = refs[:parts], refs[parts:-3]
    acc_ref, w_ref, sems = refs[-3:]
    sources, _, cols = att_ref.shape
    width = stream_ref.shape[1]
    copies = []
    for n in range(width // tile):
        part = pl.ds(n * tile, tile)
        copies.append(pltpu.make_async_copy(w_hbm.at[:, part], w_ref.at[n], sems.at[n]))
    for copy in copies:
        copy.start()
    for n in range(width // tile):
        copies[n].wait()
        total = None
        for k in range(sources):
            piece = jnp.dot(
                att_ref[k], w_ref[n, k * cols : (k + 1) * cols, :], preferred_element_type=F32
            )
            total = piece if total is None else total + piece
        acc_ref[:, n * tile : (n + 1) * tile] = total
    stream = (res_ref[...].astype(F32) + acc_ref[...]).astype(BF16)
    stream_ref[...] = stream
    wide = stream.astype(F32)
    scale = lax.rsqrt(jnp.mean(wide * wide, axis=-1, keepdims=True) + eps)
    normed = (wide * scale * gain_ref[...]).astype(BF16)
    step = width // parts
    for h in range(parts):
        part_refs[h][...] = normed[:, h * step : (h + 1) * step]
    pack(gather_ref, normed, send_refs)


def block_of(array, block):
    zeros = (0,) * (array.ndim - 1)
    return pl.BlockSpec((1,) + array.shape[1:], lambda i: (block,) + zeros)


def project(gathered, out_weight, residual, norm_gain, gather, parts):
    _, rows, _ = gathered.shape
    width = out_weight.shape[1]
    _, expert_count, slots, _ = gather.shape
    tile = min(512, width)
    whole = pl.BlockSpec(memory_space=pltpu.VMEM)
    outs = pl.pallas_call(
        functools.partial(
            project_kernel, expert_count=expert_count, parts=parts, tile=tile
        ),
        grid=(1,),
        in_specs=[whole, pl.BlockSpec(memory_space=pltpu.HBM), whole, whole, block_of(gather, 0)],
        out_specs=[whole] * (1 + parts + expert_count),
        out_shape=[jax.ShapeDtypeStruct((rows, width), BF16)]
        + [jax.ShapeDtypeStruct((rows, width // parts), BF16)] * parts
        + [jax.ShapeDtypeStruct((slots, width), BF16)] * expert_count,
        scratch_shapes=[
            pltpu.VMEM((rows, width), F32),
            pltpu.VMEM((width // tile, out_weight.shape[0], tile), BF16),
            pltpu.SemaphoreType.DMA((width // tile,)),
        ],
        name="project",
    )(gathered, out_weight, residual, norm_gain, gather)
    return outs[0], outs[1 : 1 + parts], outs[1 + parts :]


def pack_kernel(gather_ref, far_ref, *send_refs):
    pack(gather_ref, far_ref[...], send_refs)


def pack_far(gather, far):
    _, expert_count, slots, _ = gather.shape
    whole = pl.BlockSpec(memory_space=pltpu.VMEM)
    return pl.pallas_call(
        pack_kernel,
        grid=(1,),
        in_specs=[block_of(gather, 1), whole],
        out_specs=[whole] * expert_count,
        out_shape=[jax.ShapeDtypeStruct((slots, far.shape[1]), BF16)] * expert_count,
        compiler_params=grant(4),
        name="pack_far",
    )(gather, far)


def gate_up_kernel(*refs, groups, parts, slots, pieces, hid, chunks):
    row_refs, refs = refs[: groups * parts], refs[groups * parts :]
    count = sum(chunks)
    gate_refs, ups = refs[:count], refs[count : count + pieces]
    hidden_ref, picked_ref, weight_ref, sems = refs[count + pieces :]
    copies, at = [], 0
    for p in range(pieces):
        group, row = [], 0
        for chunk in gate_refs[at : at + chunks[p]]:
            target = weight_ref.at[p, 0, pl.ds(row, chunk.shape[0])]
            group.append(pltpu.make_async_copy(chunk, target, sems.at[p, len(group)]))
            row += chunk.shape[0]
        at += chunks[p]
        group.append(pltpu.make_async_copy(ups[p], weight_ref.at[p, 1], sems.at[p, len(group)]))
        copies.append(group)
    for group in copies:
        for copy in group:
            copy.start()
    step = picked_ref.shape[1] // parts
    for b in range(groups):
        for h in range(parts):
            rows = row_refs[h * groups + b][...]
            picked_ref[b * slots : (b + 1) * slots, h * step : (h + 1) * step] = rows
    picked = picked_ref[...]
    for p in range(pieces):
        for copy in copies[p]:
            copy.wait()
        gate_pre = jnp.dot(picked, weight_ref[p, 0], preferred_element_type=F32)
        upward = jnp.dot(picked, weight_ref[p, 1], preferred_element_type=F32)
        capped = jnp.minimum(gate_pre, clamp_limit)
        linear = jnp.clip(upward, -clamp_limit, clamp_limit)
        hidden = capped * jax.nn.sigmoid(sigmoid_alpha * capped) * (linear + 1.0)
        hidden_ref[:, p * hid : (p + 1) * hid] = hidden.astype(BF16)


def gate_up(rows, parts, gates, ups):
    groups, pieces = len(rows) // parts, len(gates)
    slots = rows[0].shape[0]
    width, hid = ups[0].shape
    chunks = tuple(len(piece) for piece in gates)
    flat = [chunk for piece in gates for chunk in piece]
    whole = pl.BlockSpec(memory_space=pltpu.VMEM)
    stored = pl.BlockSpec(memory_space=pltpu.HBM)
    return pl.pallas_call(
        functools.partial(
            gate_up_kernel,
            groups=groups,
            parts=parts,
            slots=slots,
            pieces=pieces,
            hid=hid,
            chunks=chunks,
        ),
        in_specs=[whole] * len(rows) + [stored] * (len(flat) + pieces),
        out_specs=whole,
        out_shape=jax.ShapeDtypeStruct((groups * slots, pieces * hid), BF16),
        scratch_shapes=[
            pltpu.VMEM((groups * slots, width), BF16),
            pltpu.VMEM((pieces, 2, width, hid), BF16),
            pltpu.SemaphoreType.DMA((pieces, max(chunks) + 1)),
        ],
        compiler_params=grant(20),
    )(*rows, *flat, *ups)


def down_kernel(hidden_ref, *refs, groups, slots, hid, chunks, tile):
    out_refs = refs[sum(chunks) :]
    width = out_refs[0].shape[1]
    for n in range(width // tile):
        total, at = None, 0
        for p, count in enumerate(chunks):
            ref = refs[at + n * tile * count // width]
            start = n * tile % (width // count)
            at += count
            part = jnp.dot(
                hidden_ref[:, p * hid : (p + 1) * hid],
                ref[:, start : start + tile],
                preferred_element_type=F32,
            )
            total = part if total is None else total + part
        expert_out = total.astype(BF16)
        for b in range(groups):
            out_refs[b][:, n * tile : (n + 1) * tile] = expert_out[b * slots : (b + 1) * slots, :]


def down(hidden, downs, groups, part, parts):
    hid = downs[0][0].shape[0]
    full = sum(chunk.shape[1] for chunk in downs[0])
    width = full // parts
    slots = hidden.shape[0] // groups
    whole = pl.BlockSpec(memory_space=pltpu.VMEM)
    operands, specs, chunks = [], [], []
    for piece in downs:
        if len(piece) == 1:
            operands.append(piece[0])
            specs.append(pl.BlockSpec((hid, width), lambda i: (0, part)))
            chunks.append(1)
        else:
            used = piece[part * len(piece) // parts : (part + 1) * len(piece) // parts]
            operands += used
            specs += [whole] * len(used)
            chunks.append(len(used))
    body = functools.partial(
        down_kernel,
        groups=groups,
        slots=slots,
        hid=hid,
        chunks=tuple(chunks),
        tile=min(512, width),
    )
    return pl.pallas_call(
        body,
        grid=(1,),
        in_specs=[whole] + specs,
        out_specs=[whole] * groups,
        out_shape=[jax.ShapeDtypeStruct((slots, width), BF16)] * groups,
        compiler_params=grant(12),
    )(hidden, *operands)


def unpack(spread_ref, back_refs):
    slots = back_refs[0].shape[0]
    total = None
    for term in (1, 0):
        for distance, back_ref in enumerate(back_refs):
            part = jnp.dot(
                spread_ref[0, distance, term][:, :slots], back_ref[...], preferred_element_type=F32
            )
            total = part if total is None else total + part
    return total


def combine_far_kernel(spread_ref, *refs):
    refs[-1][...] = unpack(spread_ref, refs[:-1]).astype(BF16)


def combine_own_kernel(spread_ref, stream_ref, *refs, parts):
    far_refs, back_refs, out_ref = refs[:parts], refs[parts:-1], refs[-1]
    total = unpack(spread_ref, back_refs) + stream_ref[...].astype(F32)
    step = total.shape[1] // parts
    for h in range(parts):
        cols = slice(h * step, (h + 1) * step)
        out_ref[:, cols] = (total[:, cols] + far_refs[h][...].astype(F32)).astype(BF16)


def combine(kernel, spread, block, extra, backs):
    rows = spread.shape[3]
    whole = pl.BlockSpec(memory_space=pltpu.VMEM)
    return pl.pallas_call(
        kernel,
        grid=(1,),
        in_specs=[block_of(spread, block)] + [whole] * (len(extra) + len(backs)),
        out_specs=whole,
        out_shape=jax.ShapeDtypeStruct((rows, backs[0].shape[1]), BF16),
        compiler_params=grant(10),
    )(spread, *extra, *backs)


def layer(
    query_heads,
    key_heads,
    value_heads,
    sink_logit,
    residual,
    out_weight,
    norm_gain,
    routes,
    route_weight,
    gate_weight,
    up_weight,
    down_weight,
):
    expert_count = lax.axis_size("sp")
    half = lax.axis_size("tp") // 2
    tok_rows = residual.shape[0]
    choose_count = routes.shape[1]
    parts = parts_of(expert_count)
    tp_index = lax.axis_index("tp")
    index = lax.axis_index("sp").astype(jnp.int32).reshape(1)

    def across(block):
        return exchange(block, "tp", lambda i: (i + half) % (2 * half))

    def to_experts(blocks):
        return [blocks[0]] + [
            exchange(blocks[d], "sp", lambda i, d=d: i ^ d)
            for d in range(1, expert_count)
        ]

    own_gate, own_up, own_down = gate_weight[0], up_weight[0], down_weight[0]
    tail, top = first_moves(key_heads, value_heads, own_gate)
    tail = from_behind(tail, "sp")
    end, left, right = cut_weights(own_gate, own_down)
    gates, ups, downs = [[own_gate]], [[own_up]], [[own_down]]
    own_chunks = {"gate": [top, end], "up": [own_up], "down": [left, right]}
    for distance in range(1, half):
        for what, held in (("gate", gates), ("up", ups), ("down", downs)):
            if distance % 2:
                step, chunks = 1, held[distance - 1]
            else:
                step, chunks = distance, own_chunks[what]
            held.append([exchange(chunk, "tp", lambda i, s=step: i ^ s) for chunk in chunks])
    ups = [piece[0] for piece in ups]

    attended = attend(query_heads, key_heads, value_heads, sink_logit, tail, tok_rows)
    gathered = lax.all_to_all(attended, "tp", split_axis=0, concat_axis=0, tiled=True)

    capacity = max(2, 5 * tok_rows * choose_count // (4 * expert_count))
    slots = -(-capacity // SLOT_TILE) * SLOT_TILE
    starts = [tp_index * tok_rows, (tp_index + half) % (2 * half) * tok_rows]
    ids = jnp.stack([lax.dynamic_slice_in_dim(routes.T, at, tok_rows, 1) for at in starts])
    weight_own = route_weight.T
    weight_far = across(weight_own)
    gather = table(
        gather_kernel, (index, ids), (2, expert_count, slots, tok_rows), expert_count, slots
    )
    spread = table(
        spread_kernel,
        (index, ids, weight_own, weight_far),
        (2, expert_count, 2, tok_rows, LANES),
        expert_count,
        slots,
    )

    stream, normed, send_own = project(
        gathered, out_weight, residual, norm_gain.reshape(1, -1), gather, parts
    )
    rows_far = []
    for h in range(parts):
        far = across(normed[h])
        rows_far += to_experts(pack_far(gather, far))
    rows_own = to_experts(send_own)
    hidden_own = gate_up(rows_own, 1, gates, ups)
    hidden_far = gate_up(rows_far, parts, gates, ups)
    part_far = []
    for h in range(parts):
        backs = down(hidden_far, downs, expert_count, h, parts)
        backs = to_experts(backs)
        mixed = combine(combine_far_kernel, spread, 1, (), backs)
        part_far.append(across(mixed))
    backs = down(hidden_own, downs, expert_count, 0, 1)
    backs = to_experts(backs)
    return combine(
        functools.partial(combine_own_kernel, parts=parts), spread, 0, (stream, *part_far), backs
    )


def parts_of(expert_count):
    return 2 if expert_count <= 4 else 1


def solution(mesh):
    placed = (
        P("sp", "tp"),
        P("sp", "tp"),
        P("sp", "tp"),
        P("tp"),
        P(("sp", "tp"), None),
        P(),
        P(),
        P("sp", None),
        P(("sp", "tp"), None),
        P("sp", None, "tp"),
        P("sp", None, "tp"),
        P("sp", "tp", None),
    )
    return jax.shard_map(
        layer, mesh=mesh, in_specs=placed, out_specs=P(("sp", "tp"), None), check_vma=False
    )
```

time: 217 us -> 189 us (0.87)
  Pallas kernels: 51.5 us -> 33.2 us
  waiting for transfers between devices: 117 us -> 105 us
  starting transfers between devices: 38.8 us -> 44.7 us
  local copies, waits for them, and re-layouts: 7.56 us -> 5.29 us
    pallas_call x8 -> x15, Pallas kernels: 44.5 us -> 26.3 us  [the longest x2 8.96 us: gate_up(): pl.pallas_call(functools.partial(gate_up_kernel, groups=groups, parts=par...]
    ppermute x26 -> x36, waiting for transfers between devices: 115 us -> 101 us  [exchange(): return lax.ppermute(block, axis, [(i, partner(i)) for i in devices])]
    ppermute x26 -> x36, starting transfers between devices: 29 us -> 35.8 us  [exchange(): return lax.ppermute(block, axis, [(i, partner(i)) for i in devices])]
    all_to_all x1, waiting for transfers between devices: 0.01 us -> 3.18 us  [layer(): lax.all_to_all(attended, 'tp', split_axis=0, concat_axis=0, tiled=True)]
    unnamed x38 -> x36, local copies, waits for them, and re-layouts: 3.87 us -> 4.55 us
  transfers between devices with their start and end apart: 28 -> 38, of which waited for: 14 -> 16; matrix products, arithmetic and copies ran while one was open for 1% -> 0% of each run, Pallas kernels for 15% -> 15%
where the time goes in v2:
time: 189 us
  waiting for transfers between devices  105 us (56%)
  starting transfers between devices  44.7 us (24%)
  Pallas kernels  33.2 us (18%)
  local copies, waits for them, and re-layouts  5.29 us (3%)
    ppermute x36, waiting for transfers between devices, exchange(): return lax.ppermute(block, axis, [(i, partner(i)) for i in devices])  101 us
    ppermute x36, starting transfers between devices, exchange(): return lax.ppermute(block, axis, [(i, partner(i)) for i in devices])  35.8 us
    pallas_call x2, Pallas kernels, gate_up(): pl.pallas_call(functools.partial(gate_up_kernel, groups=groups, parts=par...  8.96 us
    pallas_call x1, Pallas kernels, project(): pl.pallas_call(functools.partial(project_kernel, expert_count=expert_coun...  6.87 us
    all_to_all x1, starting transfers between devices, layer(): lax.all_to_all(attended, 'tp', split_axis=0, concat_axis=0, tiled=True)  5.44 us
    unnamed x36, local copies, waits for them, and re-layouts  4.55 us
    pallas_call x1, Pallas kernels, attend(): pl.pallas_call(functools.partial(attention_kernel, blocks=span // WINDOW,...  4.19 us
  transfers between devices with their start and end apart: 38, of which 16 were waited for; matrix products, arithmetic and copies ran while one was open for 0% of the time, Pallas kernels for 15%

profile of v2, /device:TPU:0, one launch (start us, length us, event | category | flops | bytes accessed | tf_op | source)
XLA Modules:
  0.0 188.8 jit_solution(1688940999896841469)
XLA Ops:
  0.0 2.7 %first_moves.1 = (bf16[128,256]{1,0:T(8,128)(2,1)}, bf16[1024,256]{1,0:T(8,128)(2,1)}) custom-call(bf16[1024,128]{1,0:T(8,128)(2,1)} %k_hbm.1, bf16[1024,128]{1,0:T(8,128)(2,1)} %v_hbm.1, bf16[2048,256]{1,0:T(8,128)(2,1)} %bitcast.14), custom_call_target="tpu_custom_call" | custom-call | tf_op jit(solution)/shard_map/first_moves/pallas_call | solution.py:52
  2.7 3.1 %collective-permute-start.11 = (bf16[1024,256]{1,0:T(8,128)(2,1)}, bf16[1024,256]{1,0:T(8,128)(2,1)}, u32[]{:S(2)}, u32[]{:S(2)}) collective-permute-start(bf16[1024,256]{1,0:T(8,128)(2,1)} %get-tuple-element.49), channel_id=1, source_target_pairs={{0,2},{1,3},{2,0},{3,1},{4,6},{5,7},{6,4},{7,5},{8,10},{9,11},{10,... | collective-permute-start | bytes 1572872 | tf_op jit(solution)/shard_map/ppermute | solution.py:31
  5.9 2.6 %cut_weights.1 = (bf16[1024,256]{1,0:T(8,128)(2,1)}, bf16[256,1024]{1,0:T(8,128)(2,1)}, bf16[256,1024]{1,0:T(8,128)(2,1)}) custom-call(bf16[2048,256]{1,0:T(8,128)(2,1)} %bitcast.15, bf16[256,2048]{1,0:T(8,128)(2,1)} %bitcast.19), custom_call_target="tpu_custom_call" | custom-call | tf_op jit(solution)/shard_map/cut_weights/pallas_call | solution.py:82
  8.5 2.0 %collective-permute-start.12 = (bf16[1024,256]{1,0:T(8,128)(2,1)}, bf16[1024,256]{1,0:T(8,128)(2,1)S(1)}, u32[]{:S(2)}, u32[]{:S(2)}) collective-permute-start(bf16[1024,256]{1,0:T(8,128)(2,1)} %get-tuple-element.50), channel_id=1, source_target_pairs={{0,2},{1,3},{2,0},{3,1},{4,6},{5,7},{6,4},{7,5},{8,10},{9,11},{10,... | collective-permute-start | bytes 1572872 | tf_op jit(solution)/shard_map/ppermute | solution.py:31
  10.5 3.4 %collective-permute-start.1 = (bf16[128,256]{1,0:T(8,128)(2,1)}, bf16[128,256]{1,0:T(8,128)(2,1)S(1)}, u32[]{:S(2)}, u32[]{:S(2)}) collective-permute-start(bf16[128,256]{1,0:T(8,128)(2,1)} %get-tuple-element.37), channel_id=1, source_target_pairs={{0,8},{8,16},{16,24},{1,9},{9,17},{17,25},{2,10},{10,18},{18,26},{... | collective-permute-start | bytes 196616 | tf_op jit(solution)/shard_map/ppermute | solution.py:36
  14.4 1.7 collective-permute-done.1.tail_ref
  16.6 2.4 %collective-permute-done.11.refs_10_.refs_6_ = bf16[1024,256]{1,0:T(8,128)(2,1)} collective-permute-done((bf16[1024,256]{1,0:T(8,128)(2,1)}, bf16[1024,256]{1,0:T(8,128)(2,1)}, u32[]{:S(2)}, u32[]{:S(2)}) %collective-permute-start.11) | collective-permute-done | bytes 524320 | tf_op jit(solution)/shard_map/ppermute | solution.py:31
  19.0 4.2 %attend.1 = bf16[8,128,256]{2,1,0:T(8,128)(2,1)} custom-call(s32[1]{0:T(128)} %bitcast.info_ref, f32[4]{0:T(128)} %sink_ref.1, bf16[1024,256]{1,0:T(8,128)(2,1)} %q_hbm.1, bf16[1024,128]{1,0:T(8,128)(2,1)} %k_hbm.1, bf16[1024,128]{1,0:T(8,128)(2,1)} %v_hbm.1, bf16[128,256]{1,0:T(8,128)(2,1)} %copy-done.17), custom_call_target="tpu_custom_call" | custom-call | tf_op jit(solution)/shard_map/attend/pallas_call | solution.py:185
  23.2 5.4 %all-to-all-start = ((bf16[8,128,256]{2,1,0:T(8,128)(2,1)}), bf16[8,128,256]{2,1,0:T(8,128)(2,1)S(1)}, u32[]{:S(2)}, u32[]{:S(2)}) async-start(bf16[8,128,256]{2,1,0:T(8,128)(2,1)} %attend.1), calls=%async_computation | async-start | bytes 1048576 | tf_op jit(solution)/shard_map/all_to_all | solution.py:555
  28.6 26.8 %collective-permute-done.12.refs_11_.refs_7_ = bf16[1024,256]{1,0:T(8,128)(2,1)S(1)} collective-permute-done((bf16[1024,256]{1,0:T(8,128)(2,1)}, bf16[1024,256]{1,0:T(8,128)(2,1)S(1)}, u32[]{:S(2)}, u32[]{:S(2)}) %collective-permute-start.12) | collective-permute-done | bytes 524320 | tf_op jit(solution)/shard_map/ppermute | solution.py:31
  55.4 11.2 %collective-permute-done.19.refs_2_ = bf16[256,1024]{1,0:T(8,128)(2,1)S(1)} collective-permute-done((bf16[256,1024]{1,0:T(8,128)(2,1)}, bf16[256,1024]{1,0:T(8,128)(2,1)S(1)}, u32[]{:S(2)}, u32[]{:S(2)}) %collective-permute-start.19) | collective-permute-done | bytes 524320 | tf_op jit(solution)/shard_map/ppermute | solution.py:31
  67.4 10.5 %collective-permute-done.25.refs_2_.refs_3_ = bf16[256,1024]{1,0:T(8,128)(2,1)S(1)} collective-permute-done((bf16[256,1024]{1,0:T(8,128)(2,1)}, bf16[256,1024]{1,0:T(8,128)(2,1)S(1)}, u32[]{:S(2)}, u32[]{:S(2)}) %collective-permute-start.25) | collective-permute-done | bytes 524320 | tf_op jit(solution)/shard_map/ppermute | solution.py:31
  79.9 3.2 %all-to-all-done.att_ref = bf16[8,128,256]{2,1,0:T(8,128)(2,1)S(1)} async-done(((bf16[8,128,256]{2,1,0:T(8,128)(2,1)}), bf16[8,128,256]{2,1,0:T(8,128)(2,1)S(1)}, u32[]{:S(2)}, u32[]{:S(2)}) %all-to-all-start) | async-done | bytes 524320 | tf_op jit(solution)/shard_map/all_to_all | solution.py:555
  83.9 6.9 %project.1 = (bf16[128,2048]{1,0:T(8,128)(2,1)}, bf16[128,1024]{1,0:T(8,128)(2,1)}, bf16[128,1024]{1,0:T(8,128)(2,1)}, bf16[80,2048]{1,0:T(8,128)(2,1)}, bf16[80...) custom-call(bf16[8,128,256]{2,1,0:T(8,128)(2,1)} %copy-done.16, bf16[2048,2048]{1,0:T(8,128)(2,1)} %w_hbm.1, ...), custom_call_target="tpu_custom_call" | custom-call | tf_op jit(solution)/shard_map/project/pallas_call | solution.py:312
  90.8 2.2 %collective-permute-start.6 = (bf16[128,1024]{1,0:T(8,128)(2,1)}, bf16[128,1024]{1,0:T(8,128)(2,1)S(1)}, u32[]{:S(2)}, u32[]{:S(2)}) collective-permute-start(bf16[128,1024]{1,0:T(8,128)(2,1)} %get-tuple-element.44), channel_id=1, source_target_pairs={{0,4},{1,5},{2,6},{3,7},{4,0},{5,1},{6,2},{7,3},{8,12},{9,13},{10,... | collective-permute-start | bytes 786440 | tf_op jit(solution)/shard_map/ppermute | solution.py:31
  93.0 12.1 %collective-permute-done.6.far_ref = bf16[128,1024]{1,0:T(8,128)(2,1)S(1)} collective-permute-done((bf16[128,1024]{1,0:T(8,128)(2,1)}, bf16[128,1024]{1,0:T(8,128)(2,1)S(1)}, u32[]{:S(2)}, u32[]{:S(2)}) %collective-permute-start.6) | collective-permute-done | bytes 262176 | tf_op jit(solution)/shard_map/ppermute | solution.py:31
  105.4 1.6 collective-permute-start.7
  107.0 5.8 %collective-permute-done.2.far_ref = bf16[128,1024]{1,0:T(8,128)(2,1)S(1)} collective-permute-done((bf16[128,1024]{1,0:T(8,128)(2,1)}, bf16[128,1024]{1,0:T(8,128)(2,1)S(1)}, u32[]{:S(2)}, u32[]{:S(2)}) %collective-permute-start.2) | collective-permute-done | bytes 262176 | tf_op jit(solution)/shard_map/ppermute | solution.py:31
  112.8 1.5 collective-permute-start.8
  114.7 1.5 collective-permute-start.9
  116.7 2.3 %collective-permute-done.8.refs_6_ = bf16[80,1024]{1,0:T(8,128)(2,1)S(1)} collective-permute-done((bf16[80,1024]{1,0:T(8,128)(2,1)S(1)}, bf16[80,1024]{1,0:T(8,128)(2,1)S(1)}, u32[]{:S(2)}, u32[]{:S(2)}) %collective-permute-start.8) | collective-permute-done | bytes 163872 | tf_op jit(solution)/shard_map/ppermute | solution.py:31
  119.0 1.9 %collective-permute-done.9.refs_7_ = bf16[80,1024]{1,0:T(8,128)(2,1)S(1)} collective-permute-done((bf16[80,1024]{1,0:T(8,128)(2,1)S(1)}, bf16[80,1024]{1,0:T(8,128)(2,1)S(1)}, u32[]{:S(2)}, u32[]{:S(2)}) %collective-permute-start.9) | collective-permute-done | bytes 163872 | tf_op jit(solution)/shard_map/ppermute | solution.py:31
  121.8 2.5 %collective-permute-start.5 = (bf16[80,1024]{1,0:T(8,128)(2,1)S(1)}, bf16[80,1024]{1,0:T(8,128)(2,1)S(1)}, u32[]{:S(2)}, u32[]{:S(2)}) collective-permute-start(bf16[80,1024]{1,0:T(8,128)(2,1)S(1)} %get-tuple-element.43), channel_id=1, source_target_pairs={{0,24},{8,16},{16,8},{24,0},{1,25},{9,17},{17,9},{25,1},{2,26},{10... | collective-permute-start | bytes 491528 | tf_op jit(solution)/shard_map/ppermute | solution.py:31
  124.2 5.0 %collective-permute-done.4.refs_2_ = bf16[80,1024]{1,0:T(8,128)(2,1)S(1)} collective-permute-done((bf16[80,1024]{1,0:T(8,128)(2,1)S(1)}, bf16[80,1024]{1,0:T(8,128)(2,1)S(1)}, u32[]{:S(2)}, u32[]{:S(2)}) %collective-permute-start.4) | collective-permute-done | bytes 163872 | tf_op jit(solution)/shard_map/ppermute | solution.py:31
  129.2 1.5 collective-permute-start.31
  130.7 1.3 collective-permute-start.32
  132.7 1.2 copy-done.2
  133.9 1.0 copy-done.7
  135.0 4.5 %shard_map.120.hidden_ref = bf16[320,1024]{1,0:T(8,128)(2,1)S(1)} custom-call(bf16[80,1024]{1,0:T(8,128)(2,1)S(1)} %get-tuple-element.40.refs_0_, bf16[80,1024]{1,0:T(8,128)(2,1)S(1)} %collective-permute-done.3.refs_1_, bf16[80,1024]{1,0:T(8,128)(2,1)S(1)} %collective-permute-done.4.refs_2_, bf16[80,1024]{1,0:T(8,128)(2,1)S(1)} %collective-permute-done.5.refs_3_, ...), custom_call_target="tpu_custom_call" | custom-call | tf_op jit(solution)/shard_map/pallas_call | solution.py:393
  139.5 0.8 shard_map.123
  140.4 1.6 collective-permute-start.27
  142.0 1.4 collective-permute-start
  143.3 0.8 shard_map.121
  144.2 2.3 %collective-permute-done.refs_1_ = f32[2,128]{1,0:T(2,128)S(1)} collective-permute-done((f32[2,128]{1,0:T(2,128)S(1)}, f32[2,128]{1,0:T(2,128)S(1)}, u32[]{:S(2)}, u32[]{:S(2)}) %collective-permute-start) | collective-permute-done | bytes 1056 | tf_op jit(solution)/shard_map/ppermute | solution.py:31
  147.0 0.9 collective-permute-start.22
  147.9 2.1 %collective-permute-start.23 = (bf16[80,1024]{1,0:T(8,128)(2,1)S(1)}, bf16[80,1024]{1,0:T(8,128)(2,1)S(1)}, u32[]{:S(2)}, u32[]{:S(2)}) collective-permute-start(bf16[80,1024]{1,0:T(8,128)(2,1)S(1)} %get-tuple-element.55), channel_id=1, source_target_pairs={{0,24},{8,16},{16,8},{24,0},{1,25},{9,17},{17,9},{25,1},{2,26},{10... | collective-permute-start | bytes 491528 | tf_op jit(solution)/shard_map/ppermute | solution.py:31
  150.0 1.3 collective-permute-start.28
  151.9 4.4 %shard_map.125.hidden_ref = bf16[320,1024]{1,0:T(8,128)(2,1)S(1)} custom-call(bf16[80,2048]{1,0:T(8,128)(2,1)S(1)} %copy-done.14, bf16[80,2048]{1,0:T(8,128)(2,1)S(1)} %collective-permute-done.31.refs_1_, bf16[80,2048]{1,0:T(8,128)(2,1)S(1)} %collective-permute-done.32.refs_2_, bf16[80,2048]{1,0:T(8,128)(2,1)S(1)} %collective-permute-done.33.refs_3_, ...), custom_call_target="tpu_custom_call" | custom-call | tf_op jit(solution)/shard_map/pallas_call | solution.py:393
  156.4 1.5 shard_map.126
  157.9 1.6 collective-permute-start.34
  159.5 1.3 collective-permute-start.35
  160.8 1.1 collective-permute-start.36
  163.0 2.4 %collective-permute-done.28.refs_2_ = bf16[80,1024]{1,0:T(8,128)(2,1)S(1)} collective-permute-done((bf16[80,1024]{1,0:T(8,128)(2,1)S(1)}, bf16[80,1024]{1,0:T(8,128)(2,1)S(1)}, u32[]{:S(2)}, u32[]{:S(2)}) %collective-permute-start.28) | collective-permute-done | bytes 163872 | tf_op jit(solution)/shard_map/ppermute | solution.py:31
  165.4 1.3 collective-permute-start.24
  167.4 1.7 collective-permute-start.30
  169.1 5.4 %collective-permute-done.35.refs_4_ = bf16[80,2048]{1,0:T(8,128)(2,1)S(1)} collective-permute-done((bf16[80,2048]{1,0:T(8,128)(2,1)S(1)}, bf16[80,2048]{1,0:T(8,128)(2,1)S(1)}, u32[]{:S(2)}, u32[]{:S(2)}) %collective-permute-start.35) | collective-permute-done | bytes 327712 | tf_op jit(solution)/shard_map/ppermute | solution.py:31
  174.5 12.2 %collective-permute-done.30.refs_1_ = bf16[128,1024]{1,0:T(8,128)(2,1)S(1)} collective-permute-done((bf16[128,1024]{1,0:T(8,128)(2,1)S(1)}, bf16[128,1024]{1,0:T(8,128)(2,1)S(1)}, u32[]{:S(2)}, u32[]{:S(2)}) %collective-permute-start.30) | collective-permute-done | bytes 262176 | tf_op jit(solution)/shard_map/ppermute | solution.py:31
  186.7 2.1 %shard_map.127 = bf16[128,2048]{1,0:T(8,128)(2,1)} custom-call(bf16[2,4,2,128,128]{4,3,2,1,0:T(8,128)(2,1)S(1)} %shard_map.118.spread_ref, bf16[128,2048]{1,0:T(8,128)(2,1)S(1)} %copy-done.13, bf16[128,1024]{1,0:T(8,128)(2,1)S(1)} %collective-permute-done.24.refs_0_, bf16[128,1024]{1,0:T(8,128)(2,1)S(1)} %collective-permute-done.30.refs_1_, ...), custom_call_target="tpu_custom_call" | custom-call | tf_op jit(solution)/shard_map/pallas_call | solution.py:498
  (82 shorter events, 10.3 us)
Async XLA Ops:
  0.0 132.7 %copy-start = (bf16[1,2048,256]{2,1,0:T(8,128)(2,1)S(1)}, bf16[1,2048,256]{2,1,0:T(8,128)(2,1)}, u32[]{:S(2)}) copy-start(bf16[1,2048,256]{2,1,0:T(8,128)(2,1)} %param.21) | copy-start | bytes 3145732
  2.7 16.2 %collective-permute-start.11 = (bf16[1024,256]{1,0:T(8,128)(2,1)}, bf16[1024,256]{1,0:T(8,128)(2,1)}, u32[]{:S(2)}, u32[]{:S(2)}) collective-permute-start(bf16[1024,256]{1,0:T(8,128)(2,1)} %get-tuple-element.49), channel_id=1, source_target_pairs={{0,2},{1,3},{2,0},{3,1},{4,6},{5,7},{6,4},{7,5},{8,10},{9,11},{10,... | collective-permute-start | bytes 1572872 | tf_op jit(solution)/shard_map/ppermute | solution.py:31
  5.9 72.7 %collective-permute-start.16 = (bf16[2048,256]{1,0:T(8,128)(2,1)}, bf16[2048,256]{1,0:T(8,128)(2,1)}, u32[]{:S(2)}, u32[]{:S(2)}) collective-permute-start(bf16[2048,256]{1,0:T(8,128)(2,1)} %bitcast.24), channel_id=1, source_target_pairs={{0,2},{1,3},{2,0},{3,1},{4,6},{5,7},{6,4},{7,5},{8,10},{9,11},{10,... | collective-permute-start | bytes 3145736 | tf_op jit(solution)/shard_map/ppermute | solution.py:31
  8.5 46.8 %collective-permute-start.12 = (bf16[1024,256]{1,0:T(8,128)(2,1)}, bf16[1024,256]{1,0:T(8,128)(2,1)S(1)}, u32[]{:S(2)}, u32[]{:S(2)}) collective-permute-start(bf16[1024,256]{1,0:T(8,128)(2,1)} %get-tuple-element.50), channel_id=1, source_target_pairs={{0,2},{1,3},{2,0},{3,1},{4,6},{5,7},{6,4},{7,5},{8,10},{9,11},{10,... | collective-permute-start | bytes 1572872 | tf_op jit(solution)/shard_map/ppermute | solution.py:31
  10.5 5.6 %collective-permute-start.1 = (bf16[128,256]{1,0:T(8,128)(2,1)}, bf16[128,256]{1,0:T(8,128)(2,1)S(1)}, u32[]{:S(2)}, u32[]{:S(2)}) collective-permute-start(bf16[128,256]{1,0:T(8,128)(2,1)} %get-tuple-element.37), channel_id=1, source_target_pairs={{0,8},{8,16},{16,24},{1,9},{9,17},{17,25},{2,10},{10,18},{18,26},{... | collective-permute-start | bytes 196616 | tf_op jit(solution)/shard_map/ppermute | solution.py:36
  13.9 52.7 %collective-permute-start.19 = (bf16[256,1024]{1,0:T(8,128)(2,1)}, bf16[256,1024]{1,0:T(8,128)(2,1)S(1)}, u32[]{:S(2)}, u32[]{:S(2)}) collective-permute-start(bf16[256,1024]{1,0:T(8,128)(2,1)} %get-tuple-element.51), channel_id=1, source_target_pairs={{0,2},{1,3},{2,0},{3,1},{4,6},{5,7},{6,4},{7,5},{8,10},{9,11},{10,... | collective-permute-start | bytes 1572872 | tf_op jit(solution)/shard_map/ppermute | solution.py:31
  16.1 61.7 %collective-permute-start.25 = (bf16[256,1024]{1,0:T(8,128)(2,1)}, bf16[256,1024]{1,0:T(8,128)(2,1)S(1)}, u32[]{:S(2)}, u32[]{:S(2)}) collective-permute-start(bf16[256,1024]{1,0:T(8,128)(2,1)} %get-tuple-element.56), channel_id=1, source_target_pairs={{0,2},{1,3},{2,0},{3,1},{4,6},{5,7},{6,4},{7,5},{8,10},{9,11},{10,... | collective-permute-start | bytes 1572872 | tf_op jit(solution)/shard_map/ppermute | solution.py:31
  18.9 74.1 %collective-permute-start.10 = (bf16[2048,256]{1,0:T(8,128)(2,1)}, bf16[2048,256]{1,0:T(8,128)(2,1)}, u32[]{:S(2)}, u32[]{:S(2)}) collective-permute-start(bf16[2048,256]{1,0:T(8,128)(2,1)} %bitcast.16), channel_id=1, source_target_pairs={{0,1},{1,0},{2,3},{3,2},{4,5},{5,4},{6,7},{7,6},{8,9},{9,8},{10,11... | collective-permute-start | bytes 3145736 | tf_op jit(solution)/shard_map/ppermute | solution.py:31
  23.2 60.0 %all-to-all-start = ((bf16[8,128,256]{2,1,0:T(8,128)(2,1)}), bf16[8,128,256]{2,1,0:T(8,128)(2,1)S(1)}, u32[]{:S(2)}, u32[]{:S(2)}) async-start(bf16[8,128,256]{2,1,0:T(8,128)(2,1)} %attend.1), calls=%async_computation | async-start | bytes 1048576 | tf_op jit(solution)/shard_map/all_to_all | solution.py:555
  55.4 11.2 %copy-start.6 = (bf16[1024,256]{1,0:T(8,128)(2,1)}, bf16[1024,256]{1,0:T(8,128)(2,1)S(1)}, u32[]{:S(2)}) copy-start(bf16[1024,256]{1,0:T(8,128)(2,1)S(1)} %collective-permute-done.12.refs_11_.refs_7_) | copy-start | bytes 1572868
  55.4 50.1 %collective-permute-start.15 = (bf16[2048,256]{1,0:T(8,128)(2,1)}, bf16[2048,256]{1,0:T(8,128)(2,1)}, u32[]{:S(2)}, u32[]{:S(2)}) collective-permute-start(bf16[2048,256]{1,0:T(8,128)(2,1)} %bitcast.25), channel_id=1, source_target_pairs={{0,1},{1,0},{2,3},{3,2},{4,5},{5,4},{6,7},{7,6},{8,9},{9,8},{10,11... | collective-permute-start | bytes 3145736 | tf_op jit(solution)/shard_map/ppermute | solution.py:31
  66.6 24.2 %collective-permute-start.13 = (bf16[1024,256]{1,0:T(8,128)(2,1)}, bf16[1024,256]{1,0:T(8,128)(2,1)}, u32[]{:S(2)}, u32[]{:S(2)}) collective-permute-start(bf16[1024,256]{1,0:T(8,128)(2,1)} %collective-permute-done.11.refs_10_.refs_6_), channel_id=1, source_target_pairs={{0,1},{1,0},{2,3},{3,2},{4,5},{5,4},{6,7},{7,6},{8,9},{9,8},{10,11... | collective-permute-start | bytes 1572872 | tf_op jit(solution)/shard_map/ppermute | solution.py:31
  77.8 36.8 %collective-permute-start.18 = (bf16[256,2048]{1,0:T(8,128)(2,1)}, bf16[256,2048]{1,0:T(8,128)(2,1)S(1)}, u32[]{:S(2)}, u32[]{:S(2)}) collective-permute-start(bf16[256,2048]{1,0:T(8,128)(2,1)} %bitcast.20), channel_id=1, source_target_pairs={{0,1},{1,0},{2,3},{3,2},{4,5},{5,4},{6,7},{7,6},{8,9},{9,8},{10,11... | collective-permute-start | bytes 3145736 | tf_op jit(solution)/shard_map/ppermute | solution.py:31
  78.6 53.4 %collective-permute-start.17 = (bf16[2048,256]{1,0:T(8,128)(2,1)}, bf16[2048,256]{1,0:T(8,128)(2,1)}, u32[]{:S(2)}, u32[]{:S(2)}) collective-permute-start(bf16[2048,256]{1,0:T(8,128)(2,1)} %collective-permute-done.16.refs_16_.refs_12_), channel_id=1, source_target_pairs={{0,1},{1,0},{2,3},{3,2},{4,5},{5,4},{6,7},{7,6},{8,9},{9,8},{10,11... | collective-permute-start | bytes 3145736 | tf_op jit(solution)/shard_map/ppermute | solution.py:31
  83.9 21.2 %copy-start.5 = (bf16[2,4,80,128]{3,2,1,0:T(8,128)(2,1)S(1)}, bf16[2,4,80,128]{3,2,1,0:T(8,128)(2,1)}, u32[]{:S(2)}) copy-start(bf16[2,4,80,128]{3,2,1,0:T(8,128)(2,1)} %copy-done.4) | copy-start | bytes 491524
  83.9 55.6 %copy-start.1 = (bf16[1,256,2048]{2,1,0:T(8,128)(2,1)S(1)}, bf16[1,256,2048]{2,1,0:T(8,128)(2,1)}, u32[]{:S(2)}) copy-start(bf16[1,256,2048]{2,1,0:T(8,128)(2,1)} %param.23) | copy-start | bytes 3145732
  90.8 51.2 %copy-start.15 = (f32[128,2]{0,1:T(2,128)S(1)}, f32[128,2]{0,1:T(2,128)}, u32[]{:S(2)}) copy-start(f32[128,2]{0,1:T(2,128)} %param.20) | copy-start | bytes 3076
  90.8 52.6 %copy-start.10 = (bf16[256,1024]{1,0:T(8,128)(2,1)S(1)}, bf16[256,1024]{1,0:T(8,128)(2,1)}, u32[]{:S(2)}) copy-start(bf16[256,1024]{1,0:T(8,128)(2,1)} %copy-done.9) | copy-start | bytes 1572868
  90.8 14.3 %collective-permute-start.6 = (bf16[128,1024]{1,0:T(8,128)(2,1)}, bf16[128,1024]{1,0:T(8,128)(2,1)S(1)}, u32[]{:S(2)}, u32[]{:S(2)}) collective-permute-start(bf16[128,1024]{1,0:T(8,128)(2,1)} %get-tuple-element.44), channel_id=1, source_target_pairs={{0,4},{1,5},{2,6},{3,7},{4,0},{5,1},{6,2},{7,3},{8,12},{9,13},{10,... | collective-permute-start | bytes 786440 | tf_op jit(solution)/shard_map/ppermute | solution.py:31
  93.0 23.2 %collective-permute-start.14 = (bf16[1024,256]{1,0:T(8,128)(2,1)}, bf16[1024,256]{1,0:T(8,128)(2,1)S(1)}, u32[]{:S(2)}, u32[]{:S(2)}) collective-permute-start(bf16[1024,256]{1,0:T(8,128)(2,1)} %copy-done.6), channel_id=1, source_target_pairs={{0,1},{1,0},{2,3},{3,2},{4,5},{5,4},{6,7},{7,6},{8,9},{9,8},{10,11... | collective-permute-start | bytes 1572872 | tf_op jit(solution)/shard_map/ppermute | solution.py:31
  105.1 7.7 %collective-permute-start.2 = (bf16[128,1024]{1,0:T(8,128)(2,1)}, bf16[128,1024]{1,0:T(8,128)(2,1)S(1)}, u32[]{:S(2)}, u32[]{:S(2)}) collective-permute-start(bf16[128,1024]{1,0:T(8,128)(2,1)} %get-tuple-element.39), channel_id=1, source_target_pairs={{0,4},{1,5},{2,6},{3,7},{4,0},{5,1},{6,2},{7,3},{8,12},{9,13},{10,... | collective-permute-start | bytes 786440 | tf_op jit(solution)/shard_map/ppermute | solution.py:31
  105.4 11.3 %collective-permute-start.7 = (bf16[80,1024]{1,0:T(8,128)(2,1)S(1)}, bf16[80,1024]{1,0:T(8,128)(2,1)S(1)}, u32[]{:S(2)}, u32[]{:S(2)}) collective-permute-start(bf16[80,1024]{1,0:T(8,128)(2,1)S(1)} %get-tuple-element.46), channel_id=1, source_target_pairs={{0,8},{8,0},{16,24},{24,16},{1,9},{9,1},{17,25},{25,17},{2,10},{10... | collective-permute-start | bytes 491528 | tf_op jit(solution)/shard_map/ppermute | solution.py:31
  112.8 6.2 %collective-permute-start.8 = (bf16[80,1024]{1,0:T(8,128)(2,1)S(1)}, bf16[80,1024]{1,0:T(8,128)(2,1)S(1)}, u32[]{:S(2)}, u32[]{:S(2)}) collective-permute-start(bf16[80,1024]{1,0:T(8,128)(2,1)S(1)} %get-tuple-element.47), channel_id=1, source_target_pairs={{0,16},{8,24},{16,0},{24,8},{1,17},{9,25},{17,1},{25,9},{2,18},{10... | collective-permute-start | bytes 491528 | tf_op jit(solution)/shard_map/ppermute | solution.py:31
  114.7 6.3 %collective-permute-start.9 = (bf16[80,1024]{1,0:T(8,128)(2,1)S(1)}, bf16[80,1024]{1,0:T(8,128)(2,1)S(1)}, u32[]{:S(2)}, u32[]{:S(2)}) collective-permute-start(bf16[80,1024]{1,0:T(8,128)(2,1)S(1)} %get-tuple-element.48), channel_id=1, source_target_pairs={{0,24},{8,16},{16,8},{24,0},{1,25},{9,17},{17,9},{25,1},{2,26},{10... | collective-permute-start | bytes 491528 | tf_op jit(solution)/shard_map/ppermute | solution.py:31
  116.2 5.6 %collective-permute-start.3 = (bf16[80,1024]{1,0:T(8,128)(2,1)S(1)}, bf16[80,1024]{1,0:T(8,128)(2,1)S(1)}, u32[]{:S(2)}, u32[]{:S(2)}) collective-permute-start(bf16[80,1024]{1,0:T(8,128)(2,1)S(1)} %get-tuple-element.41), channel_id=1, source_target_pairs={{0,8},{8,0},{16,24},{24,16},{1,9},{9,1},{17,25},{25,17},{2,10},{10... | collective-permute-start | bytes 491528 | tf_op jit(solution)/shard_map/ppermute | solution.py:31
  116.7 22.8 %collective-permute-start.26 = (bf16[256,1024]{1,0:T(8,128)(2,1)}, bf16[256,1024]{1,0:T(8,128)(2,1)S(1)}, u32[]{:S(2)}, u32[]{:S(2)}) collective-permute-start(bf16[256,1024]{1,0:T(8,128)(2,1)} %copy-done.11), channel_id=1, source_target_pairs={{0,1},{1,0},{2,3},{3,2},{4,5},{5,4},{6,7},{7,6},{8,9},{9,8},{10,11... | collective-permute-start | bytes 1572872 | tf_op jit(solution)/shard_map/ppermute | solution.py:31
  119.0 22.9 %collective-permute-start.20 = (bf16[256,1024]{1,0:T(8,128)(2,1)}, bf16[256,1024]{1,0:T(8,128)(2,1)S(1)}, u32[]{:S(2)}, u32[]{:S(2)}) collective-permute-start(bf16[256,1024]{1,0:T(8,128)(2,1)} %copy-done.9), channel_id=1, source_target_pairs={{0,1},{1,0},{2,3},{3,2},{4,5},{5,4},{6,7},{7,6},{8,9},{9,8},{10,11... | collective-permute-start | bytes 1572872 | tf_op jit(solution)/shard_map/ppermute | solution.py:31
  121.0 8.2 %collective-permute-start.4 = (bf16[80,1024]{1,0:T(8,128)(2,1)S(1)}, bf16[80,1024]{1,0:T(8,128)(2,1)S(1)}, u32[]{:S(2)}, u32[]{:S(2)}) collective-permute-start(bf16[80,1024]{1,0:T(8,128)(2,1)S(1)} %get-tuple-element.42), channel_id=1, source_target_pairs={{0,16},{8,24},{16,0},{24,8},{1,17},{9,25},{17,1},{25,9},{2,18},{10... | collective-permute-start | bytes 491528 | tf_op jit(solution)/shard_map/ppermute | solution.py:31
  121.8 8.9 %collective-permute-start.5 = (bf16[80,1024]{1,0:T(8,128)(2,1)S(1)}, bf16[80,1024]{1,0:T(8,128)(2,1)S(1)}, u32[]{:S(2)}, u32[]{:S(2)}) collective-permute-start(bf16[80,1024]{1,0:T(8,128)(2,1)S(1)} %get-tuple-element.43), channel_id=1, source_target_pairs={{0,24},{8,16},{16,8},{24,0},{1,25},{9,17},{17,9},{25,1},{2,26},{10... | collective-permute-start | bytes 491528 | tf_op jit(solution)/shard_map/ppermute | solution.py:31
  129.2 17.8 %collective-permute-start.31 = (bf16[80,2048]{1,0:T(8,128)(2,1)}, bf16[80,2048]{1,0:T(8,128)(2,1)S(1)}, u32[]{:S(2)}, u32[]{:S(2)}) collective-permute-start(bf16[80,2048]{1,0:T(8,128)(2,1)} %get-tuple-element.62), channel_id=1, source_target_pairs={{0,8},{8,0},{16,24},{24,16},{1,9},{9,1},{17,25},{25,17},{2,10},{10... | collective-permute-start | bytes 983048 | tf_op jit(solution)/shard_map/ppermute | solution.py:31
  130.7 17.2 %collective-permute-start.32 = (bf16[80,2048]{1,0:T(8,128)(2,1)}, bf16[80,2048]{1,0:T(8,128)(2,1)S(1)}, u32[]{:S(2)}, u32[]{:S(2)}) collective-permute-start(bf16[80,2048]{1,0:T(8,128)(2,1)} %get-tuple-element.63), channel_id=1, source_target_pairs={{0,16},{8,24},{16,0},{24,8},{1,17},{9,25},{17,1},{25,9},{2,18},{10... | collective-permute-start | bytes 983048 | tf_op jit(solution)/shard_map/ppermute | solution.py:31
  132.0 17.9 %collective-permute-start.33 = (bf16[80,2048]{1,0:T(8,128)(2,1)}, bf16[80,2048]{1,0:T(8,128)(2,1)S(1)}, u32[]{:S(2)}, u32[]{:S(2)}) collective-permute-start(bf16[80,2048]{1,0:T(8,128)(2,1)} %get-tuple-element.64), channel_id=1, source_target_pairs={{0,24},{8,16},{16,8},{24,0},{1,25},{9,17},{17,9},{25,1},{2,26},{10... | collective-permute-start | bytes 983048 | tf_op jit(solution)/shard_map/ppermute | solution.py:31
  134.9 17.0 %copy-start.3 = (bf16[1,2048,256]{2,1,0:T(8,128)(2,1)S(1)}, bf16[1,2048,256]{2,1,0:T(8,128)(2,1)}, u32[]{:S(2)}) copy-start(bf16[1,2048,256]{2,1,0:T(8,128)(2,1)} %param.22) | copy-start | bytes 3145732
  134.9 17.0 %copy-start.8 = (bf16[1024,256]{1,0:T(8,128)(2,1)S(1)}, bf16[1024,256]{1,0:T(8,128)(2,1)}, u32[]{:S(2)}) copy-start(bf16[1024,256]{1,0:T(8,128)(2,1)} %copy-done.6) | copy-start | bytes 1572868
  134.9 17.0 %copy-start.14 = (bf16[80,2048]{1,0:T(8,128)(2,1)S(1)}, bf16[80,2048]{1,0:T(8,128)(2,1)}, u32[]{:S(2)}) copy-start(bf16[80,2048]{1,0:T(8,128)(2,1)} %get-tuple-element.61.refs_0_) | copy-start | bytes 983044
  140.4 10.9 %collective-permute-start.27 = (bf16[80,1024]{1,0:T(8,128)(2,1)S(1)}, bf16[80,1024]{1,0:T(8,128)(2,1)S(1)}, u32[]{:S(2)}, u32[]{:S(2)}) collective-permute-start(bf16[80,1024]{1,0:T(8,128)(2,1)S(1)} %get-tuple-element.58), channel_id=1, source_target_pairs={{0,8},{8,0},{16,24},{24,16},{1,9},{9,1},{17,25},{25,17},{2,10},{10... | collective-permute-start | bytes 491528 | tf_op jit(solution)/shard_map/ppermute | solution.py:31
  142.0 4.5 %collective-permute-start = (f32[2,128]{1,0:T(2,128)S(1)}, f32[2,128]{1,0:T(2,128)S(1)}, u32[]{:S(2)}, u32[]{:S(2)}) collective-permute-start(f32[2,128]{1,0:T(2,128)S(1)} %bitcast.28), channel_id=1, source_target_pairs={{0,4},{1,5},{2,6},{3,7},{4,0},{5,1},{6,2},{7,3},{8,12},{9,13},{10,... | collective-permute-start | bytes 3080 | tf_op jit(solution)/shard_map/ppermute | solution.py:31
  146.5 11.5 %collective-permute-start.21 = (bf16[80,1024]{1,0:T(8,128)(2,1)S(1)}, bf16[80,1024]{1,0:T(8,128)(2,1)S(1)}, u32[]{:S(2)}, u32[]{:S(2)}) collective-permute-start(bf16[80,1024]{1,0:T(8,128)(2,1)S(1)} %get-tuple-element.53), channel_id=1, source_target_pairs={{0,8},{8,0},{16,24},{24,16},{1,9},{9,1},{17,25},{25,17},{2,10},{10... | collective-permute-start | bytes 491528 | tf_op jit(solution)/shard_map/ppermute | solution.py:31
  147.0 12.6 %collective-permute-start.22 = (bf16[80,1024]{1,0:T(8,128)(2,1)S(1)}, bf16[80,1024]{1,0:T(8,128)(2,1)S(1)}, u32[]{:S(2)}, u32[]{:S(2)}) collective-permute-start(bf16[80,1024]{1,0:T(8,128)(2,1)S(1)} %get-tuple-element.54), channel_id=1, source_target_pairs={{0,16},{8,24},{16,0},{24,8},{1,17},{9,25},{17,1},{25,9},{2,18},{10... | collective-permute-start | bytes 491528 | tf_op jit(solution)/shard_map/ppermute | solution.py:31
  147.9 13.0 %collective-permute-start.23 = (bf16[80,1024]{1,0:T(8,128)(2,1)S(1)}, bf16[80,1024]{1,0:T(8,128)(2,1)S(1)}, u32[]{:S(2)}, u32[]{:S(2)}) collective-permute-start(bf16[80,1024]{1,0:T(8,128)(2,1)S(1)} %get-tuple-element.55), channel_id=1, source_target_pairs={{0,24},{8,16},{16,8},{24,0},{1,25},{9,17},{17,9},{25,1},{2,26},{10... | collective-permute-start | bytes 491528 | tf_op jit(solution)/shard_map/ppermute | solution.py:31
  150.0 15.4 %collective-permute-start.28 = (bf16[80,1024]{1,0:T(8,128)(2,1)S(1)}, bf16[80,1024]{1,0:T(8,128)(2,1)S(1)}, u32[]{:S(2)}, u32[]{:S(2)}) collective-permute-start(bf16[80,1024]{1,0:T(8,128)(2,1)S(1)} %get-tuple-element.59), channel_id=1, source_target_pairs={{0,16},{8,24},{16,0},{24,8},{1,17},{9,25},{17,1},{25,9},{2,18},{10... | collective-permute-start | bytes 491528 | tf_op jit(solution)/shard_map/ppermute | solution.py:31
  151.3 15.4 %collective-permute-start.29 = (bf16[80,1024]{1,0:T(8,128)(2,1)S(1)}, bf16[80,1024]{1,0:T(8,128)(2,1)S(1)}, u32[]{:S(2)}, u32[]{:S(2)}) collective-permute-start(bf16[80,1024]{1,0:T(8,128)(2,1)S(1)} %get-tuple-element.60), channel_id=1, source_target_pairs={{0,24},{8,16},{16,8},{24,0},{1,25},{9,17},{17,9},{25,1},{2,26},{10... | collective-permute-start | bytes 491528 | tf_op jit(solution)/shard_map/ppermute | solution.py:31
  151.9 34.8 %copy-start.13 = (bf16[128,2048]{1,0:T(8,128)(2,1)S(1)}, bf16[128,2048]{1,0:T(8,128)(2,1)}, u32[]{:S(2)}) copy-start(bf16[128,2048]{1,0:T(8,128)(2,1)} %get-tuple-element.38.stream_ref) | copy-start | bytes 1572868
  157.9 11.2 %collective-permute-start.34 = (bf16[80,2048]{1,0:T(8,128)(2,1)S(1)}, bf16[80,2048]{1,0:T(8,128)(2,1)S(1)}, u32[]{:S(2)}, u32[]{:S(2)}) collective-permute-start(bf16[80,2048]{1,0:T(8,128)(2,1)S(1)} %get-tuple-element.66), channel_id=1, source_target_pairs={{0,8},{8,0},{16,24},{24,16},{1,9},{9,1},{17,25},{25,17},{2,10},{10... | collective-permute-start | bytes 983048 | tf_op jit(solution)/shard_map/ppermute | solution.py:31
  159.5 15.0 %collective-permute-start.35 = (bf16[80,2048]{1,0:T(8,128)(2,1)S(1)}, bf16[80,2048]{1,0:T(8,128)(2,1)S(1)}, u32[]{:S(2)}, u32[]{:S(2)}) collective-permute-start(bf16[80,2048]{1,0:T(8,128)(2,1)S(1)} %get-tuple-element.67), channel_id=1, source_target_pairs={{0,16},{8,24},{16,0},{24,8},{1,17},{9,25},{17,1},{25,9},{2,18},{10... | collective-permute-start | bytes 983048 | tf_op jit(solution)/shard_map/ppermute | solution.py:31
  160.8 13.7 %collective-permute-start.36 = (bf16[80,2048]{1,0:T(8,128)(2,1)S(1)}, bf16[80,2048]{1,0:T(8,128)(2,1)S(1)}, u32[]{:S(2)}, u32[]{:S(2)}) collective-permute-start(bf16[80,2048]{1,0:T(8,128)(2,1)S(1)} %get-tuple-element.68), channel_id=1, source_target_pairs={{0,24},{8,16},{16,8},{24,0},{1,25},{9,17},{17,9},{25,1},{2,26},{10... | collective-permute-start | bytes 983048 | tf_op jit(solution)/shard_map/ppermute | solution.py:31
  165.4 9.1 %collective-permute-start.24 = (bf16[128,1024]{1,0:T(8,128)(2,1)S(1)}, bf16[128,1024]{1,0:T(8,128)(2,1)S(1)}, u32[]{:S(2)}, u32[]{:S(2)}) collective-permute-start(bf16[128,1024]{1,0:T(8,128)(2,1)S(1)} %shard_map.122), channel_id=1, source_target_pairs={{0,4},{1,5},{2,6},{3,7},{4,0},{5,1},{6,2},{7,3},{8,12},{9,13},{10,... | collective-permute-start | bytes 786440 | tf_op jit(solution)/shard_map/ppermute | solution.py:31
  167.4 19.3 %collective-permute-start.30 = (bf16[128,1024]{1,0:T(8,128)(2,1)S(1)}, bf16[128,1024]{1,0:T(8,128)(2,1)S(1)}, u32[]{:S(2)}, u32[]{:S(2)}) collective-permute-start(bf16[128,1024]{1,0:T(8,128)(2,1)S(1)} %shard_map.124), channel_id=1, source_target_pairs={{0,4},{1,5},{2,6},{3,7},{4,0},{5,1},{6,2},{7,3},{8,12},{9,13},{10,... | collective-permute-start | bytes 786440 | tf_op jit(solution)/shard_map/ppermute | solution.py:31
  (8 other events, 17.2 us)

commit v3 on v2

--- a/solution.py
+++ b/solution.py
@@ -36,39 +36,30 @@
     return lax.ppermute(block, axis, [(i - 1, i) for i in devices if i > 0])
 
 
-def first_kernel(k_ref, v_ref, gate_ref, tail_ref, top_ref, sem):
-    top = pltpu.make_async_copy(gate_ref.at[pl.ds(0, top_ref.shape[0])], top_ref, sem)
-    top.start()
+def first_kernel(k_ref, v_ref, tail_ref):
     kv_cols = k_ref.shape[1]
     tail_ref[:, :kv_cols] = k_ref[...]
     tail_ref[:, kv_cols:] = v_ref[...]
-    top.wait()
-
-
-def first_moves(key_heads, value_heads, gate):
+
+
+def first_moves(key_heads, value_heads):
     span, kv_cols = key_heads.shape
     last = pl.BlockSpec((WINDOW, kv_cols), lambda i: (span // WINDOW - 1, 0))
-    stored = pl.BlockSpec(memory_space=pltpu.HBM)
     return pl.pallas_call(
         first_kernel,
         grid=(1,),
-        in_specs=[last, last, stored],
-        out_specs=[pl.BlockSpec(memory_space=pltpu.VMEM)] * 2,
-        out_shape=[
-            jax.ShapeDtypeStruct((WINDOW, 2 * kv_cols), BF16),
-            jax.ShapeDtypeStruct((gate.shape[0] // 2, gate.shape[1]), BF16),
-        ],
-        scratch_shapes=[pltpu.SemaphoreType.DMA],
+        in_specs=[last, last],
+        out_specs=pl.BlockSpec(memory_space=pltpu.VMEM),
+        out_shape=jax.ShapeDtypeStruct((WINDOW, 2 * kv_cols), BF16),
         name="first_moves",
-    )(key_heads, value_heads, gate)
-
-
-def cut_kernel(gate_ref, down_ref, end_ref, left_ref, right_ref, sems):
-    rows, cols = end_ref.shape[0], left_ref.shape[1]
+    )(key_heads, value_heads)
+
+
+def cut_kernel(down_ref, left_ref, right_ref, sems):
+    cols = left_ref.shape[1]
     copies = [
-        pltpu.make_async_copy(gate_ref.at[pl.ds(rows, rows)], end_ref, sems.at[0]),
-        pltpu.make_async_copy(down_ref.at[:, pl.ds(0, cols)], left_ref, sems.at[1]),
-        pltpu.make_async_copy(down_ref.at[:, pl.ds(cols, cols)], right_ref, sems.at[2]),
+        pltpu.make_async_copy(down_ref.at[:, pl.ds(0, cols)], left_ref, sems.at[0]),
+        pltpu.make_async_copy(down_ref.at[:, pl.ds(cols, cols)], right_ref, sems.at[1]),
     ]
     for copy in copies:
         copy.start()
@@ -76,21 +67,16 @@
         copy.wait()
 
 
-def cut_weights(gate, down):
-    stored = pl.BlockSpec(memory_space=pltpu.HBM)
+def cut_weight(down):
     half_down = jax.ShapeDtypeStruct((down.shape[0], down.shape[1] // 2), BF16)
     return pl.pallas_call(
         cut_kernel,
-        in_specs=[stored] * 2,
-        out_specs=[pl.BlockSpec(memory_space=pltpu.VMEM)] * 3,
-        out_shape=[
-            jax.ShapeDtypeStruct((gate.shape[0] // 2, gate.shape[1]), BF16),
-            half_down,
-            half_down,
-        ],
-        scratch_shapes=[pltpu.SemaphoreType.DMA((3,))],
-        name="cut_weights",
-    )(gate, down)
+        in_specs=[pl.BlockSpec(memory_space=pltpu.HBM)],
+        out_specs=[pl.BlockSpec(memory_space=pltpu.VMEM)] * 2,
+        out_shape=[half_down, half_down],
+        scratch_shapes=[pltpu.SemaphoreType.DMA((2,))],
+        name="cut_weight",
+    )(down)
 
 
 def attention_kernel(
@@ -537,11 +523,10 @@
         ]
 
     own_gate, own_up, own_down = gate_weight[0], up_weight[0], down_weight[0]
-    tail, top = first_moves(key_heads, value_heads, own_gate)
-    tail = from_behind(tail, "sp")
-    end, left, right = cut_weights(own_gate, own_down)
+    tail = from_behind(first_moves(key_heads, value_heads), "sp")
+    left, right = cut_weight(own_down)
     gates, ups, downs = [[own_gate]], [[own_up]], [[own_down]]
-    own_chunks = {"gate": [top, end], "up": [own_up], "down": [left, right]}
+    own_chunks = {"gate": [own_gate], "up": [own_up], "down": [left, right]}
     for distance in range(1, half):
         for what, held in (("gate", gates), ("up", ups), ("down", downs)):
             if distance % 2:

time: 189 us -> 191 us (1.011)
  waiting for transfers between devices: 105 us -> 111 us
  local copies, waits for them, and re-layouts: 5.29 us -> 2 us
  starting transfers between devices: 44.7 us -> 42 us
    all_to_all x1, waiting for transfers between devices: 3.18 us -> 50.7 us  [layer(): lax.all_to_all(attended, 'tp', split_axis=0, concat_axis=0, tiled=True)]
    ppermute x36 -> x34, waiting for transfers between devices: 101 us -> 58.5 us  [exchange(): return lax.ppermute(block, axis, [(i, partner(i)) for i in devices])]
    pallas_call x3, Pallas kernels: 3.24 us -> 6.98 us  [down(): pl.pallas_call(body, grid=(1,), in_specs=[whole] + specs, out_specs=[whol...]
    unnamed x36 -> x18, local copies, waits for them, and re-layouts: 4.55 us -> 1.3 us
    ppermute x36 -> x34, starting transfers between devices: 35.8 us -> 34.4 us  [exchange(): return lax.ppermute(block, axis, [(i, partner(i)) for i in devices])]
  transfers between devices with their start and end apart: 38 -> 36, of which waited for: 16 -> 14; matrix products, arithmetic and copies ran while one was open for 0% -> 0% of each run, Pallas kernels for 15% -> 16%
where the time goes in v3:
time: 191 us; the launch traced here: 190 us
  waiting for transfers between devices  111 us (58%)
  starting transfers between devices  42 us (22%)
  Pallas kernels  35 us (18%)
  local copies, waits for them, and re-layouts  2 us (1%)
    ppermute x34, waiting for transfers between devices, exchange(): return lax.ppermute(block, axis, [(i, partner(i)) for i in devices])  58.5 us
    all_to_all x1, waiting for transfers between devices, layer(): lax.all_to_all(attended, 'tp', split_axis=0, concat_axis=0, tiled=True)  50.7 us
    ppermute x34, starting transfers between devices, exchange(): return lax.ppermute(block, axis, [(i, partner(i)) for i in devices])  34.4 us
    pallas_call x2, Pallas kernels, gate_up(): pl.pallas_call(functools.partial(gate_up_kernel, groups=groups, parts=par...  8.73 us
    pallas_call x3, Pallas kernels, down(): pl.pallas_call(body, grid=(1,), in_specs=[whole] + specs, out_specs=[whol...  6.98 us
    pallas_call x1, Pallas kernels, project(): pl.pallas_call(functools.partial(project_kernel, expert_count=expert_coun...  6.76 us
    pallas_call x1, Pallas kernels, attend(): pl.pallas_call(functools.partial(attention_kernel, blocks=span // WINDOW,...  4.19 us
    all_to_all x1, starting transfers between devices, layer(): lax.all_to_all(attended, 'tp', split_axis=0, concat_axis=0, tiled=True)  4.16 us
  transfers between devices with their start and end apart: 36, of which 14 were waited for; matrix products, arithmetic and copies ran while one was open for 0% of the time, Pallas kernels for 16%

profile of v3, /device:TPU:0, one launch (start us, length us, event | category | flops | bytes accessed | tf_op | source)
XLA Modules:
  0.0 190.2 jit_solution(1616827800509567205)
XLA Ops:
  0.0 2.3 %cut_weight.1 = (bf16[256,1024]{1,0:T(8,128)(2,1)}, bf16[256,1024]{1,0:T(8,128)(2,1)}) custom-call(bf16[256,2048]{1,0:T(8,128)(2,1)} %bitcast.14), custom_call_target="tpu_custom_call" | custom-call | tf_op jit(solution)/shard_map/cut_weight/pallas_call | solution.py:72
  2.4 3.1 %collective-permute-start.17 = (bf16[256,1024]{1,0:T(8,128)(2,1)}, bf16[256,1024]{1,0:T(8,128)(2,1)}, u32[]{:S(2)}, u32[]{:S(2)}) collective-permute-start(bf16[256,1024]{1,0:T(8,128)(2,1)} %get-tuple-element.45), channel_id=1, source_target_pairs={{0,2},{1,3},{2,0},{3,1},{4,6},{5,7},{6,4},{7,5},{8,10},{9,11},{10,... | collective-permute-start | bytes 1572872 | tf_op jit(solution)/shard_map/ppermute | solution.py:31
  5.6 1.9 %collective-permute-start.11 = (bf16[2048,256]{1,0:T(8,128)(2,1)}, bf16[2048,256]{1,0:T(8,128)(2,1)}, u32[]{:S(2)}, u32[]{:S(2)}) collective-permute-start(bf16[2048,256]{1,0:T(8,128)(2,1)} %bitcast.19), channel_id=1, source_target_pairs={{0,2},{1,3},{2,0},{3,1},{4,6},{5,7},{6,4},{7,5},{8,10},{9,11},{10,... | collective-permute-start | bytes 3145736 | tf_op jit(solution)/shard_map/ppermute | solution.py:31
  7.5 1.4 first_moves.1
  8.9 3.4 %collective-permute-start.1 = (bf16[128,256]{1,0:T(8,128)(2,1)}, bf16[128,256]{1,0:T(8,128)(2,1)S(1)}, u32[]{:S(2)}, u32[]{:S(2)}) collective-permute-start(bf16[128,256]{1,0:T(8,128)(2,1)} %first_moves.1), channel_id=1, source_target_pairs={{0,8},{8,16},{16,24},{1,9},{9,17},{17,25},{2,10},{10,18},{18,26},{... | collective-permute-start | bytes 196616 | tf_op jit(solution)/shard_map/ppermute | solution.py:36
  12.8 1.7 collective-permute-done.1.tail_ref
  15.1 4.2 %attend.1 = bf16[8,128,256]{2,1,0:T(8,128)(2,1)} custom-call(s32[1]{0:T(128)} %bitcast.info_ref, f32[4]{0:T(128)} %sink_ref.1, bf16[1024,256]{1,0:T(8,128)(2,1)} %q_hbm.1, bf16[1024,128]{1,0:T(8,128)(2,1)} %k_hbm.1, bf16[1024,128]{1,0:T(8,128)(2,1)} %v_hbm.1, bf16[128,256]{1,0:T(8,128)(2,1)} %copy-done.8), custom_call_target="tpu_custom_call" | custom-call | tf_op jit(solution)/shard_map/attend/pallas_call | solution.py:171
  19.3 4.2 %all-to-all-start = ((bf16[8,128,256]{2,1,0:T(8,128)(2,1)}), bf16[8,128,256]{2,1,0:T(8,128)(2,1)}, u32[]{:S(2)}, u32[]{:S(2)}) async-start(bf16[8,128,256]{2,1,0:T(8,128)(2,1)} %attend.1), calls=%async_computation | async-start | bytes 1048576 | tf_op jit(solution)/shard_map/all_to_all | solution.py:540
  24.1 6.4 %collective-permute-done.23.refs_2_.refs_3_ = bf16[256,1024]{1,0:T(8,128)(2,1)} collective-permute-done((bf16[256,1024]{1,0:T(8,128)(2,1)}, bf16[256,1024]{1,0:T(8,128)(2,1)}, u32[]{:S(2)}, u32[]{:S(2)}) %collective-permute-start.23) | collective-permute-done | bytes 524320 | tf_op jit(solution)/shard_map/ppermute | solution.py:31
  30.5 0.7 dynamic-slice_bitcast_fusion.1
  31.4 0.7 copy-done.3
  32.1 50.7 %all-to-all-done.att_ref = bf16[8,128,256]{2,1,0:T(8,128)(2,1)} async-done(((bf16[8,128,256]{2,1,0:T(8,128)(2,1)}), bf16[8,128,256]{2,1,0:T(8,128)(2,1)}, u32[]{:S(2)}, u32[]{:S(2)}) %all-to-all-start) | async-done | bytes 524320 | tf_op jit(solution)/shard_map/all_to_all | solution.py:540
  82.8 6.8 %project.1 = (bf16[128,2048]{1,0:T(8,128)(2,1)}, bf16[128,1024]{1,0:T(8,128)(2,1)}, bf16[128,1024]{1,0:T(8,128)(2,1)}, bf16[80,2048]{1,0:T(8,128)(2,1)}, bf16[80...) custom-call(bf16[8,128,256]{2,1,0:T(8,128)(2,1)} %all-to-all-done.att_ref, ...), custom_call_target="tpu_custom_call" | custom-call | tf_op jit(solution)/shard_map/project/pallas_call | solution.py:298
  89.6 2.2 %collective-permute-start.6 = (bf16[128,1024]{1,0:T(8,128)(2,1)}, bf16[128,1024]{1,0:T(8,128)(2,1)S(1)}, u32[]{:S(2)}, u32[]{:S(2)}) collective-permute-start(bf16[128,1024]{1,0:T(8,128)(2,1)} %get-tuple-element.40), channel_id=1, source_target_pairs={{0,4},{1,5},{2,6},{3,7},{4,0},{5,1},{6,2},{7,3},{8,12},{9,13},{10,... | collective-permute-start | bytes 786440 | tf_op jit(solution)/shard_map/ppermute | solution.py:31
  92.4 10.8 %collective-permute-done.6.far_ref = bf16[128,1024]{1,0:T(8,128)(2,1)S(1)} collective-permute-done((bf16[128,1024]{1,0:T(8,128)(2,1)}, bf16[128,1024]{1,0:T(8,128)(2,1)S(1)}, u32[]{:S(2)}, u32[]{:S(2)}) %collective-permute-start.6) | collective-permute-done | bytes 262176 | tf_op jit(solution)/shard_map/ppermute | solution.py:31
  103.6 1.5 collective-permute-start.7
  105.1 5.6 %collective-permute-done.2.far_ref = bf16[128,1024]{1,0:T(8,128)(2,1)S(1)} collective-permute-done((bf16[128,1024]{1,0:T(8,128)(2,1)}, bf16[128,1024]{1,0:T(8,128)(2,1)S(1)}, u32[]{:S(2)}, u32[]{:S(2)}) %collective-permute-start.2) | collective-permute-done | bytes 262176 | tf_op jit(solution)/shard_map/ppermute | solution.py:31
  110.7 1.5 collective-permute-start.8
  112.2 1.4 collective-permute-start.9
  114.0 2.0 %collective-permute-done.8.refs_6_ = bf16[80,1024]{1,0:T(8,128)(2,1)S(1)} collective-permute-done((bf16[80,1024]{1,0:T(8,128)(2,1)S(1)}, bf16[80,1024]{1,0:T(8,128)(2,1)S(1)}, u32[]{:S(2)}, u32[]{:S(2)}) %collective-permute-start.8) | collective-permute-done | bytes 163872 | tf_op jit(solution)/shard_map/ppermute | solution.py:31
  116.0 1.5 collective-permute-start.3
  117.5 2.5 %collective-permute-done.9.refs_7_ = bf16[80,1024]{1,0:T(8,128)(2,1)S(1)} collective-permute-done((bf16[80,1024]{1,0:T(8,128)(2,1)S(1)}, bf16[80,1024]{1,0:T(8,128)(2,1)S(1)}, u32[]{:S(2)}, u32[]{:S(2)}) %collective-permute-start.9) | collective-permute-done | bytes 163872 | tf_op jit(solution)/shard_map/ppermute | solution.py:31
  120.3 1.1 collective-permute-done.3.refs_1_
  121.4 4.0 %collective-permute-done.4.refs_2_ = bf16[80,1024]{1,0:T(8,128)(2,1)S(1)} collective-permute-done((bf16[80,1024]{1,0:T(8,128)(2,1)S(1)}, bf16[80,1024]{1,0:T(8,128)(2,1)S(1)}, u32[]{:S(2)}, u32[]{:S(2)}) %collective-permute-start.4) | collective-permute-done | bytes 163872 | tf_op jit(solution)/shard_map/ppermute | solution.py:31
  125.4 1.2 collective-permute-start.5
  126.6 5.6 %collective-permute-done.5.refs_3_ = bf16[80,1024]{1,0:T(8,128)(2,1)S(1)} collective-permute-done((bf16[80,1024]{1,0:T(8,128)(2,1)S(1)}, bf16[80,1024]{1,0:T(8,128)(2,1)S(1)}, u32[]{:S(2)}, u32[]{:S(2)}) %collective-permute-start.5) | collective-permute-done | bytes 163872 | tf_op jit(solution)/shard_map/ppermute | solution.py:31
  132.2 1.2 collective-permute-start.29
  133.4 0.6 collective-permute-start.30
  134.0 1.6 collective-permute-start.31
  135.7 4.3 %shard_map.120.hidden_ref = bf16[320,1024]{1,0:T(8,128)(2,1)S(1)} custom-call(bf16[80,1024]{1,0:T(8,128)(2,1)S(1)} %get-tuple-element.36.refs_0_, bf16[80,1024]{1,0:T(8,128)(2,1)S(1)} %collective-permute-done.3.refs_1_, bf16[80,1024]{1,0:T(8,128)(2,1)S(1)} %collective-permute-done.4.refs_2_, bf16[80,1024]{1,0:T(8,128)(2,1)S(1)} %collective-permute-done.5.refs_3_, ...), custom_call_target="tpu_custom_call" | custom-call | tf_op jit(solution)/shard_map/pallas_call | solution.py:379
  140.0 2.1 %shard_map.123 = (bf16[80,1024]{1,0:T(8,128)(2,1)S(1)}, bf16[80,1024]{1,0:T(8,128)(2,1)S(1)}, bf16[80,1024]{1,0:T(8,128)(2,1)S(1)}, bf16[80,1024]{1,0:T(8,128)(2,1)S(1)}) custom-call(bf16[320,1024]{1,0:T(8,128)(2,1)S(1)} %shard_map.120.hidden_ref, bf16[256,2048]{1,0:T(8,128)(2,1)S(1)} %bitcast.16, bf16[256,2048]{1,0:T(8,128)(2,1)S(1)} %collective-permute-done.16.refs_1_, ...), custom_call_target="tpu_custom_call" | custom-call | tf_op jit(solution)/shard_map/pallas_call | solution.py:446
  142.1 1.3 collective-permute-start.25
  143.5 2.0 %shard_map.121 = (bf16[80,1024]{1,0:T(8,128)(2,1)S(1)}, bf16[80,1024]{1,0:T(8,128)(2,1)S(1)}, bf16[80,1024]{1,0:T(8,128)(2,1)S(1)}, bf16[80,1024]{1,0:T(8,128)(2,1)S(1)}) custom-call(bf16[320,1024]{1,0:T(8,128)(2,1)S(1)} %shard_map.120.hidden_ref, bf16[256,2048]{1,0:T(8,128)(2,1)S(1)} %bitcast.17, bf16[256,2048]{1,0:T(8,128)(2,1)S(1)} %collective-permute-done.16.refs_1_, ...), custom_call_target="tpu_custom_call" | custom-call | tf_op jit(solution)/shard_map/pallas_call | solution.py:446
  145.4 2.5 %collective-permute-done.refs_1_ = f32[2,128]{1,0:T(2,128)S(1)} collective-permute-done((f32[2,128]{1,0:T(2,128)S(1)}, f32[2,128]{1,0:T(2,128)S(1)}, u32[]{:S(2)}, u32[]{:S(2)}) %collective-permute-start) | collective-permute-done | bytes 1056 | tf_op jit(solution)/shard_map/ppermute | solution.py:31
  147.9 0.8 collective-permute-start.19
  148.8 2.6 %collective-permute-start.21 = (bf16[80,1024]{1,0:T(8,128)(2,1)S(1)}, bf16[80,1024]{1,0:T(8,128)(2,1)S(1)}, u32[]{:S(2)}, u32[]{:S(2)}) collective-permute-start(bf16[80,1024]{1,0:T(8,128)(2,1)S(1)} %get-tuple-element.49), channel_id=1, source_target_pairs={{0,24},{8,16},{16,8},{24,0},{1,25},{9,17},{17,9},{25,1},{2,26},{10... | collective-permute-start | bytes 491528 | tf_op jit(solution)/shard_map/ppermute | solution.py:31
  151.4 0.6 collective-permute-start.26
  152.3 2.5 %collective-permute-start.27 = (bf16[80,1024]{1,0:T(8,128)(2,1)S(1)}, bf16[80,1024]{1,0:T(8,128)(2,1)S(1)}, u32[]{:S(2)}, u32[]{:S(2)}) collective-permute-start(bf16[80,1024]{1,0:T(8,128)(2,1)S(1)} %get-tuple-element.54), channel_id=1, source_target_pairs={{0,24},{8,16},{16,8},{24,0},{1,25},{9,17},{17,9},{25,1},{2,26},{10... | collective-permute-start | bytes 491528 | tf_op jit(solution)/shard_map/ppermute | solution.py:31
  154.8 4.4 %shard_map.125.hidden_ref = bf16[320,1024]{1,0:T(8,128)(2,1)S(1)} custom-call(bf16[80,2048]{1,0:T(8,128)(2,1)S(1)} %copy-done.6, bf16[80,2048]{1,0:T(8,128)(2,1)S(1)} %collective-permute-done.29.refs_1_, bf16[80,2048]{1,0:T(8,128)(2,1)S(1)} %collective-permute-done.30.refs_2_, bf16[80,2048]{1,0:T(8,128)(2,1)S(1)} %collective-permute-done.31.refs_3_, ...), custom_call_target="tpu_custom_call" | custom-call | tf_op jit(solution)/shard_map/pallas_call | solution.py:379
  159.2 2.9 %shard_map.126 = (bf16[80,2048]{1,0:T(8,128)(2,1)S(1)}, bf16[80,2048]{1,0:T(8,128)(2,1)S(1)}, bf16[80,2048]{1,0:T(8,128)(2,1)S(1)}, bf16[80,2048]{1,0:T(8,128)(2,1)S(1)}) custom-call(bf16[320,1024]{1,0:T(8,128)(2,1)S(1)} %shard_map.125.hidden_ref, bf16[256,2048]{1,0:T(8,128)(2,1)S(1)} %bitcast.18, bf16[256,2048]{1,0:T(8,128)(2,1)S(1)} %collective-permute-done.16.refs_1_, ...), custom_call_target="tpu_custom_call" | custom-call | tf_op jit(solution)/shard_map/pallas_call | solution.py:446
  162.3 1.4 collective-permute-start.33
  163.7 2.0 %collective-permute-start.34 = (bf16[80,2048]{1,0:T(8,128)(2,1)S(1)}, bf16[80,2048]{1,0:T(8,128)(2,1)S(1)}, u32[]{:S(2)}, u32[]{:S(2)}) collective-permute-start(bf16[80,2048]{1,0:T(8,128)(2,1)S(1)} %get-tuple-element.62), channel_id=1, source_target_pairs={{0,24},{8,16},{16,8},{24,0},{1,25},{9,17},{17,9},{25,1},{2,26},{10... | collective-permute-start | bytes 983048 | tf_op jit(solution)/shard_map/ppermute | solution.py:31
  166.1 0.7 shard_map.122
  166.8 0.7 shard_map.124
  167.5 3.0 %collective-permute-start.28 = (bf16[128,1024]{1,0:T(8,128)(2,1)S(1)}, bf16[128,1024]{1,0:T(8,128)(2,1)S(1)}, u32[]{:S(2)}, u32[]{:S(2)}) collective-permute-start(bf16[128,1024]{1,0:T(8,128)(2,1)S(1)} %shard_map.124), channel_id=1, source_target_pairs={{0,4},{1,5},{2,6},{3,7},{4,0},{5,1},{6,2},{7,3},{8,12},{9,13},{10,... | collective-permute-start | bytes 786440 | tf_op jit(solution)/shard_map/ppermute | solution.py:31
  170.5 4.7 %collective-permute-done.33.refs_4_ = bf16[80,2048]{1,0:T(8,128)(2,1)S(1)} collective-permute-done((bf16[80,2048]{1,0:T(8,128)(2,1)S(1)}, bf16[80,2048]{1,0:T(8,128)(2,1)S(1)}, u32[]{:S(2)}, u32[]{:S(2)}) %collective-permute-start.33) | collective-permute-done | bytes 327712 | tf_op jit(solution)/shard_map/ppermute | solution.py:31
  175.2 13.0 %collective-permute-done.28.refs_1_ = bf16[128,1024]{1,0:T(8,128)(2,1)S(1)} collective-permute-done((bf16[128,1024]{1,0:T(8,128)(2,1)S(1)}, bf16[128,1024]{1,0:T(8,128)(2,1)S(1)}, u32[]{:S(2)}, u32[]{:S(2)}) %collective-permute-start.28) | collective-permute-done | bytes 262176 | tf_op jit(solution)/shard_map/ppermute | solution.py:31
  188.1 2.1 %shard_map.127 = bf16[128,2048]{1,0:T(8,128)(2,1)} custom-call(bf16[2,4,2,128,128]{4,3,2,1,0:T(8,128)(2,1)S(1)} %shard_map.118.spread_ref, bf16[128,2048]{1,0:T(8,128)(2,1)S(1)} %copy-done.5, bf16[128,1024]{1,0:T(8,128)(2,1)S(1)} %collective-permute-done.22.refs_0_, bf16[128,1024]{1,0:T(8,128)(2,1)S(1)} %collective-permute-done.28.refs_1_, ...), custom_call_target="tpu_custom_call" | custom-call | tf_op jit(solution)/shard_map/pallas_call | solution.py:484
  (60 shorter events, 4.5 us)
Async XLA Ops:
  0.0 92.3 %copy-start = (bf16[1,256,2048]{2,1,0:T(8,128)(2,1)S(1)}, bf16[1,256,2048]{2,1,0:T(8,128)(2,1)}, u32[]{:S(2)}) copy-start(bf16[1,256,2048]{2,1,0:T(8,128)(2,1)} %param.23) | copy-start | bytes 3145732
  0.0 135.7 %copy-start.1 = (bf16[1,2048,256]{2,1,0:T(8,128)(2,1)S(1)}, bf16[1,2048,256]{2,1,0:T(8,128)(2,1)}, u32[]{:S(2)}) copy-start(bf16[1,2048,256]{2,1,0:T(8,128)(2,1)} %param.21) | copy-start | bytes 3145732
  0.0 135.7 %copy-start.2 = (bf16[1,2048,256]{2,1,0:T(8,128)(2,1)S(1)}, bf16[1,2048,256]{2,1,0:T(8,128)(2,1)}, u32[]{:S(2)}) copy-start(bf16[1,2048,256]{2,1,0:T(8,128)(2,1)} %param.22) | copy-start | bytes 3145732
  2.4 21.5 %collective-permute-start.17 = (bf16[256,1024]{1,0:T(8,128)(2,1)}, bf16[256,1024]{1,0:T(8,128)(2,1)}, u32[]{:S(2)}, u32[]{:S(2)}) collective-permute-start(bf16[256,1024]{1,0:T(8,128)(2,1)} %get-tuple-element.45), channel_id=1, source_target_pairs={{0,2},{1,3},{2,0},{3,1},{4,6},{5,7},{6,4},{7,5},{8,10},{9,11},{10,... | collective-permute-start | bytes 1572872 | tf_op jit(solution)/shard_map/ppermute | solution.py:31
  5.5 25.0 %collective-permute-start.23 = (bf16[256,1024]{1,0:T(8,128)(2,1)}, bf16[256,1024]{1,0:T(8,128)(2,1)}, u32[]{:S(2)}, u32[]{:S(2)}) collective-permute-start(bf16[256,1024]{1,0:T(8,128)(2,1)} %get-tuple-element.50), channel_id=1, source_target_pairs={{0,2},{1,3},{2,0},{3,1},{4,6},{5,7},{6,4},{7,5},{8,10},{9,11},{10,... | collective-permute-start | bytes 1572872 | tf_op jit(solution)/shard_map/ppermute | solution.py:31
  5.6 86.3 %collective-permute-start.11 = (bf16[2048,256]{1,0:T(8,128)(2,1)}, bf16[2048,256]{1,0:T(8,128)(2,1)}, u32[]{:S(2)}, u32[]{:S(2)}) collective-permute-start(bf16[2048,256]{1,0:T(8,128)(2,1)} %bitcast.19), channel_id=1, source_target_pairs={{0,2},{1,3},{2,0},{3,1},{4,6},{5,7},{6,4},{7,5},{8,10},{9,11},{10,... | collective-permute-start | bytes 3145736 | tf_op jit(solution)/shard_map/ppermute | solution.py:31
  8.9 5.6 %collective-permute-start.1 = (bf16[128,256]{1,0:T(8,128)(2,1)}, bf16[128,256]{1,0:T(8,128)(2,1)S(1)}, u32[]{:S(2)}, u32[]{:S(2)}) collective-permute-start(bf16[128,256]{1,0:T(8,128)(2,1)} %first_moves.1), channel_id=1, source_target_pairs={{0,8},{8,16},{16,24},{1,9},{9,17},{17,25},{2,10},{10,18},{18,26},{... | collective-permute-start | bytes 196616 | tf_op jit(solution)/shard_map/ppermute | solution.py:36
  12.3 79.5 %collective-permute-start.14 = (bf16[2048,256]{1,0:T(8,128)(2,1)}, bf16[2048,256]{1,0:T(8,128)(2,1)}, u32[]{:S(2)}, u32[]{:S(2)}) collective-permute-start(bf16[2048,256]{1,0:T(8,128)(2,1)} %bitcast.23), channel_id=1, source_target_pairs={{0,2},{1,3},{2,0},{3,1},{4,6},{5,7},{6,4},{7,5},{8,10},{9,11},{10,... | collective-permute-start | bytes 3145736 | tf_op jit(solution)/shard_map/ppermute | solution.py:31
  14.5 0.6 copy-start.8
  19.3 63.5 %all-to-all-start = ((bf16[8,128,256]{2,1,0:T(8,128)(2,1)}), bf16[8,128,256]{2,1,0:T(8,128)(2,1)}, u32[]{:S(2)}, u32[]{:S(2)}) async-start(bf16[8,128,256]{2,1,0:T(8,128)(2,1)} %attend.1), calls=%async_computation | async-start | bytes 1048576 | tf_op jit(solution)/shard_map/all_to_all | solution.py:540
  23.5 68.8 %collective-permute-start.10 = (bf16[2048,256]{1,0:T(8,128)(2,1)}, bf16[2048,256]{1,0:T(8,128)(2,1)}, u32[]{:S(2)}, u32[]{:S(2)}) collective-permute-start(bf16[2048,256]{1,0:T(8,128)(2,1)} %bitcast.20), channel_id=1, source_target_pairs={{0,1},{1,0},{2,3},{3,2},{4,5},{5,4},{6,7},{7,6},{8,9},{9,8},{10,11... | collective-permute-start | bytes 3145736 | tf_op jit(solution)/shard_map/ppermute | solution.py:31
  23.9 79.7 %collective-permute-start.13 = (bf16[2048,256]{1,0:T(8,128)(2,1)}, bf16[2048,256]{1,0:T(8,128)(2,1)}, u32[]{:S(2)}, u32[]{:S(2)}) collective-permute-start(bf16[2048,256]{1,0:T(8,128)(2,1)} %bitcast.24), channel_id=1, source_target_pairs={{0,1},{1,0},{2,3},{3,2},{4,5},{5,4},{6,7},{7,6},{8,9},{9,8},{10,11... | collective-permute-start | bytes 3145736 | tf_op jit(solution)/shard_map/ppermute | solution.py:31
  30.5 59.1 %collective-permute-start.24 = (bf16[256,1024]{1,0:T(8,128)(2,1)}, bf16[256,1024]{1,0:T(8,128)(2,1)}, u32[]{:S(2)}, u32[]{:S(2)}) collective-permute-start(bf16[256,1024]{1,0:T(8,128)(2,1)} %collective-permute-done.23.refs_2_.refs_3_), channel_id=1, source_target_pairs={{0,1},{1,0},{2,3},{3,2},{4,5},{5,4},{6,7},{7,6},{8,9},{9,8},{10,11... | collective-permute-start | bytes 1572872 | tf_op jit(solution)/shard_map/ppermute | solution.py:31
  31.4 0.7 copy-start.3
  82.8 20.4 %copy-start.4 = (bf16[2,4,80,128]{3,2,1,0:T(8,128)(2,1)S(1)}, bf16[2,4,80,128]{3,2,1,0:T(8,128)(2,1)}, u32[]{:S(2)}) copy-start(bf16[2,4,80,128]{3,2,1,0:T(8,128)(2,1)} %copy-done.3) | copy-start | bytes 491524
  89.6 53.9 %copy-start.7 = (f32[128,2]{0,1:T(2,128)S(1)}, f32[128,2]{0,1:T(2,128)}, u32[]{:S(2)}) copy-start(f32[128,2]{0,1:T(2,128)} %param.20) | copy-start | bytes 3076
  89.6 13.6 %collective-permute-start.6 = (bf16[128,1024]{1,0:T(8,128)(2,1)}, bf16[128,1024]{1,0:T(8,128)(2,1)S(1)}, u32[]{:S(2)}, u32[]{:S(2)}) collective-permute-start(bf16[128,1024]{1,0:T(8,128)(2,1)} %get-tuple-element.40), channel_id=1, source_target_pairs={{0,4},{1,5},{2,6},{3,7},{4,0},{5,1},{6,2},{7,3},{8,12},{9,13},{10,... | collective-permute-start | bytes 786440 | tf_op jit(solution)/shard_map/ppermute | solution.py:31
  91.8 41.6 %collective-permute-start.12 = (bf16[2048,256]{1,0:T(8,128)(2,1)}, bf16[2048,256]{1,0:T(8,128)(2,1)S(1)}, u32[]{:S(2)}, u32[]{:S(2)}) collective-permute-start(bf16[2048,256]{1,0:T(8,128)(2,1)} %collective-permute-done.11.refs_10_.refs_6_), channel_id=1, source_target_pairs={{0,1},{1,0},{2,3},{3,2},{4,5},{5,4},{6,7},{7,6},{8,9},{9,8},{10,11... | collective-permute-start | bytes 3145736 | tf_op jit(solution)/shard_map/ppermute | solution.py:31
  91.8 42.2 %collective-permute-start.15 = (bf16[2048,256]{1,0:T(8,128)(2,1)}, bf16[2048,256]{1,0:T(8,128)(2,1)S(1)}, u32[]{:S(2)}, u32[]{:S(2)}) collective-permute-start(bf16[2048,256]{1,0:T(8,128)(2,1)} %collective-permute-done.14.refs_14_.refs_10_), channel_id=1, source_target_pairs={{0,1},{1,0},{2,3},{3,2},{4,5},{5,4},{6,7},{7,6},{8,9},{9,8},{10,11... | collective-permute-start | bytes 3145736 | tf_op jit(solution)/shard_map/ppermute | solution.py:31
  92.3 47.7 %collective-permute-start.16 = (bf16[256,2048]{1,0:T(8,128)(2,1)S(1)}, bf16[256,2048]{1,0:T(8,128)(2,1)S(1)}, u32[]{:S(2)}, u32[]{:S(2)}) collective-permute-start(bf16[256,2048]{1,0:T(8,128)(2,1)S(1)} %bitcast.15), channel_id=1, source_target_pairs={{0,1},{1,0},{2,3},{3,2},{4,5},{5,4},{6,7},{7,6},{8,9},{9,8},{10,11... | collective-permute-start | bytes 3145736 | tf_op jit(solution)/shard_map/ppermute | solution.py:31
  103.2 7.5 %collective-permute-start.2 = (bf16[128,1024]{1,0:T(8,128)(2,1)}, bf16[128,1024]{1,0:T(8,128)(2,1)S(1)}, u32[]{:S(2)}, u32[]{:S(2)}) collective-permute-start(bf16[128,1024]{1,0:T(8,128)(2,1)} %get-tuple-element.35), channel_id=1, source_target_pairs={{0,4},{1,5},{2,6},{3,7},{4,0},{5,1},{6,2},{7,3},{8,12},{9,13},{10,... | collective-permute-start | bytes 786440 | tf_op jit(solution)/shard_map/ppermute | solution.py:31
  103.6 8.7 %collective-permute-start.7 = (bf16[80,1024]{1,0:T(8,128)(2,1)S(1)}, bf16[80,1024]{1,0:T(8,128)(2,1)S(1)}, u32[]{:S(2)}, u32[]{:S(2)}) collective-permute-start(bf16[80,1024]{1,0:T(8,128)(2,1)S(1)} %get-tuple-element.42), channel_id=1, source_target_pairs={{0,8},{8,0},{16,24},{24,16},{1,9},{9,1},{17,25},{25,17},{2,10},{10... | collective-permute-start | bytes 491528 | tf_op jit(solution)/shard_map/ppermute | solution.py:31
  110.7 5.3 %collective-permute-start.8 = (bf16[80,1024]{1,0:T(8,128)(2,1)S(1)}, bf16[80,1024]{1,0:T(8,128)(2,1)S(1)}, u32[]{:S(2)}, u32[]{:S(2)}) collective-permute-start(bf16[80,1024]{1,0:T(8,128)(2,1)S(1)} %get-tuple-element.43), channel_id=1, source_target_pairs={{0,16},{8,24},{16,0},{24,8},{1,17},{9,25},{17,1},{25,9},{2,18},{10... | collective-permute-start | bytes 491528 | tf_op jit(solution)/shard_map/ppermute | solution.py:31
  112.2 7.8 %collective-permute-start.9 = (bf16[80,1024]{1,0:T(8,128)(2,1)S(1)}, bf16[80,1024]{1,0:T(8,128)(2,1)S(1)}, u32[]{:S(2)}, u32[]{:S(2)}) collective-permute-start(bf16[80,1024]{1,0:T(8,128)(2,1)S(1)} %get-tuple-element.44), channel_id=1, source_target_pairs={{0,24},{8,16},{16,8},{24,0},{1,25},{9,17},{17,9},{25,1},{2,26},{10... | collective-permute-start | bytes 491528 | tf_op jit(solution)/shard_map/ppermute | solution.py:31
  116.0 5.3 %collective-permute-start.3 = (bf16[80,1024]{1,0:T(8,128)(2,1)S(1)}, bf16[80,1024]{1,0:T(8,128)(2,1)S(1)}, u32[]{:S(2)}, u32[]{:S(2)}) collective-permute-start(bf16[80,1024]{1,0:T(8,128)(2,1)S(1)} %get-tuple-element.37), channel_id=1, source_target_pairs={{0,8},{8,0},{16,24},{24,16},{1,9},{9,1},{17,25},{25,17},{2,10},{10... | collective-permute-start | bytes 491528 | tf_op jit(solution)/shard_map/ppermute | solution.py:31
  120.1 5.3 %collective-permute-start.4 = (bf16[80,1024]{1,0:T(8,128)(2,1)S(1)}, bf16[80,1024]{1,0:T(8,128)(2,1)S(1)}, u32[]{:S(2)}, u32[]{:S(2)}) collective-permute-start(bf16[80,1024]{1,0:T(8,128)(2,1)S(1)} %get-tuple-element.38), channel_id=1, source_target_pairs={{0,16},{8,24},{16,0},{24,8},{1,17},{9,25},{17,1},{25,9},{2,18},{10... | collective-permute-start | bytes 491528 | tf_op jit(solution)/shard_map/ppermute | solution.py:31
  121.4 22.1 %collective-permute-start.18 = (bf16[256,1024]{1,0:T(8,128)(2,1)}, bf16[256,1024]{1,0:T(8,128)(2,1)S(1)}, u32[]{:S(2)}, u32[]{:S(2)}) collective-permute-start(bf16[256,1024]{1,0:T(8,128)(2,1)} %collective-permute-done.17.refs_2_), channel_id=1, source_target_pairs={{0,1},{1,0},{2,3},{3,2},{4,5},{5,4},{6,7},{7,6},{8,9},{9,8},{10,11... | collective-permute-start | bytes 1572872 | tf_op jit(solution)/shard_map/ppermute | solution.py:31
  125.4 6.8 %collective-permute-start.5 = (bf16[80,1024]{1,0:T(8,128)(2,1)S(1)}, bf16[80,1024]{1,0:T(8,128)(2,1)S(1)}, u32[]{:S(2)}, u32[]{:S(2)}) collective-permute-start(bf16[80,1024]{1,0:T(8,128)(2,1)S(1)} %get-tuple-element.39), channel_id=1, source_target_pairs={{0,24},{8,16},{16,8},{24,0},{1,25},{9,17},{17,9},{25,1},{2,26},{10... | collective-permute-start | bytes 491528 | tf_op jit(solution)/shard_map/ppermute | solution.py:31
  132.2 16.6 %collective-permute-start.29 = (bf16[80,2048]{1,0:T(8,128)(2,1)}, bf16[80,2048]{1,0:T(8,128)(2,1)S(1)}, u32[]{:S(2)}, u32[]{:S(2)}) collective-permute-start(bf16[80,2048]{1,0:T(8,128)(2,1)} %get-tuple-element.56), channel_id=1, source_target_pairs={{0,8},{8,0},{16,24},{24,16},{1,9},{9,1},{17,25},{25,17},{2,10},{10... | collective-permute-start | bytes 983048 | tf_op jit(solution)/shard_map/ppermute | solution.py:31
  133.4 15.4 %collective-permute-start.30 = (bf16[80,2048]{1,0:T(8,128)(2,1)}, bf16[80,2048]{1,0:T(8,128)(2,1)S(1)}, u32[]{:S(2)}, u32[]{:S(2)}) collective-permute-start(bf16[80,2048]{1,0:T(8,128)(2,1)} %get-tuple-element.57), channel_id=1, source_target_pairs={{0,16},{8,24},{16,0},{24,8},{1,17},{9,25},{17,1},{25,9},{2,18},{10... | collective-permute-start | bytes 983048 | tf_op jit(solution)/shard_map/ppermute | solution.py:31
  134.0 17.4 %collective-permute-start.31 = (bf16[80,2048]{1,0:T(8,128)(2,1)}, bf16[80,2048]{1,0:T(8,128)(2,1)S(1)}, u32[]{:S(2)}, u32[]{:S(2)}) collective-permute-start(bf16[80,2048]{1,0:T(8,128)(2,1)} %get-tuple-element.58), channel_id=1, source_target_pairs={{0,24},{8,16},{16,8},{24,0},{1,25},{9,17},{17,9},{25,1},{2,26},{10... | collective-permute-start | bytes 983048 | tf_op jit(solution)/shard_map/ppermute | solution.py:31
  135.7 19.2 %copy-start.6 = (bf16[80,2048]{1,0:T(8,128)(2,1)S(1)}, bf16[80,2048]{1,0:T(8,128)(2,1)}, u32[]{:S(2)}) copy-start(bf16[80,2048]{1,0:T(8,128)(2,1)} %get-tuple-element.55.refs_0_) | copy-start | bytes 983044
  142.1 10.2 %collective-permute-start.25 = (bf16[80,1024]{1,0:T(8,128)(2,1)S(1)}, bf16[80,1024]{1,0:T(8,128)(2,1)S(1)}, u32[]{:S(2)}, u32[]{:S(2)}) collective-permute-start(bf16[80,1024]{1,0:T(8,128)(2,1)S(1)} %get-tuple-element.52), channel_id=1, source_target_pairs={{0,8},{8,0},{16,24},{24,16},{1,9},{9,1},{17,25},{25,17},{2,10},{10... | collective-permute-start | bytes 491528 | tf_op jit(solution)/shard_map/ppermute | solution.py:31
  143.5 4.5 %collective-permute-start = (f32[2,128]{1,0:T(2,128)S(1)}, f32[2,128]{1,0:T(2,128)S(1)}, u32[]{:S(2)}, u32[]{:S(2)}) collective-permute-start(f32[2,128]{1,0:T(2,128)S(1)} %bitcast.27), channel_id=1, source_target_pairs={{0,4},{1,5},{2,6},{3,7},{4,0},{5,1},{6,2},{7,3},{8,12},{9,13},{10,... | collective-permute-start | bytes 3080 | tf_op jit(solution)/shard_map/ppermute | solution.py:31
  147.9 14.2 %collective-permute-start.19 = (bf16[80,1024]{1,0:T(8,128)(2,1)S(1)}, bf16[80,1024]{1,0:T(8,128)(2,1)S(1)}, u32[]{:S(2)}, u32[]{:S(2)}) collective-permute-start(bf16[80,1024]{1,0:T(8,128)(2,1)S(1)} %get-tuple-element.47), channel_id=1, source_target_pairs={{0,8},{8,0},{16,24},{24,16},{1,9},{9,1},{17,25},{25,17},{2,10},{10... | collective-permute-start | bytes 491528 | tf_op jit(solution)/shard_map/ppermute | solution.py:31
  148.7 13.6 %collective-permute-start.20 = (bf16[80,1024]{1,0:T(8,128)(2,1)S(1)}, bf16[80,1024]{1,0:T(8,128)(2,1)S(1)}, u32[]{:S(2)}, u32[]{:S(2)}) collective-permute-start(bf16[80,1024]{1,0:T(8,128)(2,1)S(1)} %get-tuple-element.48), channel_id=1, source_target_pairs={{0,16},{8,24},{16,0},{24,8},{1,17},{9,25},{17,1},{25,9},{2,18},{10... | collective-permute-start | bytes 491528 | tf_op jit(solution)/shard_map/ppermute | solution.py:31
  148.8 14.9 %collective-permute-start.21 = (bf16[80,1024]{1,0:T(8,128)(2,1)S(1)}, bf16[80,1024]{1,0:T(8,128)(2,1)S(1)}, u32[]{:S(2)}, u32[]{:S(2)}) collective-permute-start(bf16[80,1024]{1,0:T(8,128)(2,1)S(1)} %get-tuple-element.49), channel_id=1, source_target_pairs={{0,24},{8,16},{16,8},{24,0},{1,25},{9,17},{17,9},{25,1},{2,26},{10... | collective-permute-start | bytes 491528 | tf_op jit(solution)/shard_map/ppermute | solution.py:31
  151.4 15.3 %collective-permute-start.26 = (bf16[80,1024]{1,0:T(8,128)(2,1)S(1)}, bf16[80,1024]{1,0:T(8,128)(2,1)S(1)}, u32[]{:S(2)}, u32[]{:S(2)}) collective-permute-start(bf16[80,1024]{1,0:T(8,128)(2,1)S(1)} %get-tuple-element.53), channel_id=1, source_target_pairs={{0,16},{8,24},{16,0},{24,8},{1,17},{9,25},{17,1},{25,9},{2,18},{10... | collective-permute-start | bytes 491528 | tf_op jit(solution)/shard_map/ppermute | solution.py:31
  152.3 14.5 %collective-permute-start.27 = (bf16[80,1024]{1,0:T(8,128)(2,1)S(1)}, bf16[80,1024]{1,0:T(8,128)(2,1)S(1)}, u32[]{:S(2)}, u32[]{:S(2)}) collective-permute-start(bf16[80,1024]{1,0:T(8,128)(2,1)S(1)} %get-tuple-element.54), channel_id=1, source_target_pairs={{0,24},{8,16},{16,8},{24,0},{1,25},{9,17},{17,9},{25,1},{2,26},{10... | collective-permute-start | bytes 491528 | tf_op jit(solution)/shard_map/ppermute | solution.py:31
  154.8 33.3 %copy-start.5 = (bf16[128,2048]{1,0:T(8,128)(2,1)S(1)}, bf16[128,2048]{1,0:T(8,128)(2,1)}, u32[]{:S(2)}) copy-start(bf16[128,2048]{1,0:T(8,128)(2,1)} %get-tuple-element.34.stream_ref) | copy-start | bytes 1572868
  162.1 8.4 %collective-permute-start.32 = (bf16[80,2048]{1,0:T(8,128)(2,1)S(1)}, bf16[80,2048]{1,0:T(8,128)(2,1)S(1)}, u32[]{:S(2)}, u32[]{:S(2)}) collective-permute-start(bf16[80,2048]{1,0:T(8,128)(2,1)S(1)} %get-tuple-element.60), channel_id=1, source_target_pairs={{0,8},{8,0},{16,24},{24,16},{1,9},{9,1},{17,25},{25,17},{2,10},{10... | collective-permute-start | bytes 983048 | tf_op jit(solution)/shard_map/ppermute | solution.py:31
  162.3 12.9 %collective-permute-start.33 = (bf16[80,2048]{1,0:T(8,128)(2,1)S(1)}, bf16[80,2048]{1,0:T(8,128)(2,1)S(1)}, u32[]{:S(2)}, u32[]{:S(2)}) collective-permute-start(bf16[80,2048]{1,0:T(8,128)(2,1)S(1)} %get-tuple-element.61), channel_id=1, source_target_pairs={{0,16},{8,24},{16,0},{24,8},{1,17},{9,25},{17,1},{25,9},{2,18},{10... | collective-permute-start | bytes 983048 | tf_op jit(solution)/shard_map/ppermute | solution.py:31
  163.7 11.5 %collective-permute-start.34 = (bf16[80,2048]{1,0:T(8,128)(2,1)S(1)}, bf16[80,2048]{1,0:T(8,128)(2,1)S(1)}, u32[]{:S(2)}, u32[]{:S(2)}) collective-permute-start(bf16[80,2048]{1,0:T(8,128)(2,1)S(1)} %get-tuple-element.62), channel_id=1, source_target_pairs={{0,24},{8,16},{16,8},{24,0},{1,25},{9,17},{17,9},{25,1},{2,26},{10... | collective-permute-start | bytes 983048 | tf_op jit(solution)/shard_map/ppermute | solution.py:31
  166.8 8.4 %collective-permute-start.22 = (bf16[128,1024]{1,0:T(8,128)(2,1)S(1)}, bf16[128,1024]{1,0:T(8,128)(2,1)S(1)}, u32[]{:S(2)}, u32[]{:S(2)}) collective-permute-start(bf16[128,1024]{1,0:T(8,128)(2,1)S(1)} %shard_map.122), channel_id=1, source_target_pairs={{0,4},{1,5},{2,6},{3,7},{4,0},{5,1},{6,2},{7,3},{8,12},{9,13},{10,... | collective-permute-start | bytes 786440 | tf_op jit(solution)/shard_map/ppermute | solution.py:31
  167.5 20.6 %collective-permute-start.28 = (bf16[128,1024]{1,0:T(8,128)(2,1)S(1)}, bf16[128,1024]{1,0:T(8,128)(2,1)S(1)}, u32[]{:S(2)}, u32[]{:S(2)}) collective-permute-start(bf16[128,1024]{1,0:T(8,128)(2,1)S(1)} %shard_map.124), channel_id=1, source_target_pairs={{0,4},{1,5},{2,6},{3,7},{4,0},{5,1},{6,2},{7,3},{8,12},{9,13},{10,... | collective-permute-start | bytes 786440 | tf_op jit(solution)/shard_map/ppermute | solution.py:31

commit v4 on v3

--- a/solution.py
+++ b/solution.py
@@ -244,18 +244,9 @@
     )(*operands)
 
 
-def pack(gather_ref, normed, send_refs):
-    for distance, send_ref in enumerate(send_refs):
-        send_ref[...] = jnp.dot(
-            gather_ref[0, distance], normed, preferred_element_type=F32
-        ).astype(BF16)
-
-
-def project_kernel(
-    att_ref, w_hbm, res_ref, gain_ref, gather_ref, stream_ref, *refs, expert_count, parts, tile
-):
-    part_refs, send_refs = refs[:parts], refs[parts:-3]
-    acc_ref, w_ref, sems = refs[-3:]
+def project_kernel(att_ref, w_hbm, res_ref, gain_ref, stream_ref, *refs, parts, tile):
+    part_refs = refs[:parts]
+    acc_ref, w_ref, sems = refs[parts:]
     sources, _, cols = att_ref.shape
     width = stream_ref.shape[1]
     copies = []
@@ -264,7 +255,9 @@
         copies.append(pltpu.make_async_copy(w_hbm.at[:, part], w_ref.at[n], sems.at[n]))
     for copy in copies:
         copy.start()
+    square = None
     for n in range(width // tile):
+        part = slice(n * tile, (n + 1) * tile)
         copies[n].wait()
         total = None
         for k in range(sources):
@@ -272,65 +265,68 @@
                 att_ref[k], w_ref[n, k * cols : (k + 1) * cols, :], preferred_element_type=F32
             )
             total = piece if total is None else total + piece
-        acc_ref[:, n * tile : (n + 1) * tile] = total
-    stream = (res_ref[...].astype(F32) + acc_ref[...]).astype(BF16)
-    stream_ref[...] = stream
-    wide = stream.astype(F32)
-    scale = lax.rsqrt(jnp.mean(wide * wide, axis=-1, keepdims=True) + eps)
-    normed = (wide * scale * gain_ref[...]).astype(BF16)
+        stream = (res_ref[:, part].astype(F32) + total).astype(BF16)
+        stream_ref[:, part] = stream
+        wide = stream.astype(F32)
+        acc_ref[:, part] = wide
+        summed = jnp.sum(wide * wide, axis=-1, keepdims=True)
+        square = summed if square is None else square + summed
+    scale = lax.rsqrt(square / width + eps)
     step = width // parts
     for h in range(parts):
-        part_refs[h][...] = normed[:, h * step : (h + 1) * step]
-    pack(gather_ref, normed, send_refs)
-
-
-def block_of(array, block):
-    zeros = (0,) * (array.ndim - 1)
-    return pl.BlockSpec((1,) + array.shape[1:], lambda i: (block,) + zeros)
-
-
-def project(gathered, out_weight, residual, norm_gain, gather, parts):
+        part = slice(h * step, (h + 1) * step)
+        part_refs[h][...] = (acc_ref[:, part] * scale * gain_ref[:, part]).astype(BF16)
+
+
+def project(gathered, out_weight, residual, norm_gain, parts):
     _, rows, _ = gathered.shape
     width = out_weight.shape[1]
-    _, expert_count, slots, _ = gather.shape
     tile = min(512, width)
     whole = pl.BlockSpec(memory_space=pltpu.VMEM)
     outs = pl.pallas_call(
-        functools.partial(
-            project_kernel, expert_count=expert_count, parts=parts, tile=tile
-        ),
-        grid=(1,),
-        in_specs=[whole, pl.BlockSpec(memory_space=pltpu.HBM), whole, whole, block_of(gather, 0)],
-        out_specs=[whole] * (1 + parts + expert_count),
+        functools.partial(project_kernel, parts=parts, tile=tile),
+        in_specs=[whole, pl.BlockSpec(memory_space=pltpu.HBM), whole, whole],
+        out_specs=[whole] * (1 + parts),
         out_shape=[jax.ShapeDtypeStruct((rows, width), BF16)]
-        + [jax.ShapeDtypeStruct((rows, width // parts), BF16)] * parts
-        + [jax.ShapeDtypeStruct((slots, width), BF16)] * expert_count,
+        + [jax.ShapeDtypeStruct((rows, width // parts), BF16)] * parts,
         scratch_shapes=[
             pltpu.VMEM((rows, width), F32),
             pltpu.VMEM((width // tile, out_weight.shape[0], tile), BF16),
             pltpu.SemaphoreType.DMA((width // tile,)),
         ],
         name="project",
-    )(gathered, out_weight, residual, norm_gain, gather)
-    return outs[0], outs[1 : 1 + parts], outs[1 + parts :]
-
-
-def pack_kernel(gather_ref, far_ref, *send_refs):
-    pack(gather_ref, far_ref[...], send_refs)
-
-
-def pack_far(gather, far):
+    )(gathered, out_weight, residual, norm_gain)
+    return outs[0], outs[1:]
+
+
+def pack_kernel(gather_ref, *refs, parts):
+    part_refs, send_refs = refs[:parts], refs[parts:]
+    step = part_refs[0].shape[1]
+    for distance, send_ref in enumerate(send_refs):
+        for h in range(parts):
+            send_ref[:, h * step : (h + 1) * step] = jnp.dot(
+                gather_ref[0, distance], part_refs[h][...], preferred_element_type=F32
+            ).astype(BF16)
+
+
+def block_of(array, block):
+    zeros = (0,) * (array.ndim - 1)
+    return pl.BlockSpec((1,) + array.shape[1:], lambda i: (block,) + zeros)
+
+
+def pack(gather, block, rows):
     _, expert_count, slots, _ = gather.shape
-    whole = pl.BlockSpec(memory_space=pltpu.VMEM)
-    return pl.pallas_call(
-        pack_kernel,
+    width = sum(part.shape[1] for part in rows)
+    whole = pl.BlockSpec(memory_space=pltpu.VMEM)
+    return pl.pallas_call(
+        functools.partial(pack_kernel, parts=len(rows)),
         grid=(1,),
-        in_specs=[block_of(gather, 1), whole],
+        in_specs=[block_of(gather, block)] + [whole] * len(rows),
         out_specs=[whole] * expert_count,
-        out_shape=[jax.ShapeDtypeStruct((slots, far.shape[1]), BF16)] * expert_count,
-        compiler_params=grant(4),
-        name="pack_far",
-    )(gather, far)
+        out_shape=[jax.ShapeDtypeStruct((slots, width), BF16)] * expert_count,
+        compiler_params=grant(6),
+        name="pack",
+    )(gather, *rows)
 
 
 def gate_up_kernel(*refs, groups, parts, slots, pieces, hid, chunks):
@@ -469,16 +465,31 @@
     refs[-1][...] = unpack(spread_ref, refs[:-1]).astype(BF16)
 
 
-def combine_own_kernel(spread_ref, stream_ref, *refs, parts):
-    far_refs, back_refs, out_ref = refs[:parts], refs[parts:-1], refs[-1]
-    total = unpack(spread_ref, back_refs) + stream_ref[...].astype(F32)
-    step = total.shape[1] // parts
-    for h in range(parts):
+def combine_own_kernel(spread_ref, stream_ref, *refs):
+    refs[-1][...] = unpack(spread_ref, refs[:-1]) + stream_ref[...].astype(F32)
+
+
+def finish_kernel(own_ref, *refs):
+    out_ref = refs[-1]
+    step = refs[0].shape[1]
+    for h, far_ref in enumerate(refs[:-1]):
         cols = slice(h * step, (h + 1) * step)
-        out_ref[:, cols] = (total[:, cols] + far_refs[h][...].astype(F32)).astype(BF16)
-
-
-def combine(kernel, spread, block, extra, backs):
+        out_ref[:, cols] = (own_ref[:, cols] + far_ref[...].astype(F32)).astype(BF16)
+
+
+def finish(own, parts):
+    whole = pl.BlockSpec(memory_space=pltpu.VMEM)
+    return pl.pallas_call(
+        finish_kernel,
+        in_specs=[whole] * (1 + len(parts)),
+        out_specs=whole,
+        out_shape=jax.ShapeDtypeStruct(own.shape, BF16),
+        compiler_params=grant(10),
+        name="finish",
+    )(own, *parts)
+
+
+def combine(kernel, spread, block, extra, backs, dtype):
     rows = spread.shape[3]
     whole = pl.BlockSpec(memory_space=pltpu.VMEM)
     return pl.pallas_call(
@@ -486,7 +497,7 @@
         grid=(1,),
         in_specs=[block_of(spread, block)] + [whole] * (len(extra) + len(backs)),
         out_specs=whole,
-        out_shape=jax.ShapeDtypeStruct((rows, backs[0].shape[1]), BF16),
+        out_shape=jax.ShapeDtypeStruct((rows, backs[0].shape[1]), dtype),
         compiler_params=grant(10),
     )(spread, *extra, *backs)
 
@@ -556,27 +567,24 @@
         slots,
     )
 
-    stream, normed, send_own = project(
-        gathered, out_weight, residual, norm_gain.reshape(1, -1), gather, parts
-    )
+    stream, normed = project(gathered, out_weight, residual, norm_gain.reshape(1, -1), parts)
     rows_far = []
     for h in range(parts):
         far = across(normed[h])
-        rows_far += to_experts(pack_far(gather, far))
-    rows_own = to_experts(send_own)
+        rows_far += to_experts(pack(gather, 1, (far,)))
+    rows_own = to_experts(pack(gather, 0, normed))
     hidden_own = gate_up(rows_own, 1, gates, ups)
     hidden_far = gate_up(rows_far, parts, gates, ups)
     part_far = []
     for h in range(parts):
         backs = down(hidden_far, downs, expert_count, h, parts)
         backs = to_experts(backs)
-        mixed = combine(combine_far_kernel, spread, 1, (), backs)
+        mixed = combine(combine_far_kernel, spread, 1, (), backs, BF16)
         part_far.append(across(mixed))
     backs = down(hidden_own, downs, expert_count, 0, 1)
     backs = to_experts(backs)
-    return combine(
-        functools.partial(combine_own_kernel, parts=parts), spread, 0, (stream, *part_far), backs
-    )
+    own = combine(combine_own_kernel, spread, 0, (stream,), backs, F32)
+    return finish(own, part_far)
 
 
 def parts_of(expert_count):

time: 191 us -> 184 us (0.963)
  waiting for transfers between devices: 111 us -> 95 us
  starting transfers between devices: 42 us -> 49.5 us
    all_to_all x1, waiting for transfers between devices: 50.7 us -> 28.1 us  [layer(): lax.all_to_all(attended, 'tp', split_axis=0, concat_axis=0, tiled=True)]
    ppermute x34, waiting for transfers between devices: 58.5 us -> 66.4 us  [exchange(): return lax.ppermute(block, axis, [(i, partner(i)) for i in devices])]
    ppermute x34, starting transfers between devices: 34.4 us -> 40.9 us  [exchange(): return lax.ppermute(block, axis, [(i, partner(i)) for i in devices])]
    pallas_call x3 -> x5, Pallas kernels: 7.41 us -> 8.24 us  [the longest x1 6.2 us: project(): pl.pallas_call(functools.partial(project_kernel, parts=parts, tile=tile),...]
  transfers between devices with their start and end apart: 36 -> 36, of which waited for: 14 -> 15; matrix products, arithmetic and copies ran while one was open for 0% -> 0% of each run, Pallas kernels for 16% -> 17%
where the time goes in v4:
time: 184 us; the launch traced here: 183 us
  waiting for transfers between devices  95 us (52%)
  starting transfers between devices  49.5 us (27%)
  Pallas kernels  35.2 us (19%)
  local copies, waits for them, and re-layouts  3.23 us (2%)
    ppermute x34, waiting for transfers between devices, exchange(): return lax.ppermute(block, axis, [(i, partner(i)) for i in devices])  66.4 us
    ppermute x34, starting transfers between devices, exchange(): return lax.ppermute(block, axis, [(i, partner(i)) for i in devices])  40.9 us
    all_to_all x1, waiting for transfers between devices, layer(): lax.all_to_all(attended, 'tp', split_axis=0, concat_axis=0, tiled=True)  28.1 us
    pallas_call x2, Pallas kernels, gate_up(): pl.pallas_call(functools.partial(gate_up_kernel, groups=groups, parts=par...  8.88 us
    pallas_call x3, Pallas kernels, down(): pl.pallas_call(body, grid=(1,), in_specs=[whole] + specs, out_specs=[whol...  6.97 us
    pallas_call x1, Pallas kernels, project(): pl.pallas_call(functools.partial(project_kernel, parts=parts, tile=tile),...  6.2 us
    all_to_all x1, starting transfers between devices, layer(): lax.all_to_all(attended, 'tp', split_axis=0, concat_axis=0, tiled=True)  4.89 us
    pallas_call x1, Pallas kernels, attend(): pl.pallas_call(functools.partial(attention_kernel, blocks=span // WINDOW,...  4.19 us
  transfers between devices with their start and end apart: 36, of which 15 were waited for; matrix products, arithmetic and copies ran while one was open for 0% of the time, Pallas kernels for 17%

profile of v4, /device:TPU:0, one launch (start us, length us, event | category | flops | bytes accessed | tf_op | source)
XLA Modules:
  0.0 183.2 jit_solution(153956457932690113)
XLA Ops:
  0.0 2.3 %cut_weight.1 = (bf16[256,1024]{1,0:T(8,128)(2,1)}, bf16[256,1024]{1,0:T(8,128)(2,1)}) custom-call(bf16[256,2048]{1,0:T(8,128)(2,1)} %bitcast.14), custom_call_target="tpu_custom_call" | custom-call | tf_op jit(solution)/shard_map/cut_weight/pallas_call | solution.py:72
  2.4 3.1 %collective-permute-start.12 = (bf16[256,1024]{1,0:T(8,128)(2,1)}, bf16[256,1024]{1,0:T(8,128)(2,1)}, u32[]{:S(2)}, u32[]{:S(2)}) collective-permute-start(bf16[256,1024]{1,0:T(8,128)(2,1)} %get-tuple-element.41), channel_id=1, source_target_pairs={{0,2},{1,3},{2,0},{3,1},{4,6},{5,7},{6,4},{7,5},{8,10},{9,11},{10,... | collective-permute-start | bytes 1572872 | tf_op jit(solution)/shard_map/ppermute | solution.py:31
  5.6 1.4 first_moves.1
  7.0 3.8 %collective-permute-start.1 = (bf16[128,256]{1,0:T(8,128)(2,1)}, bf16[128,256]{1,0:T(8,128)(2,1)S(1)}, u32[]{:S(2)}, u32[]{:S(2)}) collective-permute-start(bf16[128,256]{1,0:T(8,128)(2,1)} %first_moves.1), channel_id=1, source_target_pairs={{0,8},{8,16},{16,24},{1,9},{9,17},{17,25},{2,10},{10,18},{18,26},{... | collective-permute-start | bytes 196616 | tf_op jit(solution)/shard_map/ppermute | solution.py:36
  10.7 1.6 collective-permute-start.6
  13.6 4.2 %attend.1 = bf16[8,128,256]{2,1,0:T(8,128)(2,1)} custom-call(s32[1]{0:T(128)} %bitcast.info_ref, f32[4]{0:T(128)} %sink_ref.1, bf16[1024,256]{1,0:T(8,128)(2,1)} %q_hbm.1, bf16[1024,128]{1,0:T(8,128)(2,1)} %k_hbm.1, bf16[1024,128]{1,0:T(8,128)(2,1)} %v_hbm.1, bf16[128,256]{1,0:T(8,128)(2,1)} %copy-done.7), custom_call_target="tpu_custom_call" | custom-call | tf_op jit(solution)/shard_map/attend/pallas_call | solution.py:171
  17.8 4.9 %all-to-all-start = ((bf16[8,128,256]{2,1,0:T(8,128)(2,1)}), bf16[8,128,256]{2,1,0:T(8,128)(2,1)}, u32[]{:S(2)}, u32[]{:S(2)}) async-start(bf16[8,128,256]{2,1,0:T(8,128)(2,1)} %attend.1), calls=%async_computation | async-start | bytes 1048576 | tf_op jit(solution)/shard_map/all_to_all | solution.py:551
  22.6 2.0 %collective-permute-start.9 = (bf16[2048,256]{1,0:T(8,128)(2,1)}, bf16[2048,256]{1,0:T(8,128)(2,1)}, u32[]{:S(2)}, u32[]{:S(2)}) collective-permute-start(bf16[2048,256]{1,0:T(8,128)(2,1)} %bitcast.23), channel_id=1, source_target_pairs={{0,2},{1,3},{2,0},{3,1},{4,6},{5,7},{6,4},{7,5},{8,10},{9,11},{10,... | collective-permute-start | bytes 3145736 | tf_op jit(solution)/shard_map/ppermute | solution.py:31
  25.2 7.4 %collective-permute-done.13.refs_3_.refs_2_ = bf16[256,1024]{1,0:T(8,128)(2,1)} collective-permute-done((bf16[256,1024]{1,0:T(8,128)(2,1)}, bf16[256,1024]{1,0:T(8,128)(2,1)}, u32[]{:S(2)}, u32[]{:S(2)}) %collective-permute-start.13) | collective-permute-done | bytes 524320 | tf_op jit(solution)/shard_map/ppermute | solution.py:31
  32.6 28.1 %all-to-all-done.att_ref = bf16[8,128,256]{2,1,0:T(8,128)(2,1)} async-done(((bf16[8,128,256]{2,1,0:T(8,128)(2,1)}), bf16[8,128,256]{2,1,0:T(8,128)(2,1)}, u32[]{:S(2)}, u32[]{:S(2)}) %all-to-all-start) | async-done | bytes 524320 | tf_op jit(solution)/shard_map/all_to_all | solution.py:551
  60.7 6.2 %project.1 = (bf16[128,2048]{1,0:T(8,128)(2,1)}, bf16[128,1024]{1,0:T(8,128)(2,1)}, bf16[128,1024]{1,0:T(8,128)(2,1)}) custom-call(bf16[8,128,256]{2,1,0:T(8,128)(2,1)} %all-to-all-done.att_ref, bf16[2048,2048]{1,0:T(8,128)(2,1)} %w_hbm.1, bf16[128,2048]{1,0:T(8,128)(2,1)} %res_ref.1, f32[1,2048]{1,0:T(1,128)} %bitcast.29), custom_call_target="tpu_custom_call" | custom-call | tf_op jit(solution)/shard_map/project/pallas_call | solution.py:286
  66.9 3.0 %collective-permute-start.23 = (bf16[128,1024]{1,0:T(8,128)(2,1)}, bf16[128,1024]{1,0:T(8,128)(2,1)S(1)}, u32[]{:S(2)}, u32[]{:S(2)}) collective-permute-start(bf16[128,1024]{1,0:T(8,128)(2,1)} %get-tuple-element.36.refs_1_), channel_id=1, source_target_pairs={{0,4},{1,5},{2,6},{3,7},{4,0},{5,1},{6,2},{7,3},{8,12},{9,13},{10,... | collective-permute-start | bytes 786440 | tf_op jit(solution)/shard_map/ppermute | solution.py:31
  69.9 18.0 %collective-permute-done.9.refs_10_.refs_14_ = bf16[2048,256]{1,0:T(8,128)(2,1)} collective-permute-done((bf16[2048,256]{1,0:T(8,128)(2,1)}, bf16[2048,256]{1,0:T(8,128)(2,1)}, u32[]{:S(2)}, u32[]{:S(2)}) %collective-permute-start.9) | collective-permute-done | bytes 1048608 | tf_op jit(solution)/shard_map/ppermute | solution.py:31
  88.5 2.0 %collective-permute-start.19 = (bf16[128,1024]{1,0:T(8,128)(2,1)}, bf16[128,1024]{1,0:T(8,128)(2,1)S(1)}, u32[]{:S(2)}, u32[]{:S(2)}) collective-permute-start(bf16[128,1024]{1,0:T(8,128)(2,1)} %get-tuple-element.35.refs_0_), channel_id=1, source_target_pairs={{0,4},{1,5},{2,6},{3,7},{4,0},{5,1},{6,2},{7,3},{8,12},{9,13},{10,... | collective-permute-start | bytes 786440 | tf_op jit(solution)/shard_map/ppermute | solution.py:31
  91.7 1.6 collective-permute-start.24
  93.3 10.2 %collective-permute-done.19.refs_0_ = bf16[128,1024]{1,0:T(8,128)(2,1)S(1)} collective-permute-done((bf16[128,1024]{1,0:T(8,128)(2,1)}, bf16[128,1024]{1,0:T(8,128)(2,1)S(1)}, u32[]{:S(2)}, u32[]{:S(2)}) %collective-permute-start.19) | collective-permute-done | bytes 262176 | tf_op jit(solution)/shard_map/ppermute | solution.py:31
  103.5 1.7 collective-permute-start.25
  105.2 1.4 collective-permute-start.26
  106.9 5.4 %collective-permute-done.25.refs_6_ = bf16[80,1024]{1,0:T(8,128)(2,1)S(1)} collective-permute-done((bf16[80,1024]{1,0:T(8,128)(2,1)S(1)}, bf16[80,1024]{1,0:T(8,128)(2,1)S(1)}, u32[]{:S(2)}, u32[]{:S(2)}) %collective-permute-start.25) | collective-permute-done | bytes 163872 | tf_op jit(solution)/shard_map/ppermute | solution.py:31
  112.3 1.7 collective-permute-start.20
  114.0 1.5 collective-permute-start.21
  115.5 2.1 %collective-permute-done.20.refs_1_ = bf16[80,1024]{1,0:T(8,128)(2,1)S(1)} collective-permute-done((bf16[80,1024]{1,0:T(8,128)(2,1)S(1)}, bf16[80,1024]{1,0:T(8,128)(2,1)S(1)}, u32[]{:S(2)}, u32[]{:S(2)}) %collective-permute-start.20) | collective-permute-done | bytes 163872 | tf_op jit(solution)/shard_map/ppermute | solution.py:31
  117.6 1.7 collective-permute-done.21.refs_2_
  119.3 1.5 collective-permute-start.22
  120.8 0.9 copy-done.4
  121.7 0.9 copy-done.5
  123.2 2.3 %collective-permute-done.22.refs_3_ = bf16[80,1024]{1,0:T(8,128)(2,1)S(1)} collective-permute-done((bf16[80,1024]{1,0:T(8,128)(2,1)S(1)}, bf16[80,1024]{1,0:T(8,128)(2,1)S(1)}, u32[]{:S(2)}, u32[]{:S(2)}) %collective-permute-start.22) | collective-permute-done | bytes 163872 | tf_op jit(solution)/shard_map/ppermute | solution.py:31
  125.5 1.3 collective-permute-start.2
  126.8 1.5 collective-permute-start.3
  129.0 4.4 %shard_map.123.hidden_ref = bf16[320,1024]{1,0:T(8,128)(2,1)S(1)} custom-call(bf16[80,1024]{1,0:T(8,128)(2,1)S(1)} %get-tuple-element.47.refs_0_, bf16[80,1024]{1,0:T(8,128)(2,1)S(1)} %collective-permute-done.20.refs_1_, bf16[80,1024]{1,0:T(8,128)(2,1)S(1)} %collective-permute-done.21.refs_2_, bf16[80,1024]{1,0:T(8,128)(2,1)S(1)} %collective-permute-done.22.refs_3_, ...), custom_call_target="tpu_custom_call" | custom-call | tf_op jit(solution)/shard_map/pallas_call | solution.py:375
  133.4 2.1 %shard_map.126 = (bf16[80,1024]{1,0:T(8,128)(2,1)S(1)}, bf16[80,1024]{1,0:T(8,128)(2,1)S(1)}, bf16[80,1024]{1,0:T(8,128)(2,1)S(1)}, bf16[80,1024]{1,0:T(8,128)(2,1)S(1)}) custom-call(bf16[320,1024]{1,0:T(8,128)(2,1)S(1)} %shard_map.123.hidden_ref, bf16[256,2048]{1,0:T(8,128)(2,1)S(1)} %bitcast.16, bf16[256,2048]{1,0:T(8,128)(2,1)S(1)} %collective-permute-done.11.refs_1_, ...), custom_call_target="tpu_custom_call" | custom-call | tf_op jit(solution)/shard_map/pallas_call | solution.py:442
  135.5 1.4 collective-permute-start.31
  136.9 2.0 %shard_map.124 = (bf16[80,1024]{1,0:T(8,128)(2,1)S(1)}, bf16[80,1024]{1,0:T(8,128)(2,1)S(1)}, bf16[80,1024]{1,0:T(8,128)(2,1)S(1)}, bf16[80,1024]{1,0:T(8,128)(2,1)S(1)}) custom-call(bf16[320,1024]{1,0:T(8,128)(2,1)S(1)} %shard_map.123.hidden_ref, bf16[256,2048]{1,0:T(8,128)(2,1)S(1)} %bitcast.17, bf16[256,2048]{1,0:T(8,128)(2,1)S(1)} %collective-permute-done.11.refs_1_, ...), custom_call_target="tpu_custom_call" | custom-call | tf_op jit(solution)/shard_map/pallas_call | solution.py:442
  138.8 2.5 %collective-permute-done.refs_1_ = f32[2,128]{1,0:T(2,128)S(1)} collective-permute-done((f32[2,128]{1,0:T(2,128)S(1)}, f32[2,128]{1,0:T(2,128)S(1)}, u32[]{:S(2)}, u32[]{:S(2)}) %collective-permute-start) | collective-permute-done | bytes 1056 | tf_op jit(solution)/shard_map/ppermute | solution.py:31
  142.1 1.5 collective-permute-start.28
  143.6 1.2 collective-permute-start.29
  144.8 1.5 collective-permute-start.32
  146.7 2.2 %collective-permute-start.33 = (bf16[80,1024]{1,0:T(8,128)(2,1)S(1)}, bf16[80,1024]{1,0:T(8,128)(2,1)S(1)}, u32[]{:S(2)}, u32[]{:S(2)}) collective-permute-start(bf16[80,1024]{1,0:T(8,128)(2,1)S(1)} %get-tuple-element.62), channel_id=1, source_target_pairs={{0,24},{8,16},{16,8},{24,0},{1,25},{9,17},{17,9},{25,1},{2,26},{10... | collective-permute-start | bytes 491528 | tf_op jit(solution)/shard_map/ppermute | solution.py:31
  148.9 4.5 %shard_map.120.hidden_ref = bf16[320,1024]{1,0:T(8,128)(2,1)S(1)} custom-call(bf16[80,2048]{1,0:T(8,128)(2,1)S(1)} %get-tuple-element.37.refs_0_, bf16[80,2048]{1,0:T(8,128)(2,1)S(1)} %collective-permute-done.2.refs_1_, bf16[80,2048]{1,0:T(8,128)(2,1)S(1)} %collective-permute-done.3.refs_2_, bf16[80,2048]{1,0:T(8,128)(2,1)S(1)} %collective-permute-done.4.refs_3_, ...), custom_call_target="tpu_custom_call" | custom-call | tf_op jit(solution)/shard_map/pallas_call | solution.py:375
  153.4 2.9 %shard_map.121 = (bf16[80,2048]{1,0:T(8,128)(2,1)S(1)}, bf16[80,2048]{1,0:T(8,128)(2,1)S(1)}, bf16[80,2048]{1,0:T(8,128)(2,1)S(1)}, bf16[80,2048]{1,0:T(8,128)(2,1)S(1)}) custom-call(bf16[320,1024]{1,0:T(8,128)(2,1)S(1)} %shard_map.120.hidden_ref, bf16[256,2048]{1,0:T(8,128)(2,1)S(1)} %bitcast.18, bf16[256,2048]{1,0:T(8,128)(2,1)S(1)} %collective-permute-done.11.refs_1_, ...), custom_call_target="tpu_custom_call" | custom-call | tf_op jit(solution)/shard_map/pallas_call | solution.py:442
  157.7 2.2 %collective-permute-start.18 = (bf16[80,2048]{1,0:T(8,128)(2,1)S(1)}, bf16[80,2048]{1,0:T(8,128)(2,1)S(1)}, u32[]{:S(2)}, u32[]{:S(2)}) collective-permute-start(bf16[80,2048]{1,0:T(8,128)(2,1)S(1)} %get-tuple-element.46), channel_id=1, source_target_pairs={{0,24},{8,16},{16,8},{24,0},{1,25},{9,17},{17,9},{25,1},{2,26},{10... | collective-permute-start | bytes 983048 | tf_op jit(solution)/shard_map/ppermute | solution.py:31
  161.7 3.0 %collective-permute-start.34 = (bf16[128,1024]{1,0:T(8,128)(2,1)S(1)}, bf16[128,1024]{1,0:T(8,128)(2,1)S(1)}, u32[]{:S(2)}, u32[]{:S(2)}) collective-permute-start(bf16[128,1024]{1,0:T(8,128)(2,1)S(1)} %shard_map.127), channel_id=1, source_target_pairs={{0,4},{1,5},{2,6},{3,7},{4,0},{5,1},{6,2},{7,3},{8,12},{9,13},{10,... | collective-permute-start | bytes 786440 | tf_op jit(solution)/shard_map/ppermute | solution.py:31
  164.7 1.0 collective-permute-done.16.refs_1_
  165.7 5.1 %collective-permute-done.17.refs_2_ = bf16[80,2048]{1,0:T(8,128)(2,1)S(1)} collective-permute-done((bf16[80,2048]{1,0:T(8,128)(2,1)S(1)}, bf16[80,2048]{1,0:T(8,128)(2,1)S(1)}, u32[]{:S(2)}, u32[]{:S(2)}) %collective-permute-start.17) | collective-permute-done | bytes 327712 | tf_op jit(solution)/shard_map/ppermute | solution.py:31
  170.8 1.2 shard_map.122.own_ref
  172.1 5.7 %collective-permute-done.30.refs_0_ = bf16[128,1024]{1,0:T(8,128)(2,1)S(1)} collective-permute-done((bf16[128,1024]{1,0:T(8,128)(2,1)S(1)}, bf16[128,1024]{1,0:T(8,128)(2,1)S(1)}, u32[]{:S(2)}, u32[]{:S(2)}) %collective-permute-start.30) | collective-permute-done | bytes 262176 | tf_op jit(solution)/shard_map/ppermute | solution.py:31
  177.7 4.6 %collective-permute-done.34.refs_1_ = bf16[128,1024]{1,0:T(8,128)(2,1)S(1)} collective-permute-done((bf16[128,1024]{1,0:T(8,128)(2,1)S(1)}, bf16[128,1024]{1,0:T(8,128)(2,1)S(1)}, u32[]{:S(2)}, u32[]{:S(2)}) %collective-permute-start.34) | collective-permute-done | bytes 262176 | tf_op jit(solution)/shard_map/ppermute | solution.py:31
  182.3 0.9 finish.1
  (60 shorter events, 9.2 us)
Async XLA Ops:
  0.0 88.0 %copy-start = (bf16[1,256,2048]{2,1,0:T(8,128)(2,1)S(1)}, bf16[1,256,2048]{2,1,0:T(8,128)(2,1)}, u32[]{:S(2)}) copy-start(bf16[1,256,2048]{2,1,0:T(8,128)(2,1)} %param.23) | copy-start | bytes 3145732
  0.0 129.0 %copy-start.1 = (bf16[1,2048,256]{2,1,0:T(8,128)(2,1)S(1)}, bf16[1,2048,256]{2,1,0:T(8,128)(2,1)}, u32[]{:S(2)}) copy-start(bf16[1,2048,256]{2,1,0:T(8,128)(2,1)} %param.21) | copy-start | bytes 3145732
  0.0 129.0 %copy-start.2 = (bf16[1,2048,256]{2,1,0:T(8,128)(2,1)S(1)}, bf16[1,2048,256]{2,1,0:T(8,128)(2,1)}, u32[]{:S(2)}) copy-start(bf16[1,2048,256]{2,1,0:T(8,128)(2,1)} %param.22) | copy-start | bytes 3145732
  2.4 22.3 %collective-permute-start.12 = (bf16[256,1024]{1,0:T(8,128)(2,1)}, bf16[256,1024]{1,0:T(8,128)(2,1)}, u32[]{:S(2)}, u32[]{:S(2)}) collective-permute-start(bf16[256,1024]{1,0:T(8,128)(2,1)} %get-tuple-element.41), channel_id=1, source_target_pairs={{0,2},{1,3},{2,0},{3,1},{4,6},{5,7},{6,4},{7,5},{8,10},{9,11},{10,... | collective-permute-start | bytes 1572872 | tf_op jit(solution)/shard_map/ppermute | solution.py:31
  5.5 27.1 %collective-permute-start.13 = (bf16[256,1024]{1,0:T(8,128)(2,1)}, bf16[256,1024]{1,0:T(8,128)(2,1)}, u32[]{:S(2)}, u32[]{:S(2)}) collective-permute-start(bf16[256,1024]{1,0:T(8,128)(2,1)} %get-tuple-element.42), channel_id=1, source_target_pairs={{0,2},{1,3},{2,0},{3,1},{4,6},{5,7},{6,4},{7,5},{8,10},{9,11},{10,... | collective-permute-start | bytes 1572872 | tf_op jit(solution)/shard_map/ppermute | solution.py:31
  7.0 6.0 %collective-permute-start.1 = (bf16[128,256]{1,0:T(8,128)(2,1)}, bf16[128,256]{1,0:T(8,128)(2,1)S(1)}, u32[]{:S(2)}, u32[]{:S(2)}) collective-permute-start(bf16[128,256]{1,0:T(8,128)(2,1)} %first_moves.1), channel_id=1, source_target_pairs={{0,8},{8,16},{16,24},{1,9},{9,17},{17,25},{2,10},{10,18},{18,26},{... | collective-permute-start | bytes 196616 | tf_op jit(solution)/shard_map/ppermute | solution.py:36
  10.7 59.2 %collective-permute-start.6 = (bf16[2048,256]{1,0:T(8,128)(2,1)}, bf16[2048,256]{1,0:T(8,128)(2,1)}, u32[]{:S(2)}, u32[]{:S(2)}) collective-permute-start(bf16[2048,256]{1,0:T(8,128)(2,1)} %bitcast.19), channel_id=1, source_target_pairs={{0,2},{1,3},{2,0},{3,1},{4,6},{5,7},{6,4},{7,5},{8,10},{9,11},{10,... | collective-permute-start | bytes 3145736 | tf_op jit(solution)/shard_map/ppermute | solution.py:31
  12.9 0.6 copy-start.7
  17.8 42.9 %all-to-all-start = ((bf16[8,128,256]{2,1,0:T(8,128)(2,1)}), bf16[8,128,256]{2,1,0:T(8,128)(2,1)}, u32[]{:S(2)}, u32[]{:S(2)}) async-start(bf16[8,128,256]{2,1,0:T(8,128)(2,1)} %attend.1), calls=%async_computation | async-start | bytes 1048576 | tf_op jit(solution)/shard_map/all_to_all | solution.py:551
  22.6 65.3 %collective-permute-start.9 = (bf16[2048,256]{1,0:T(8,128)(2,1)}, bf16[2048,256]{1,0:T(8,128)(2,1)}, u32[]{:S(2)}, u32[]{:S(2)}) collective-permute-start(bf16[2048,256]{1,0:T(8,128)(2,1)} %bitcast.23), channel_id=1, source_target_pairs={{0,2},{1,3},{2,0},{3,1},{4,6},{5,7},{6,4},{7,5},{8,10},{9,11},{10,... | collective-permute-start | bytes 3145736 | tf_op jit(solution)/shard_map/ppermute | solution.py:31
  24.7 63.3 %collective-permute-start.5 = (bf16[2048,256]{1,0:T(8,128)(2,1)}, bf16[2048,256]{1,0:T(8,128)(2,1)}, u32[]{:S(2)}, u32[]{:S(2)}) collective-permute-start(bf16[2048,256]{1,0:T(8,128)(2,1)} %bitcast.20), channel_id=1, source_target_pairs={{0,1},{1,0},{2,3},{3,2},{4,5},{5,4},{6,7},{7,6},{8,9},{9,8},{10,11... | collective-permute-start | bytes 3145736 | tf_op jit(solution)/shard_map/ppermute | solution.py:31
  24.7 67.0 %collective-permute-start.8 = (bf16[2048,256]{1,0:T(8,128)(2,1)}, bf16[2048,256]{1,0:T(8,128)(2,1)}, u32[]{:S(2)}, u32[]{:S(2)}) collective-permute-start(bf16[2048,256]{1,0:T(8,128)(2,1)} %bitcast.24), channel_id=1, source_target_pairs={{0,1},{1,0},{2,3},{3,2},{4,5},{5,4},{6,7},{7,6},{8,9},{9,8},{10,11... | collective-permute-start | bytes 3145736 | tf_op jit(solution)/shard_map/ppermute | solution.py:31
  32.6 34.3 %collective-permute-start.15 = (bf16[256,1024]{1,0:T(8,128)(2,1)}, bf16[256,1024]{1,0:T(8,128)(2,1)}, u32[]{:S(2)}, u32[]{:S(2)}) collective-permute-start(bf16[256,1024]{1,0:T(8,128)(2,1)} %collective-permute-done.13.refs_3_.refs_2_), channel_id=1, source_target_pairs={{0,1},{1,0},{2,3},{3,2},{4,5},{5,4},{6,7},{7,6},{8,9},{9,8},{10,11... | collective-permute-start | bytes 1572872 | tf_op jit(solution)/shard_map/ppermute | solution.py:31
  66.9 70.0 %copy-start.6 = (f32[128,2]{0,1:T(2,128)S(1)}, f32[128,2]{0,1:T(2,128)}, u32[]{:S(2)}) copy-start(f32[128,2]{0,1:T(2,128)} %param.20) | copy-start | bytes 3076
  66.9 21.5 %collective-permute-start.23 = (bf16[128,1024]{1,0:T(8,128)(2,1)}, bf16[128,1024]{1,0:T(8,128)(2,1)S(1)}, u32[]{:S(2)}, u32[]{:S(2)}) collective-permute-start(bf16[128,1024]{1,0:T(8,128)(2,1)} %get-tuple-element.36.refs_1_), channel_id=1, source_target_pairs={{0,4},{1,5},{2,6},{3,7},{4,0},{5,1},{6,2},{7,3},{8,12},{9,13},{10,... | collective-permute-start | bytes 786440 | tf_op jit(solution)/shard_map/ppermute | solution.py:31
  69.9 56.9 %collective-permute-start.7 = (bf16[2048,256]{1,0:T(8,128)(2,1)}, bf16[2048,256]{1,0:T(8,128)(2,1)}, u32[]{:S(2)}, u32[]{:S(2)}) collective-permute-start(bf16[2048,256]{1,0:T(8,128)(2,1)} %collective-permute-done.6.refs_6_.refs_10_), channel_id=1, source_target_pairs={{0,1},{1,0},{2,3},{3,2},{4,5},{5,4},{6,7},{7,6},{8,9},{9,8},{10,11... | collective-permute-start | bytes 3145736 | tf_op jit(solution)/shard_map/ppermute | solution.py:31
  87.9 40.4 %collective-permute-start.10 = (bf16[2048,256]{1,0:T(8,128)(2,1)}, bf16[2048,256]{1,0:T(8,128)(2,1)}, u32[]{:S(2)}, u32[]{:S(2)}) collective-permute-start(bf16[2048,256]{1,0:T(8,128)(2,1)} %collective-permute-done.9.refs_10_.refs_14_), channel_id=1, source_target_pairs={{0,1},{1,0},{2,3},{3,2},{4,5},{5,4},{6,7},{7,6},{8,9},{9,8},{10,11... | collective-permute-start | bytes 3145736 | tf_op jit(solution)/shard_map/ppermute | solution.py:31
  88.0 45.4 %collective-permute-start.11 = (bf16[256,2048]{1,0:T(8,128)(2,1)S(1)}, bf16[256,2048]{1,0:T(8,128)(2,1)S(1)}, u32[]{:S(2)}, u32[]{:S(2)}) collective-permute-start(bf16[256,2048]{1,0:T(8,128)(2,1)S(1)} %bitcast.15), channel_id=1, source_target_pairs={{0,1},{1,0},{2,3},{3,2},{4,5},{5,4},{6,7},{7,6},{8,9},{9,8},{10,11... | collective-permute-start | bytes 3145736 | tf_op jit(solution)/shard_map/ppermute | solution.py:31
  88.5 15.0 %collective-permute-start.19 = (bf16[128,1024]{1,0:T(8,128)(2,1)}, bf16[128,1024]{1,0:T(8,128)(2,1)S(1)}, u32[]{:S(2)}, u32[]{:S(2)}) collective-permute-start(bf16[128,1024]{1,0:T(8,128)(2,1)} %get-tuple-element.35.refs_0_), channel_id=1, source_target_pairs={{0,4},{1,5},{2,6},{3,7},{4,0},{5,1},{6,2},{7,3},{8,12},{9,13},{10,... | collective-permute-start | bytes 786440 | tf_op jit(solution)/shard_map/ppermute | solution.py:31
  91.7 13.4 %collective-permute-start.24 = (bf16[80,1024]{1,0:T(8,128)(2,1)S(1)}, bf16[80,1024]{1,0:T(8,128)(2,1)S(1)}, u32[]{:S(2)}, u32[]{:S(2)}) collective-permute-start(bf16[80,1024]{1,0:T(8,128)(2,1)S(1)} %get-tuple-element.52), channel_id=1, source_target_pairs={{0,8},{8,0},{16,24},{24,16},{1,9},{9,1},{17,25},{25,17},{2,10},{10... | collective-permute-start | bytes 491528 | tf_op jit(solution)/shard_map/ppermute | solution.py:31
  103.5 8.8 %collective-permute-start.25 = (bf16[80,1024]{1,0:T(8,128)(2,1)S(1)}, bf16[80,1024]{1,0:T(8,128)(2,1)S(1)}, u32[]{:S(2)}, u32[]{:S(2)}) collective-permute-start(bf16[80,1024]{1,0:T(8,128)(2,1)S(1)} %get-tuple-element.53), channel_id=1, source_target_pairs={{0,16},{8,24},{16,0},{24,8},{1,17},{9,25},{17,1},{25,9},{2,18},{10... | collective-permute-start | bytes 491528 | tf_op jit(solution)/shard_map/ppermute | solution.py:31
  105.2 8.8 %collective-permute-start.26 = (bf16[80,1024]{1,0:T(8,128)(2,1)S(1)}, bf16[80,1024]{1,0:T(8,128)(2,1)S(1)}, u32[]{:S(2)}, u32[]{:S(2)}) collective-permute-start(bf16[80,1024]{1,0:T(8,128)(2,1)S(1)} %get-tuple-element.54), channel_id=1, source_target_pairs={{0,24},{8,16},{16,8},{24,0},{1,25},{9,17},{17,9},{25,1},{2,26},{10... | collective-permute-start | bytes 491528 | tf_op jit(solution)/shard_map/ppermute | solution.py:31
  112.3 5.3 %collective-permute-start.20 = (bf16[80,1024]{1,0:T(8,128)(2,1)S(1)}, bf16[80,1024]{1,0:T(8,128)(2,1)S(1)}, u32[]{:S(2)}, u32[]{:S(2)}) collective-permute-start(bf16[80,1024]{1,0:T(8,128)(2,1)S(1)} %get-tuple-element.48), channel_id=1, source_target_pairs={{0,8},{8,0},{16,24},{24,16},{1,9},{9,1},{17,25},{25,17},{2,10},{10... | collective-permute-start | bytes 491528 | tf_op jit(solution)/shard_map/ppermute | solution.py:31
  114.0 5.3 %collective-permute-start.21 = (bf16[80,1024]{1,0:T(8,128)(2,1)S(1)}, bf16[80,1024]{1,0:T(8,128)(2,1)S(1)}, u32[]{:S(2)}, u32[]{:S(2)}) collective-permute-start(bf16[80,1024]{1,0:T(8,128)(2,1)S(1)} %get-tuple-element.49), channel_id=1, source_target_pairs={{0,16},{8,24},{16,0},{24,8},{1,17},{9,25},{17,1},{25,9},{2,18},{10... | collective-permute-start | bytes 491528 | tf_op jit(solution)/shard_map/ppermute | solution.py:31
  117.6 19.2 %collective-permute-start.14 = (bf16[256,1024]{1,0:T(8,128)(2,1)}, bf16[256,1024]{1,0:T(8,128)(2,1)S(1)}, u32[]{:S(2)}, u32[]{:S(2)}) collective-permute-start(bf16[256,1024]{1,0:T(8,128)(2,1)} %collective-permute-done.12.refs_2_), channel_id=1, source_target_pairs={{0,1},{1,0},{2,3},{3,2},{4,5},{5,4},{6,7},{7,6},{8,9},{9,8},{10,11... | collective-permute-start | bytes 1572872 | tf_op jit(solution)/shard_map/ppermute | solution.py:31
  119.3 6.2 %collective-permute-start.22 = (bf16[80,1024]{1,0:T(8,128)(2,1)S(1)}, bf16[80,1024]{1,0:T(8,128)(2,1)S(1)}, u32[]{:S(2)}, u32[]{:S(2)}) collective-permute-start(bf16[80,1024]{1,0:T(8,128)(2,1)S(1)} %get-tuple-element.50), channel_id=1, source_target_pairs={{0,24},{8,16},{16,8},{24,0},{1,25},{9,17},{17,9},{25,1},{2,26},{10... | collective-permute-start | bytes 491528 | tf_op jit(solution)/shard_map/ppermute | solution.py:31
  120.8 0.9 copy-start.4
  121.7 0.9 copy-start.5
  125.5 16.6 %collective-permute-start.2 = (bf16[80,2048]{1,0:T(8,128)(2,1)S(1)}, bf16[80,2048]{1,0:T(8,128)(2,1)S(1)}, u32[]{:S(2)}, u32[]{:S(2)}) collective-permute-start(bf16[80,2048]{1,0:T(8,128)(2,1)S(1)} %get-tuple-element.38), channel_id=1, source_target_pairs={{0,8},{8,0},{16,24},{24,16},{1,9},{9,1},{17,25},{25,17},{2,10},{10... | collective-permute-start | bytes 983048 | tf_op jit(solution)/shard_map/ppermute | solution.py:31
  126.8 16.8 %collective-permute-start.3 = (bf16[80,2048]{1,0:T(8,128)(2,1)S(1)}, bf16[80,2048]{1,0:T(8,128)(2,1)S(1)}, u32[]{:S(2)}, u32[]{:S(2)}) collective-permute-start(bf16[80,2048]{1,0:T(8,128)(2,1)S(1)} %get-tuple-element.39), channel_id=1, source_target_pairs={{0,16},{8,24},{16,0},{24,8},{1,17},{9,25},{17,1},{25,9},{2,18},{10... | collective-permute-start | bytes 983048 | tf_op jit(solution)/shard_map/ppermute | solution.py:31
  128.3 16.5 %collective-permute-start.4 = (bf16[80,2048]{1,0:T(8,128)(2,1)S(1)}, bf16[80,2048]{1,0:T(8,128)(2,1)S(1)}, u32[]{:S(2)}, u32[]{:S(2)}) collective-permute-start(bf16[80,2048]{1,0:T(8,128)(2,1)S(1)} %get-tuple-element.40), channel_id=1, source_target_pairs={{0,24},{8,16},{16,8},{24,0},{1,25},{9,17},{17,9},{25,1},{2,26},{10... | collective-permute-start | bytes 983048 | tf_op jit(solution)/shard_map/ppermute | solution.py:31
  135.5 11.2 %collective-permute-start.31 = (bf16[80,1024]{1,0:T(8,128)(2,1)S(1)}, bf16[80,1024]{1,0:T(8,128)(2,1)S(1)}, u32[]{:S(2)}, u32[]{:S(2)}) collective-permute-start(bf16[80,1024]{1,0:T(8,128)(2,1)S(1)} %get-tuple-element.60), channel_id=1, source_target_pairs={{0,8},{8,0},{16,24},{24,16},{1,9},{9,1},{17,25},{25,17},{2,10},{10... | collective-permute-start | bytes 491528 | tf_op jit(solution)/shard_map/ppermute | solution.py:31
  136.9 4.5 %collective-permute-start = (f32[2,128]{1,0:T(2,128)S(1)}, f32[2,128]{1,0:T(2,128)S(1)}, u32[]{:S(2)}, u32[]{:S(2)}) collective-permute-start(f32[2,128]{1,0:T(2,128)S(1)} %bitcast.27), channel_id=1, source_target_pairs={{0,4},{1,5},{2,6},{3,7},{4,0},{5,1},{6,2},{7,3},{8,12},{9,13},{10,... | collective-permute-start | bytes 3080 | tf_op jit(solution)/shard_map/ppermute | solution.py:31
  141.3 15.0 %collective-permute-start.27 = (bf16[80,1024]{1,0:T(8,128)(2,1)S(1)}, bf16[80,1024]{1,0:T(8,128)(2,1)S(1)}, u32[]{:S(2)}, u32[]{:S(2)}) collective-permute-start(bf16[80,1024]{1,0:T(8,128)(2,1)S(1)} %get-tuple-element.56), channel_id=1, source_target_pairs={{0,8},{8,0},{16,24},{24,16},{1,9},{9,1},{17,25},{25,17},{2,10},{10... | collective-permute-start | bytes 491528 | tf_op jit(solution)/shard_map/ppermute | solution.py:31
  142.1 15.1 %collective-permute-start.28 = (bf16[80,1024]{1,0:T(8,128)(2,1)S(1)}, bf16[80,1024]{1,0:T(8,128)(2,1)S(1)}, u32[]{:S(2)}, u32[]{:S(2)}) collective-permute-start(bf16[80,1024]{1,0:T(8,128)(2,1)S(1)} %get-tuple-element.57), channel_id=1, source_target_pairs={{0,16},{8,24},{16,0},{24,8},{1,17},{9,25},{17,1},{25,9},{2,18},{10... | collective-permute-start | bytes 491528 | tf_op jit(solution)/shard_map/ppermute | solution.py:31
  143.6 14.1 %collective-permute-start.29 = (bf16[80,1024]{1,0:T(8,128)(2,1)S(1)}, bf16[80,1024]{1,0:T(8,128)(2,1)S(1)}, u32[]{:S(2)}, u32[]{:S(2)}) collective-permute-start(bf16[80,1024]{1,0:T(8,128)(2,1)S(1)} %get-tuple-element.58), channel_id=1, source_target_pairs={{0,24},{8,16},{16,8},{24,0},{1,25},{9,17},{17,9},{25,1},{2,26},{10... | collective-permute-start | bytes 491528 | tf_op jit(solution)/shard_map/ppermute | solution.py:31
  144.8 16.1 %collective-permute-start.32 = (bf16[80,1024]{1,0:T(8,128)(2,1)S(1)}, bf16[80,1024]{1,0:T(8,128)(2,1)S(1)}, u32[]{:S(2)}, u32[]{:S(2)}) collective-permute-start(bf16[80,1024]{1,0:T(8,128)(2,1)S(1)} %get-tuple-element.61), channel_id=1, source_target_pairs={{0,16},{8,24},{16,0},{24,8},{1,17},{9,25},{17,1},{25,9},{2,18},{10... | collective-permute-start | bytes 491528 | tf_op jit(solution)/shard_map/ppermute | solution.py:31
  146.7 14.4 %collective-permute-start.33 = (bf16[80,1024]{1,0:T(8,128)(2,1)S(1)}, bf16[80,1024]{1,0:T(8,128)(2,1)S(1)}, u32[]{:S(2)}, u32[]{:S(2)}) collective-permute-start(bf16[80,1024]{1,0:T(8,128)(2,1)S(1)} %get-tuple-element.62), channel_id=1, source_target_pairs={{0,24},{8,16},{16,8},{24,0},{1,25},{9,17},{17,9},{25,1},{2,26},{10... | collective-permute-start | bytes 491528 | tf_op jit(solution)/shard_map/ppermute | solution.py:31
  148.9 21.9 %copy-start.3 = (bf16[128,2048]{1,0:T(8,128)(2,1)S(1)}, bf16[128,2048]{1,0:T(8,128)(2,1)}, u32[]{:S(2)}) copy-start(bf16[128,2048]{1,0:T(8,128)(2,1)} %get-tuple-element.34.stream_ref) | copy-start | bytes 1572868
  156.3 9.4 %collective-permute-start.16 = (bf16[80,2048]{1,0:T(8,128)(2,1)S(1)}, bf16[80,2048]{1,0:T(8,128)(2,1)S(1)}, u32[]{:S(2)}, u32[]{:S(2)}) collective-permute-start(bf16[80,2048]{1,0:T(8,128)(2,1)S(1)} %get-tuple-element.44), channel_id=1, source_target_pairs={{0,8},{8,0},{16,24},{24,16},{1,9},{9,1},{17,25},{25,17},{2,10},{10... | collective-permute-start | bytes 983048 | tf_op jit(solution)/shard_map/ppermute | solution.py:31
  157.2 13.6 %collective-permute-start.17 = (bf16[80,2048]{1,0:T(8,128)(2,1)S(1)}, bf16[80,2048]{1,0:T(8,128)(2,1)S(1)}, u32[]{:S(2)}, u32[]{:S(2)}) collective-permute-start(bf16[80,2048]{1,0:T(8,128)(2,1)S(1)} %get-tuple-element.45), channel_id=1, source_target_pairs={{0,16},{8,24},{16,0},{24,8},{1,17},{9,25},{17,1},{25,9},{2,18},{10... | collective-permute-start | bytes 983048 | tf_op jit(solution)/shard_map/ppermute | solution.py:31
  157.7 13.1 %collective-permute-start.18 = (bf16[80,2048]{1,0:T(8,128)(2,1)S(1)}, bf16[80,2048]{1,0:T(8,128)(2,1)S(1)}, u32[]{:S(2)}, u32[]{:S(2)}) collective-permute-start(bf16[80,2048]{1,0:T(8,128)(2,1)S(1)} %get-tuple-element.46), channel_id=1, source_target_pairs={{0,24},{8,16},{16,8},{24,0},{1,25},{9,17},{17,9},{25,1},{2,26},{10... | collective-permute-start | bytes 983048 | tf_op jit(solution)/shard_map/ppermute | solution.py:31
  161.0 16.8 %collective-permute-start.30 = (bf16[128,1024]{1,0:T(8,128)(2,1)S(1)}, bf16[128,1024]{1,0:T(8,128)(2,1)S(1)}, u32[]{:S(2)}, u32[]{:S(2)}) collective-permute-start(bf16[128,1024]{1,0:T(8,128)(2,1)S(1)} %shard_map.125), channel_id=1, source_target_pairs={{0,4},{1,5},{2,6},{3,7},{4,0},{5,1},{6,2},{7,3},{8,12},{9,13},{10,... | collective-permute-start | bytes 786440 | tf_op jit(solution)/shard_map/ppermute | solution.py:31
  161.7 20.5 %collective-permute-start.34 = (bf16[128,1024]{1,0:T(8,128)(2,1)S(1)}, bf16[128,1024]{1,0:T(8,128)(2,1)S(1)}, u32[]{:S(2)}, u32[]{:S(2)}) collective-permute-start(bf16[128,1024]{1,0:T(8,128)(2,1)S(1)} %shard_map.127), channel_id=1, source_target_pairs={{0,4},{1,5},{2,6},{3,7},{4,0},{5,1},{6,2},{7,3},{8,12},{9,13},{10,... | collective-permute-start | bytes 786440 | tf_op jit(solution)/shard_map/ppermute | solution.py:31
